TPU v7x, 128 devices: a whole 4x4x4 slice. The times are simulated.
128 devices in a mesh: ep: 128 (over z, y, x, core).
Axes of the slice: x: 4, y: 4, z: 4, core: 2. Of those that a mesh axis runs over, the one named last changes fastest.
Arguments:
- tokens: bfloat16 [512, 2048], P('ep'), may hold values from -6 to 6
- lengths: int32 [512], P('ep'), may hold values from 1 to 1023
- cache_keys: bfloat16 [512, 1024, 2, 128], P('ep')
- cache_values: bfloat16 [512, 1024, 2, 128], P('ep'), may hold values from -6 to 6
- query_w: bfloat16 [2048, 1024], replicated, may hold values from -0.125 to 0.125
- key_w: bfloat16 [2048, 256], replicated, may hold values from -0.125 to 0.125
- value_w: bfloat16 [2048, 256], replicated, may hold values from -0.125 to 0.125
- out_w: bfloat16 [1024, 2048], replicated, may hold values from -0.1875 to 0.1875
- mix_lambda: float32 [8], replicated, may hold values from 0.3 to 0.8
- head_gain: float32 [128], replicated, may hold values from 0.1 to 1.9
- attn_gain: float32 [2048], replicated, may hold values from 0.1 to 1.9
- ffn_gain: float32 [2048], replicated, may hold values from 0.1 to 1.9
- routes: int32 [512, 2], P('ep'), may hold values from 0 to 7, all different within a row; in each aligned block of 4 rows (0 to 3, 4 to 7, ...) at most 2 rows name the same one
- route_weights: float32 [512, 2], P('ep'), may hold values from 0.2 to 1
- exp_gate: bfloat16 [2048, 49152], P(None, 'ep'), may hold values from -0.125 to 0.125
- exp_up: bfloat16 [2048, 49152], P(None, 'ep'), may hold values from -0.125 to 0.125
- exp_down: bfloat16 [49152, 2048], P('ep'), may hold values from -0.078125 to 0.078125
- dense_gate: bfloat16 [128, 256, 352], P('ep'), may hold values from -0.125 to 0.125
- dense_up: bfloat16 [128, 256, 352], P('ep'), may hold values from -0.125 to 0.125
- dense_down: bfloat16 [128, 352, 256], P('ep'), may hold values from -0.078125 to 0.078125
- branch_gate: bfloat16 [2048], replicated, may hold values from -0.125 to 0.125
Outputs:
- output: bfloat16 [512, 2048], P('ep')
- new_keys: bfloat16 [512, 256], P('ep')
- new_values: bfloat16 [512, 256], P('ep')
Inputs may be any that keep to these rules, and one draw needn't show every extreme that they name: `routes`: each row names 2 different experts; among the 4 rows of one device no expert is named by more than 2 rows, a bound that some block reaches.
All inputs are finite; a program needn't handle non-finite values.
Results may differ from a plain program's by a relative error of at most 0.015.
Values may be sent and summed in bfloat16 or wider, within the bound.
No kernel may reach another device: no remote copies, remote signals or barrier semaphores. Data moves between devices by JAX's collectives and lax.ppermute only.
A program may use at most 128 MiB of HBM per device.

v0:
```python
import jax
import jax.numpy as jnp
from jax import lax
from jax.experimental import pallas as pl
from jax.experimental.pallas import tpu as pltpu
from jax.sharding import PartitionSpec as P

HEADS = 8
KV_HEADS = 2
HEAD_DIM = 128
DEVICES = 128
D = 2048
HALF = D // 2
UNITS = 48
PIECE = 3 * UNITS
TAIL = 128
f32 = jnp.float32
bf16 = jnp.bfloat16

def to_partner(x):
    return lax.ppermute(x, "ep", [(i, i ^ 1) for i in range(DEVICES)])


def rms_norm(values, gain, epsilon):
    scale = lax.rsqrt(jnp.mean(values * values, axis=-1, keepdims=True) + epsilon)
    return values * scale * gain


def softmax_pair(scores, own_score, valid):
    masked = jnp.where(valid, scores, -jnp.inf)
    largest = jnp.maximum(jnp.max(masked, axis=-1), own_score)
    raised = jnp.where(valid, jnp.exp(scores - largest[..., None]), 0.0)
    own_raised = jnp.exp(own_score - largest)
    total = jnp.sum(raised, axis=-1) + own_raised
    return (raised / total[..., None], own_raised / total)


def attend(tokens, lengths, cache_keys, cache_values, query_w, key_w, value_w, out_w, mix_lambda, head_gain, attn_gain, ffn_gain):
    rows = tokens.shape[0]
    groups = HEADS // KV_HEADS
    half = HEAD_DIM // 2
    scale = half ** (-0.5)
    cache_len = cache_keys.shape[1]
    xfull = tokens.astype(f32)
    normed = rms_norm(xfull, attn_gain, 1e-06).astype(bf16)
    query = jnp.dot(normed, query_w, preferred_element_type=f32).astype(bf16)
    key_new = jnp.dot(normed, key_w, preferred_element_type=f32).astype(bf16)
    value_new = jnp.dot(normed, value_w, preferred_element_type=f32).astype(bf16)
    qheads = query.reshape(rows, KV_HEADS, groups, HEAD_DIM)
    knew = key_new.reshape(rows, KV_HEADS, HEAD_DIM)
    vnew = value_new.reshape(rows, KV_HEADS, HEAD_DIM)
    valid = (jnp.arange(cache_len, dtype=jnp.int32)[None, :] < lengths[:, None])[:, None, None, :]
    probs = []
    for lo in (0, half):
        part = slice(lo, lo + half)
        scores = jnp.einsum("sgqd,spgd->sgqp", qheads[..., part], cache_keys[..., part], preferred_element_type=f32) * scale
        own = jnp.einsum("sgqd,sgd->sgq", qheads[..., part], knew[..., part], preferred_element_type=f32) * scale
        probs.append(softmax_pair(scores, own, valid))
    (prob_one, own_one), (prob_two, own_two) = probs
    lam = mix_lambda.reshape(KV_HEADS, groups)
    weights = (prob_one - lam[None, :, :, None] * prob_two).astype(bf16)
    own_weights = (own_one - lam[None] * own_two).astype(bf16)
    mixed = jnp.einsum("sgqp,spgd->sgqd", weights, cache_values, preferred_element_type=f32)
    mixed = mixed + own_weights.astype(f32)[..., None] * vnew.astype(f32)[:, :, None, :]
    heads = rms_norm(mixed, head_gain, 1e-05).astype(bf16).reshape(rows, HEADS * HEAD_DIM)
    hidden_state = xfull + jnp.dot(heads, out_w, preferred_element_type=f32)
    ffn_in = rms_norm(hidden_state, ffn_gain, 1e-06).astype(bf16)
    return hidden_state, ffn_in, key_new, value_new


def pieces_kernel(gate, up, down, out):
    for m, ref in enumerate((gate, up, down)):
        for k in range(8):
            size = min(UNITS, ref.shape[0] - k * UNITS)
            out[k, m * UNITS : m * UNITS + size, :] = ref[k * UNITS : k * UNITS + size, :]
            if size < UNITS:
                out[k, m * UNITS + size : (m + 1) * UNITS, :] = jnp.zeros((UNITS - size, 256), bf16)


def dot(a, b):
    return jnp.dot(a, b, preferred_element_type=f32)


def ffn_kernel(ids, own, theirs, pieces, w_gate, w_up, w_down, branch, y_other, y_own, rows, near, far):
    core, expert = ids[0], ids[1]
    for side, ref in enumerate((own, theirs)):
        rows[side] = ref[...].reshape(512, HALF + TAIL)
    near[...] = jnp.zeros_like(near)
    far[...] = jnp.zeros_like(far)
    for b in range(8):
        near[b, 0:UNITS, :] = pieces[b, 0:UNITS, :]
        near[b, 128 : 128 + UNITS, :] = pieces[b, UNITS : 2 * UNITS, :]
        near[b, 64:72, :] = jnp.broadcast_to(branch[:, b * 256 : (b + 1) * 256], (8, 256))
        far[0:UNITS, b * 256 : (b + 1) * 256] = pieces[b, 2 * UNITS :, :]
    halves = (core, 1 - core)
    gate_sum = up_sum = both = None
    for side in range(2):
        base = pl.multiple_of(halves[side] * HALF, HALF)
        x = rows[side, :, 0:HALF]
        gate_part = dot(x, w_gate[pl.ds(base, HALF), :])
        up_part = dot(x, w_up[pl.ds(base, HALF), :])
        gate_sum = gate_part if side == 0 else gate_sum + gate_part
        up_sum = up_part if side == 0 else up_sum + up_part
        for j in range(4):
            xj = rows[side, :, j * 256 : (j + 1) * 256]
            term = lax.dot_general(xj, near[halves[side] * 4 + j], (((1,), (1,)), ((), ())), preferred_element_type=f32)
            both = term if both is None else both + term
    act = (gate_sum * jax.nn.sigmoid(gate_sum) * up_sum).astype(bf16)
    dense_gate = both[:, 0:128]
    dense_act = dense_gate * jax.nn.sigmoid(dense_gate) * both[:, 128:256]
    lane = lax.broadcasted_iota(jnp.int32, (512, 128), 1)
    gate = jax.nn.sigmoid(jnp.sum(jnp.where(lane == 64, dense_gate, 0.0), axis=1, keepdims=True))
    tail = rows[0, :, HALF : HALF + TAIL].astype(f32)
    weight = jnp.sum(jnp.where((lane == expert) | (lane == expert + 8), tail, 0.0), axis=1, keepdims=True)
    dense_act = jnp.where(lane < UNITS, dense_act, 0.0).astype(bf16)
    for side, ref in ((1, y_other), (0, y_own)):
        base = pl.multiple_of(halves[side] * HALF, HALF)
        total = weight * dot(act, w_down[:, pl.ds(base, HALF)]) + gate * dot(dense_act, far[:, pl.ds(base, HALF)])
        ref[...] = total.astype(ref.dtype)


def join_kernel(y_own, y_recv, out):
    out[...] = (y_own[...] + y_recv[...].astype(f32)).astype(bf16).reshape(128, 4, HALF)


def last_kernel(hidden, parts, out):
    for half in range(2):
        total = jnp.zeros((4, HALF), f32)
        for chip in range(64):
            total = total + parts[2 * chip + half].astype(f32)
        cols = slice(half * HALF, (half + 1) * HALF)
        out[:, cols] = (hidden[:, cols] + total).astype(bf16)


def call(kernel, outs, operands, scratch=(), ids=None):
    vmem = pl.BlockSpec(memory_space=pltpu.VMEM)
    specs = [vmem] * len(operands)
    if ids is not None:
        specs = [pl.BlockSpec(memory_space=pltpu.SMEM)] + specs
        operands = [ids] + list(operands)
    return pl.pallas_call(
        kernel,
        in_specs=specs,
        out_specs=[vmem] * len(outs),
        out_shape=[jax.ShapeDtypeStruct(s, d) for s, d in outs],
        scratch_shapes=list(scratch),
        compiler_params=pltpu.CompilerParams(vmem_limit_bytes=40 * 1024 * 1024),
        name=kernel.__name__,
    )(*operands)


def per_device(
    tokens, lengths, cache_keys, cache_values, query_w, key_w, value_w, out_w, mix_lambda, head_gain, attn_gain, ffn_gain,
    routes, route_weights, exp_gate, exp_up, exp_down, dense_gate, dense_up, dense_down, branch_gate,
):
    rows = tokens.shape[0]
    me = lax.axis_index("ep")
    core = me % 2
    ids = jnp.stack([core, me // 16]).astype(jnp.int32)

    (pieces,) = call(
        pieces_kernel,
        [((8, PIECE, 256), bf16)],
        [jnp.swapaxes(dense_gate[0], 0, 1), jnp.swapaxes(dense_up[0], 0, 1), dense_down[0]],
    )
    columns = [[16 * b + j for b in range(8)] for j in range(16)]
    pieces = lax.all_to_all(pieces, "ep", 0, 0, axis_index_groups=columns, tiled=True)

    hidden_state, ffn_in, key_new, value_new = attend(
        tokens, lengths, cache_keys, cache_values, query_w, key_w, value_w, out_w, mix_lambda, head_gain, attn_gain, ffn_gain
    )

    spread = jnp.sum(jnp.where(routes[:, :, None] == jnp.arange(8, dtype=jnp.int32), route_weights[:, :, None], 0.0), axis=1)
    upper = lax.reduce_precision(spread, 8, 7)
    tail = jnp.concatenate([upper, spread - upper, jnp.zeros((rows, TAIL - 16), f32)], axis=1).astype(bf16)
    pair = jnp.stack([jnp.concatenate([ffn_in[:, :HALF], tail], axis=1), jnp.concatenate([ffn_in[:, HALF:], tail], axis=1)])
    outgoing = jnp.broadcast_to(pair[None], (64, 2, rows, HALF + TAIL)).reshape(DEVICES, rows, HALF + TAIL)
    own = lax.all_to_all(outgoing, "ep", 0, 0, tiled=True)
    theirs = to_partner(own)
    y_other, y_own = call(
        ffn_kernel,
        [((512, HALF), bf16), ((512, HALF), f32)],
        [own, theirs, pieces, exp_gate, exp_up, exp_down, branch_gate.reshape(1, D)],
        [pltpu.VMEM((2, 512, HALF + TAIL), bf16), pltpu.VMEM((8, 256, 256), bf16), pltpu.VMEM((128, D), bf16)],
        ids,
    )
    y_recv = to_partner(y_other)
    (joined,) = call(join_kernel, [((DEVICES, rows, HALF), bf16)], [y_own, y_recv])
    parts = lax.all_to_all(joined, "ep", 0, 0, tiled=True)
    (output,) = call(last_kernel, [((rows, D), bf16)], [hidden_state, parts])
    return (output, key_new, value_new)


def solution(mesh):
    placed = (
        P("ep", None),
        P("ep"),
        P("ep", None, None, None),
        P("ep", None, None, None),
        P(),
        P(),
        P(),
        P(),
        P(),
        P(),
        P(),
        P(),
        P("ep", None),
        P("ep", None),
        P(None, "ep"),
        P(None, "ep"),
        P("ep", None),
        P("ep", None, None),
        P("ep", None, None),
        P("ep", None, None),
        P(),
    )
    return jax.shard_map(
        per_device,
        mesh=mesh,
        in_specs=placed,
        out_specs=(P("ep", None), P("ep", None), P("ep", None)),
        check_vma=False,
    )
```

profile of v0, /device:TPU:1, one launch (start us, length us, event | category | flops | bytes accessed | tf_op | source)
XLA Modules:
  0.0 111.2 jit_solution(12707274585435127854)
XLA Ops:
  0.6 0.0 copy-start
  0.6 0.0 copy-start.8
  0.7 0.0 copy-start.9
  0.7 0.0 copy-start.14
  0.7 0.0 copy-start.15
  0.7 1.0 fusion.26
  1.7 0.7 mul.107
  2.4 1.5 %convolution_convert_fusion.2 = bf16[4,256]{1,0:T(4,128)(2,1)S(1)} fusion(bf16[2048,256]{1,0:T(8,128)(2,1)} %param.26, bf16[4,2048]{1,0:T(4,128)(2,1)} %param.21, f32[2048]{0:T(1024)} %param.31, f32[4]{0:T(128)S(1)} %add_rsqrt_fusion.2), kind=kOutput, calls=%fused_computation.12 | convolution fusion | flops 4228096 | bytes 1075216 | tf_op jit(solution)/shard_map/dot_general | solution.py:47
  4.0 1.5 %convolution_convert_fusion.1 = bf16[4,256]{1,0:T(4,128)(2,1)S(1)} fusion(bf16[2048,256]{1,0:T(8,128)(2,1)} %param.27, bf16[4,2048]{1,0:T(4,128)(2,1)} %param.21, f32[2048]{0:T(1024)} %param.31, f32[4]{0:T(128)S(1)} %add_rsqrt_fusion.2), kind=kOutput, calls=%fused_computation.11 | convolution fusion | flops 4228096 | bytes 1075216 | tf_op jit(solution)/shard_map/dot_general | solution.py:48
  5.6 0.1 select_reduce_fusion.2
  5.7 0.1 slice_bitcast_fusion
  5.7 0.1 iota_compare_fusion
  5.8 2.9 %convolution_convert_fusion = bf16[4,1024]{1,0:T(4,128)(2,1)S(1)} fusion(bf16[2048,1024]{1,0:T(8,128)(2,1)} %param.25, bf16[4,2048]{1,0:T(4,128)(2,1)S(1)} %copy-done.8, f32[2048]{0:T(1024)S(1)} %copy-done.9, f32[4]{0:T(128)S(1)} %add_rsqrt_fusion.2), kind=kOutput, calls=%fused_computation.10 | convolution fusion | flops 16814080 | bytes 4227088 | tf_op jit(solution)/shard_map/dot_general | solution.py:46
  8.7 0.1 fusion.32
  8.9 0.2 fusion.29
  9.1 5.7 %fusion.45 = (bf16[4,1024,2,64]{3,2,1,0:T(2,128)(2,1)S(1)}, bf16[4,1024,2,64]{3,2,1,0:T(2,128)(2,1)S(1)}) fusion(bf16[4,1024,2,128]{3,2,1,0:T(2,128)(2,1)} %param.23), kind=kLoop, calls=%fused_computation.67 | loop fusion | bytes 4194304 | tf_op jit(solution)/shard_map/slice | solution.py:56
  14.7 0.7 select_reduce_fusion.1
  15.5 0.8 fusion.16
  16.3 0.2 fusion.17
  16.5 0.0 copy-start.16
  16.6 0.6 multiply_reduce_fusion.1
  17.2 0.0 copy-done.16
  17.2 0.1 multiply_convert_fusion.1
  17.3 3.0 %multiply_reduce_fusion = (f32[4]{0:T(128)S(1)}, f32[4,2048]{1,0:T(4,128)S(1)}) fusion(bf16[4,1024]{1,0:T(4,128)(2,1)S(1)} %reshape.85, bf16[1024,2048]{1,0:T(8,128)(2,1)} %param.28, bf16[4,2048]{1,0:T(4,128)(2,1)S(1)} %copy-done.8), kind=kOutput, calls=%fused_computation.34 | convolution fusion | flops 16809980 | bytes 4251664 | tf_op jit(solution)/shard_map/dot_general | solution.py:66
  20.3 0.0 copy-start.5
  20.3 0.1 multiply_convert_fusion
  20.4 0.1 concatenate.10
  20.5 0.1 concatenate.11
  20.6 0.3 broadcast_in_dim.71
  20.9 0.0 copy-start.13
  20.9 31.9 %all_to_all.15.own = bf16[128,4,1152]{2,1,0:T(4,128)(2,1)S(1)} all-to-all(bf16[128,4,1152]{2,1,0:T(4,128)(2,1)S(1)} %bitcast.28), channel_id=1, replica_groups=mesh['ep'=128] {'ep'}, dimensions={0} | all-to-all | bytes 2359296 | tf_op jit(solution)/shard_map/all_to_all | solution.py:178
  52.9 1.0 collective-permute-start
  53.8 0.9 copy-done.6
  54.8 0.9 copy-done.7
  55.7 0.8 copy-done.1
  56.6 4.2 %all-to-all-start.1 = ((bf16[8,144,256]{2,1,0:T(8,128)(2,1)}), bf16[8,144,256]{2,1,0:T(8,128)(2,1)}, u32[]{:S(2)}, u32[]{:S(2)}) async-start(bf16[8,144,256]{2,1,0:T(8,128)(2,1)} %copy-done.1), calls=%async_computation.1 | async-start | bytes 1179648 | tf_op jit(solution)/shard_map/all_to_all | solution.py:167
  60.8 0.1 pad_add_fusion.ids
  60.9 12.3 %all-to-all-done.1.pieces = bf16[8,144,256]{2,1,0:T(8,128)(2,1)} async-done(((bf16[8,144,256]{2,1,0:T(8,128)(2,1)}), bf16[8,144,256]{2,1,0:T(8,128)(2,1)}, u32[]{:S(2)}, u32[]{:S(2)}) %all-to-all-start.1) | async-done | bytes 589856 | tf_op jit(solution)/shard_map/all_to_all | solution.py:167
  73.1 0.0 collective-permute-done.theirs
  73.2 1.4 %copy-done.2 = bf16[2048,384]{1,0:T(8,128)(2,1)S(1)} copy-done((bf16[2048,384]{1,0:T(8,128)(2,1)S(1)}, bf16[2048,384]{1,0:T(8,128)(2,1)}, u32[]{:S(2)}) %copy-start.2) | copy-done | bytes 1572888
  74.6 1.4 %copy-done.3 = bf16[2048,384]{1,0:T(8,128)(2,1)S(1)} copy-done((bf16[2048,384]{1,0:T(8,128)(2,1)S(1)}, bf16[2048,384]{1,0:T(8,128)(2,1)}, u32[]{:S(2)}) %copy-start.3) | copy-done | bytes 1572888
  76.0 1.4 %copy-done.4 = bf16[384,2048]{1,0:T(8,128)(2,1)S(1)} copy-done((bf16[384,2048]{1,0:T(8,128)(2,1)S(1)}, bf16[384,2048]{1,0:T(8,128)(2,1)}, u32[]{:S(2)}) %copy-start.4) | copy-done | bytes 1572888
  77.4 7.0 %ffn_kernel.1 = (bf16[512,1024]{1,0:T(8,128)(2,1)S(1)}, f32[512,1024]{1,0:T(8,128)S(1)}) custom-call(s32[2]{0:T(128)S(1)} %pad_add_fusion.ids, bf16[128,4,1152]{2,1,0:T(4,128)(2,1)S(1)} %all_to_all.15.own, bf16[128,4,1152]{2,1,0:T(4,128)(2,1)} %collective-permute-done.theirs, bf16[8,144,256]{2,1,0:T(8,128)(2,1)} %all-to-all-done.1.pieces, ...), custom_call_target="tpu_custom_call" | custom-call | tf_op jit(solution)/shard_map/ffn_kernel/pallas_call | solution.py:141
  84.4 0.9 collective-permute-start.1
  85.3 2.3 %collective-permute-done.1.y_recv = bf16[512,1024]{1,0:T(8,128)(2,1)S(1)} collective-permute-done((bf16[512,1024]{1,0:T(8,128)(2,1)S(1)}, bf16[512,1024]{1,0:T(8,128)(2,1)S(1)}, u32[]{:S(2)}, u32[]{:S(2)}) %collective-permute-start.1) | collective-permute-done | bytes 1048608 | tf_op jit(solution)/shard_map/ppermute | solution.py:21
  87.6 0.2 join_kernel.1
  87.9 22.5 %all_to_all.16.parts = bf16[128,4,1024]{2,1,0:T(4,128)(2,1)S(1)} all-to-all(bf16[128,4,1024]{2,1,0:T(4,128)(2,1)S(1)} %join_kernel.1), channel_id=1, replica_groups=mesh['ep'=128] {'ep'}, dimensions={0} | all-to-all | bytes 2097152 | tf_op jit(solution)/shard_map/all_to_all | solution.py:189
  110.4 0.8 last_kernel.1
  (37 shorter events, 0.2 us)
Async XLA Ops:
  0.6 15.9 %copy-start = (bf16[4,1024,2,128]{3,2,1,0:T(2,128)(2,1)S(1)}, bf16[4,1024,2,128]{3,2,1,0:T(2,128)(2,1)}, u32[]{:S(2)}) copy-start(bf16[4,1024,2,128]{3,2,1,0:T(2,128)(2,1)} %param.24) | copy-start | bytes 6291460
  0.6 5.2 %copy-start.8 = (bf16[4,2048]{1,0:T(4,128)(2,1)S(1)}, bf16[4,2048]{1,0:T(4,128)(2,1)}, u32[]{:S(2)}) copy-start(bf16[4,2048]{1,0:T(4,128)(2,1)} %param.21) | copy-start | bytes 49156
  0.7 5.2 %copy-start.9 = (f32[2048]{0:T(1024)S(1)}, f32[2048]{0:T(1024)}, u32[]{:S(2)}) copy-start(f32[2048]{0:T(1024)} %param.31) | copy-start | bytes 24580
  0.7 4.9 %copy-start.14 = (f32[4,2]{0,1:T(2,128)S(1)}, f32[4,2]{0,1:T(2,128)}, u32[]{:S(2)}) copy-start(f32[4,2]{0,1:T(2,128)} %param.34) | copy-start | bytes 100
  0.7 4.9 %copy-start.15 = (s32[4,2]{0,1:T(2,128)S(1)}, s32[4,2]{0,1:T(2,128)}, u32[]{:S(2)}) copy-start(s32[4,2]{0,1:T(2,128)} %param.33) | copy-start | bytes 100
  0.7 5.0 %copy-start.17 = (s32[4]{0:T(128)S(1)}, s32[4]{0:T(128)}, u32[]{:S(2)}) copy-start(s32[4]{0:T(128)} %param.22) | copy-start | bytes 52
  4.0 4.7 %copy-start.11 = (bf16[4,256]{1,0:T(4,128)(2,1)}, bf16[4,256]{1,0:T(4,128)(2,1)S(1)}, u32[]{:S(2)}) copy-start(bf16[4,256]{1,0:T(4,128)(2,1)S(1)} %convolution_convert_fusion.2) | copy-start | bytes 6148
  5.5 3.2 %copy-start.10 = (bf16[4,256]{1,0:T(4,128)(2,1)}, bf16[4,256]{1,0:T(4,128)(2,1)S(1)}, u32[]{:S(2)}) copy-start(bf16[4,256]{1,0:T(4,128)(2,1)S(1)} %convolution_convert_fusion.1) | copy-start | bytes 6148
  16.5 0.7 copy-start.16
  17.3 3.0 %copy-start.12 = (f32[2048]{0:T(1024)S(1)}, f32[2048]{0:T(1024)}, u32[]{:S(2)}) copy-start(f32[2048]{0:T(1024)} %param.32) | copy-start | bytes 24580
  20.3 33.6 %copy-start.5 = (bf16[1,256,352]{1,2,0:T(8,128)(2,1)S(1)}, bf16[1,256,352]{1,2,0:T(8,128)(2,1)}, u32[]{:S(2)}) copy-start(bf16[1,256,352]{1,2,0:T(8,128)(2,1)} %param.38) | copy-start | bytes 540676
  20.9 39.8 %copy-start.13 = (bf16[2048]{0:T(1024)(128)(2,1)S(1)}, bf16[2048]{0:T(1024)(128)(2,1)}, u32[]{:S(2)}) copy-start(bf16[2048]{0:T(1024)(128)(2,1)} %param.41) | copy-start | bytes 12292
  52.9 20.3 %collective-permute-start = (bf16[128,4,1152]{2,1,0:T(4,128)(2,1)S(1)}, bf16[128,4,1152]{2,1,0:T(4,128)(2,1)}, u32[]{:S(2)}, u32[]{:S(2)}) collective-permute-start(bf16[128,4,1152]{2,1,0:T(4,128)(2,1)S(1)} %all_to_all.15.own), channel_id=1, source_target_pairs={{0,1},{1,0},{2,3},{3,2},{4,5},{5,4},{6,7},{7,6},{8,9},{9,8},{10,11... | collective-permute-start | bytes 3538952 | tf_op jit(solution)/shard_map/ppermute | solution.py:21
  53.8 0.9 copy-start.6
  54.8 0.9 copy-start.7
  55.7 0.8 copy-start.1
  56.6 16.6 %all-to-all-start.1 = ((bf16[8,144,256]{2,1,0:T(8,128)(2,1)}), bf16[8,144,256]{2,1,0:T(8,128)(2,1)}, u32[]{:S(2)}, u32[]{:S(2)}) async-start(bf16[8,144,256]{2,1,0:T(8,128)(2,1)} %copy-done.1), calls=%async_computation.1 | async-start | bytes 1179648 | tf_op jit(solution)/shard_map/all_to_all | solution.py:167
  73.2 1.4 %copy-start.2 = (bf16[2048,384]{1,0:T(8,128)(2,1)S(1)}, bf16[2048,384]{1,0:T(8,128)(2,1)}, u32[]{:S(2)}) copy-start(bf16[2048,384]{1,0:T(8,128)(2,1)} %w_gate.1) | copy-start | bytes 4718596
  74.6 1.4 %copy-start.3 = (bf16[2048,384]{1,0:T(8,128)(2,1)S(1)}, bf16[2048,384]{1,0:T(8,128)(2,1)}, u32[]{:S(2)}) copy-start(bf16[2048,384]{1,0:T(8,128)(2,1)} %w_up.1) | copy-start | bytes 4718596
  76.0 1.4 %copy-start.4 = (bf16[384,2048]{1,0:T(8,128)(2,1)S(1)}, bf16[384,2048]{1,0:T(8,128)(2,1)}, u32[]{:S(2)}) copy-start(bf16[384,2048]{1,0:T(8,128)(2,1)} %w_down.1) | copy-start | bytes 4718596
  84.4 3.2 %collective-permute-start.1 = (bf16[512,1024]{1,0:T(8,128)(2,1)S(1)}, bf16[512,1024]{1,0:T(8,128)(2,1)S(1)}, u32[]{:S(2)}, u32[]{:S(2)}) collective-permute-start(bf16[512,1024]{1,0:T(8,128)(2,1)S(1)} %get-tuple-element.6), channel_id=1, source_target_pairs={{0,1},{1,0},{2,3},{3,2},{4,5},{5,4},{6,7},{7,6},{8,9},{9,8},{10,11... | collective-permute-start | bytes 3145736 | tf_op jit(solution)/shard_map/ppermute | solution.py:21
where the time goes:
time: 112 us; the launch traced here: 111 us
  blocking collectives  54.4 us (49%)
  waiting for transfers between devices  14.6 us (13%)
  local copies, waits for them, and re-layouts  14 us (12%)
  matrix products  11.4 us (10%)
  Pallas kernels  8.06 us (7%)
  starting transfers between devices  6.1 us (5%)
  other arithmetic  1.68 us (2%)
    all_to_all x1, blocking collectives, per_device(): own = lax.all_to_all(outgoing, 'ep', 0, 0, tiled=True)  31.9 us
    all_to_all x1, blocking collectives, per_device(): parts = lax.all_to_all(joined, 'ep', 0, 0, tiled=True)  22.5 us
    all_to_all x1, waiting for transfers between devices, per_device(): lax.all_to_all(pieces, 'ep', 0, 0, axis_index_groups=columns, tiled=True)  12.3 us
    pallas_call x4, Pallas kernels, call(): pl.pallas_call(kernel, in_specs=specs, out_specs=[vmem] * len(outs), out_...  8.06 us
    unnamed x36, local copies, waits for them, and re-layouts  6.99 us
    slice x1, local copies, waits for them, and re-layouts, attend(): cache_keys[..., part]  5.66 us
    all_to_all x1, starting transfers between devices, per_device(): lax.all_to_all(pieces, 'ep', 0, 0, axis_index_groups=columns, tiled=True)  4.19 us
    dot_general x1, matrix products, attend(): hidden_state = xfull + jnp.dot(heads, out_w, preferred_element_type=f32)  2.96 us
  transfers between devices with their start and end apart: 3, of which 2 were waited for; matrix products, arithmetic and copies ran while one was open for 0% of the time, Pallas kernels for 0%

commit v1 on v0

v1 whole, which is shorter than its diff:
```python
import jax
import jax.numpy as jnp
from jax import lax
from jax.experimental import pallas as pl
from jax.experimental.pallas import tpu as pltpu
from jax.sharding import PartitionSpec as P


HEADS = 8
KV_HEADS = 2
HEAD_DIM = 128
DEVICES = 128
D = 2048
HALF = D // 2
UNITS = 48
PIECE = 3 * UNITS
TAIL = 128
f32 = jnp.float32
bf16 = jnp.bfloat16


def to_partner(x):
    return lax.ppermute(x, "ep", [(i, i ^ 1) for i in range(DEVICES)])


def rms_norm(values, gain, epsilon):
    scale = lax.rsqrt(jnp.mean(values * values, axis=-1, keepdims=True) + epsilon)
    return values * scale * gain


def dot_last(a, b):
    return lax.dot_general(a, b, (((1,), (1,)), ((), ())), preferred_element_type=f32)


def attend_kernel(
    lengths, routes, route_weights, tokens, mix_lambda, head_gain, attn_gain, ffn_gain,
    query_hbm, key_hbm, value_hbm, cache_keys, cache_values, out_hbm, gate_hbm, up_hbm, down_hbm,
    pair, hidden, key_new, value_new, w_gate, w_up, w_down,
    query_w, key_w, value_w, keys, values, out_w, sem, query_rows, head_rows,
):
    span = keys.shape[0] // 4
    copies = []

    def fetch(source, target):
        copies.append(pltpu.make_async_copy(source, target, sem.at[len(copies)]))
        copies[-1].start()
        return copies[-1]

    on_query = [fetch(query_hbm.at[pl.ds(k * 512, 512), :], query_w.at[pl.ds(k * 512, 512), :]) for k in range(4)]
    on_key = fetch(key_hbm, key_w)
    on_value = fetch(value_hbm, value_w)
    on_keys, on_values = [], []
    for s in range(4):
        on_keys.append(fetch(cache_keys.at[pl.ds(s * span, span), :], keys.at[pl.ds(s * span, span), :]))
    for s in range(4):
        on_values.append(fetch(cache_values.at[pl.ds(s * span, span), :], values.at[pl.ds(s * span, span), :]))
    on_out = [fetch(out_hbm.at[pl.ds(k * 256, 256), :], out_w.at[pl.ds(k * 256, 256), :]) for k in range(4)]
    ahead = [fetch(gate_hbm, w_gate), fetch(up_hbm, w_up), fetch(down_hbm, w_down)]

    x = tokens[...].astype(f32)
    normed = rms_norm(x, attn_gain[...], 1e-06).astype(bf16)
    query = None
    for k in range(4):
        on_query[k].wait()
        term = dot(normed[:, k * 512 : (k + 1) * 512], query_w[k * 512 : (k + 1) * 512, :])
        query = term if query is None else query + term
    query = query.astype(bf16).astype(f32)
    for s in range(4):
        for h in range(HEADS):
            query_rows[s * 8 + h : s * 8 + h + 1, :] = query[s : s + 1, h * HEAD_DIM : (h + 1) * HEAD_DIM]
    on_key.wait()
    knew = dot(normed, key_w[...]).astype(bf16)
    key_new[...] = knew
    on_value.wait()
    vnew = dot(normed, value_w[...]).astype(bf16)
    value_new[...] = vnew
    knew = knew.astype(f32)
    vnew = vnew.astype(f32)
    first = lax.broadcasted_iota(jnp.int32, (8, HEAD_DIM), 1) < HEAD_DIM // 2
    low_head = lax.broadcasted_iota(jnp.int32, (8, HEAD_DIM), 0) < 4
    lane = lax.broadcasted_iota(jnp.int32, (16, span), 1)
    row = lax.broadcasted_iota(jnp.int32, (16, span), 0)
    own_head = (lane & 1) == ((row >> 2) & 1)
    place = lane >> 1
    scale = (HEAD_DIM // 2) ** (-0.5)
    weights, own_weights = [], []
    for s in range(4):
        q = query_rows[s * 8 : s * 8 + 8, :]
        q = jnp.concatenate([jnp.where(first, q, 0.0), jnp.where(first, 0.0, q)])
        k_own = jnp.where(low_head, knew[s : s + 1, 0:HEAD_DIM], knew[s : s + 1, HEAD_DIM:])
        own = jnp.sum(q * jnp.concatenate([k_own, k_own]), axis=1, keepdims=True) * scale
        on_keys[s].wait()
        scores = dot_last(q.astype(bf16), keys[s * span : (s + 1) * span, :]) * scale
        scores = jnp.where(own_head & (place < lengths[s]), scores, -jnp.inf)
        largest = jnp.maximum(jnp.max(scores, axis=1, keepdims=True), own)
        raised = jnp.exp(scores - largest)
        own_raised = jnp.exp(own - largest)
        total = jnp.sum(raised, axis=1, keepdims=True) + own_raised
        prob = raised / total
        own_prob = own_raised / total
        lam = mix_lambda[...]
        weights.append((prob[0:8] - lam * prob[8:16]).astype(bf16))
        own_weights.append((own_prob[0:8] - lam * own_prob[8:16]).astype(bf16).astype(f32))
    for s in range(4):
        v_own = jnp.where(low_head, vnew[s : s + 1, 0:HEAD_DIM], vnew[s : s + 1, HEAD_DIM:])
        on_values[s].wait()
        mixed = dot(weights[s], values[s * span : (s + 1) * span, :]) + own_weights[s] * v_own
        heads = rms_norm(mixed, head_gain[...], 1e-05)
        for h in range(HEADS):
            head_rows[s : s + 1, h * HEAD_DIM : (h + 1) * HEAD_DIM] = heads[h : h + 1, :]
    heads = head_rows[...].astype(bf16)
    state = x
    for k in range(4):
        on_out[k].wait()
        state = state + dot(heads[:, k * 256 : (k + 1) * 256], out_w[k * 256 : (k + 1) * 256, :])
    hidden[...] = state
    ffn_in = rms_norm(state, ffn_gain[...], 1e-06).astype(bf16)
    lane = lax.broadcasted_iota(jnp.int32, (4, TAIL), 1)
    row = lax.broadcasted_iota(jnp.int32, (4, TAIL), 0)
    tail = jnp.zeros((4, TAIL), f32)
    for t in range(4):
        for k in range(2):
            weight = jnp.full((4, TAIL), route_weights[t, k], f32)
            upper = weight.astype(bf16).astype(f32)
            there = row == t
            tail = jnp.where(there & (lane == routes[t, k]), upper, tail)
            tail = jnp.where(there & (lane == routes[t, k] + 8), weight - upper, tail)
    for half in range(2):
        pair[half, :, 0:HALF] = ffn_in[:, half * HALF : (half + 1) * HALF]
        pair[half, :, HALF:] = tail.astype(bf16)
    for copy in ahead:
        copy.wait()


def pieces_kernel(gate, up, down, out, sem):
    copies = []
    for m, ref in enumerate((gate, up, down)):
        for k in range(8):
            size = min(UNITS, ref.shape[0] - k * UNITS)
            source = ref.at[pl.ds(k * UNITS, size), :]
            target = out.at[k, pl.ds(m * UNITS, size), :]
            copies.append(pltpu.make_async_copy(source, target, sem.at[m * 8 + k]))
            copies[-1].start()
            if size < UNITS:
                out[k, m * UNITS + size : (m + 1) * UNITS, :] = jnp.zeros((UNITS - size, 256), bf16)
    for copy in copies:
        copy.wait()


def dot(a, b):
    return jnp.dot(a, b, preferred_element_type=f32)


def ffn_kernel(ids, own, theirs, pieces, branch, w_gate, w_up, w_down, y_other, y_own, rows, near, far):
    core, expert = ids[0], ids[1]
    for side, ref in enumerate((own, theirs)):
        rows[side] = ref[...].reshape(512, HALF + TAIL)
    near[...] = jnp.zeros_like(near)
    far[...] = jnp.zeros_like(far)
    for b in range(8):
        near[b, 0:UNITS, :] = pieces[b, 0:UNITS, :]
        near[b, 128 : 128 + UNITS, :] = pieces[b, UNITS : 2 * UNITS, :]
        near[b, 64:72, :] = jnp.broadcast_to(branch[:, b * 256 : (b + 1) * 256], (8, 256))
        far[0:UNITS, b * 256 : (b + 1) * 256] = pieces[b, 2 * UNITS :, :]
    halves = (core, 1 - core)
    gate_sum = up_sum = both = None
    for side in range(2):
        base = pl.multiple_of(halves[side] * HALF, HALF)
        x = rows[side, :, 0:HALF]
        gate_part = dot(x, w_gate[pl.ds(base, HALF), :])
        up_part = dot(x, w_up[pl.ds(base, HALF), :])
        gate_sum = gate_part if side == 0 else gate_sum + gate_part
        up_sum = up_part if side == 0 else up_sum + up_part
        for j in range(4):
            xj = rows[side, :, j * 256 : (j + 1) * 256]
            term = lax.dot_general(xj, near[halves[side] * 4 + j], (((1,), (1,)), ((), ())), preferred_element_type=f32)
            both = term if both is None else both + term
    act = (gate_sum * jax.nn.sigmoid(gate_sum) * up_sum).astype(bf16)
    dense_gate = both[:, 0:128]
    dense_act = dense_gate * jax.nn.sigmoid(dense_gate) * both[:, 128:256]
    lane = lax.broadcasted_iota(jnp.int32, (512, 128), 1)
    gate = jax.nn.sigmoid(jnp.sum(jnp.where(lane == 64, dense_gate, 0.0), axis=1, keepdims=True))
    tail = rows[0, :, HALF : HALF + TAIL].astype(f32)
    weight = jnp.sum(jnp.where((lane == expert) | (lane == expert + 8), tail, 0.0), axis=1, keepdims=True)
    dense_act = jnp.where(lane < UNITS, dense_act, 0.0).astype(bf16)
    for side, ref in ((1, y_other), (0, y_own)):
        base = pl.multiple_of(halves[side] * HALF, HALF)
        total = weight * dot(act, w_down[:, pl.ds(base, HALF)]) + gate * dot(dense_act, far[:, pl.ds(base, HALF)])
        ref[...] = total.astype(ref.dtype)


def join_kernel(y_own, y_recv, out):
    out[...] = (y_own[...] + y_recv[...].astype(f32)).astype(bf16).reshape(128, 4, HALF)


def last_kernel(hidden, parts, out):
    for half in range(2):
        total = jnp.zeros((4, HALF), f32)
        for chip in range(64):
            total = total + parts[2 * chip + half].astype(f32)
        cols = slice(half * HALF, (half + 1) * HALF)
        out[:, cols] = (hidden[:, cols] + total).astype(bf16)


def call(kernel, outs, operands, scratch=(), spaces=None):
    spaces = spaces or {}
    operands = [pltpu.with_memory_space_constraint(x, pltpu.HBM) if spaces.get(k) is pltpu.HBM else x for k, x in enumerate(operands)]
    return pl.pallas_call(
        kernel,
        in_specs=[pl.BlockSpec(memory_space=spaces.get(k, pltpu.VMEM)) for k in range(len(operands))],
        out_specs=[pl.BlockSpec(memory_space=pltpu.VMEM)] * len(outs),
        out_shape=[pltpu.VMEM(shape, kind) if local else jax.ShapeDtypeStruct(shape, kind) for shape, kind, local in outs],
        scratch_shapes=list(scratch),
        compiler_params=pltpu.CompilerParams(vmem_limit_bytes=36 * 1024 * 1024),
    )(*operands)


def per_device(
    tokens, lengths, cache_keys, cache_values, query_w, key_w, value_w, out_w, mix_lambda, head_gain, attn_gain, ffn_gain,
    routes, route_weights, exp_gate, exp_up, exp_down, dense_gate, dense_up, dense_down, branch_gate,
):
    rows = tokens.shape[0]
    me = lax.axis_index("ep")
    core = me % 2
    ids = jnp.stack([core, me // 16]).astype(jnp.int32)

    smem, hbm = pltpu.SMEM, pltpu.HBM
    (pieces,) = call(
        pieces_kernel,
        [((8, PIECE, 256), bf16, True)],
        [jnp.swapaxes(dense_gate[0], 0, 1), jnp.swapaxes(dense_up[0], 0, 1), dense_down[0]],
        [pltpu.SemaphoreType.DMA((24,))],
        {0: hbm, 1: hbm, 2: hbm},
    )
    columns = [[16 * b + j for b in range(8)] for j in range(16)]
    pieces = lax.all_to_all(pieces, "ep", 0, 0, axis_index_groups=columns, tiled=True)

    positions = cache_keys.shape[0] * cache_keys.shape[1] * KV_HEADS
    pair, hidden_state, key_new, value_new, w_gate, w_up, w_down = call(
        attend_kernel,
        [
            ((2, rows, HALF + TAIL), bf16, True), ((rows, D), f32, True),
            ((rows, KV_HEADS * HEAD_DIM), bf16, False), ((rows, KV_HEADS * HEAD_DIM), bf16, False),
            (exp_gate.shape, bf16, True), (exp_up.shape, bf16, True), (exp_down.shape, bf16, True),
        ],
        [
            lengths, routes, route_weights, tokens, mix_lambda.reshape(HEADS, 1), head_gain.reshape(1, HEAD_DIM),
            attn_gain.reshape(1, D), ffn_gain.reshape(1, D), query_w, key_w, value_w,
            cache_keys.reshape(positions, HEAD_DIM), cache_values.reshape(positions, HEAD_DIM), out_w, exp_gate, exp_up, exp_down,
        ],
        [
            pltpu.VMEM(query_w.shape, bf16), pltpu.VMEM(key_w.shape, bf16), pltpu.VMEM(value_w.shape, bf16),
            pltpu.VMEM((positions, HEAD_DIM), bf16), pltpu.VMEM((positions, HEAD_DIM), bf16), pltpu.VMEM(out_w.shape, bf16),
            pltpu.SemaphoreType.DMA((21,)), pltpu.VMEM((32, HEAD_DIM), f32), pltpu.VMEM((rows, HEADS * HEAD_DIM), f32),
        ],
        {0: smem, 1: smem, 2: smem, **{k: hbm for k in range(8, 17)}},
    )
    outgoing = jnp.broadcast_to(pair[None], (64, 2, rows, HALF + TAIL)).reshape(DEVICES, rows, HALF + TAIL)
    outgoing, pieces = lax.optimization_barrier((outgoing, pieces))
    own = lax.all_to_all(outgoing, "ep", 0, 0, tiled=True)
    theirs = to_partner(own)
    y_other, y_own = call(
        ffn_kernel,
        [((512, HALF), bf16, True), ((512, HALF), f32, True)],
        [ids, own, theirs, pieces, branch_gate.reshape(1, D), w_gate, w_up, w_down],
        [pltpu.VMEM((2, 512, HALF + TAIL), bf16), pltpu.VMEM((8, 256, 256), bf16), pltpu.VMEM((128, D), bf16)],
        {0: smem},
    )
    y_recv = to_partner(y_other)
    (joined,) = call(join_kernel, [((DEVICES, rows, HALF), bf16, True)], [y_own, y_recv])
    parts = lax.all_to_all(joined, "ep", 0, 0, tiled=True)
    (output,) = call(last_kernel, [((rows, D), bf16, False)], [hidden_state, parts])
    return (output, key_new, value_new)


def solution(mesh):
    placed = (
        P("ep", None),
        P("ep"),
        P("ep", None, None, None),
        P("ep", None, None, None),
        P(),
        P(),
        P(),
        P(),
        P(),
        P(),
        P(),
        P(),
        P("ep", None),
        P("ep", None),
        P(None, "ep"),
        P(None, "ep"),
        P("ep", None),
        P("ep", None, None),
        P("ep", None, None),
        P("ep", None, None),
        P(),
    )

    return jax.shard_map(
        per_device,
        mesh=mesh,
        in_specs=placed,
        out_specs=(P("ep", None), P("ep", None), P("ep", None)),
        check_vma=False,
    )
```

time: 112 us -> 93.8 us (0.84)
  matrix products: 11.4 us -> 0 us
  Pallas kernels: 8.06 us -> 18.7 us
  waiting for transfers between devices: 14.6 us -> 4.85 us
  local copies, waits for them, and re-layouts: 14 us -> 5.73 us
  starting transfers between devices: 6.1 us -> 9.91 us
  other arithmetic: 1.68 us -> 0.08 us
    all_to_all x1, waiting for transfers between devices: 12.3 us -> 0.06 us  [per_device(): lax.all_to_all(pieces, 'ep', 0, 0, axis_index_groups=columns, tiled=True)]
    dot_general x9 -> x0, matrix products: 11.4 us -> none  [the longest x1 2.96 us: attend(): hidden_state = xfull + jnp.dot(heads, out_w, preferred_element_type=f32)]
    pallas_call x4 -> x5, Pallas kernels: 8.06 us -> 18.7 us  [call(): pl.pallas_call(kernel, in_specs=[pl.BlockSpec(memory_space=spaces.get(k,...]
    slice x3 -> x0, local copies, waits for them, and re-layouts: 5.74 us -> none  [the longest x1 5.66 us: attend(): cache_keys[..., part]]
    all_to_all x1, starting transfers between devices: 4.19 us -> 8.49 us  [per_device(): lax.all_to_all(pieces, 'ep', 0, 0, axis_index_groups=columns, tiled=True)]
    ppermute x2, waiting for transfers between devices: 2.29 us -> 4.78 us  [to_partner(): return lax.ppermute(x, 'ep', [(i, i ^ 1) for i in range(DEVICES)])]
    unnamed x36 -> x28, local copies, waits for them, and re-layouts: 6.99 us -> 5.34 us
    all_to_all x1, blocking collectives: 31.9 us -> 30.6 us  [per_device(): own = lax.all_to_all(outgoing, 'ep', 0, 0, tiled=True)]
  transfers between devices with their start and end apart: 3 -> 3, of which waited for: 2 -> 3; matrix products, arithmetic and copies ran while one was open for 0% -> 0% of each run, Pallas kernels for 0% -> 9%
where the time goes in v1:
time: 93.8 us; the launch traced here: 93.4 us
  blocking collectives  53.4 us (57%)
  Pallas kernels  18.7 us (20%)
  starting transfers between devices  9.91 us (11%)
  local copies, waits for them, and re-layouts  5.73 us (6%)
  waiting for transfers between devices  4.85 us (5%)
    all_to_all x1, blocking collectives, per_device(): own = lax.all_to_all(outgoing, 'ep', 0, 0, tiled=True)  30.6 us
    all_to_all x1, blocking collectives, per_device(): parts = lax.all_to_all(joined, 'ep', 0, 0, tiled=True)  22.8 us
    pallas_call x5, Pallas kernels, call(): pl.pallas_call(kernel, in_specs=[pl.BlockSpec(memory_space=spaces.get(k,...  18.7 us
    all_to_all x1, starting transfers between devices, per_device(): lax.all_to_all(pieces, 'ep', 0, 0, axis_index_groups=columns, tiled=True)  8.49 us
    unnamed x28, local copies, waits for them, and re-layouts  5.34 us
    ppermute x2, waiting for transfers between devices, to_partner(): return lax.ppermute(x, 'ep', [(i, i ^ 1) for i in range(DEVICES)])  4.78 us
  transfers between devices with their start and end apart: 3, of which 3 were waited for; matrix products, arithmetic and copies ran while one was open for 0% of the time, Pallas kernels for 9%

profile of v1, /device:TPU:1, one launch (start us, length us, event | category | flops | bytes accessed | tf_op | source)
XLA Modules:
  0.0 93.4 jit_solution(1541976481786837927)
XLA Ops:
  0.6 0.0 copy-start.10
  0.6 0.0 copy-start.11
  0.7 0.0 copy-start.12
  0.7 0.0 copy-start.6
  0.7 0.0 copy-start.5
  0.7 0.0 copy-start.8
  0.7 0.0 copy-start.7
  0.7 0.0 copy-start.4
  0.7 2.0 %shard_map.221 = bf16[8,144,256]{2,1,0:T(8,128)(2,1)} custom-call(bf16[352,256]{1,0:T(8,128)(2,1)} %bitcast.22, bf16[352,256]{1,0:T(8,128)(2,1)} %bitcast.23, bf16[352,256]{1,0:T(8,128)(2,1)} %bitcast.24), custom_call_target="tpu_custom_call" | custom-call | tf_op jit(solution)/shard_map/pallas_call | solution.py:208
  2.8 8.5 %all-to-all-start = ((bf16[8,144,256]{2,1,0:T(8,128)(2,1)}), bf16[8,144,256]{2,1,0:T(8,128)(2,1)S(1)}, u32[]{:S(2)}, u32[]{:S(2)}) async-start(bf16[8,144,256]{2,1,0:T(8,128)(2,1)} %shard_map.221), calls=%async_computation | async-start | bytes 1179648 | tf_op jit(solution)/shard_map/all_to_all | solution.py:236
  11.3 0.0 copy-done.10
  11.3 0.1 copy.24.routes
  11.4 0.0 copy-done.11
  11.4 0.1 copy.25.route_weights
  11.4 0.0 copy-done.12
  11.5 0.1 copy.26.mix_lambda
  11.5 0.0 copy-done.6
  11.5 0.0 copy-done.5
  11.5 0.0 copy-done.8
  11.5 0.0 copy-done.7
  11.5 0.0 copy-done.4
  11.6 8.7 %shard_map.220 = (bf16[2,4,1152]{2,1,0:T(4,128)(2,1)S(1)}, f32[4,2048]{1,0:T(4,128)S(1)}, bf16[4,256]{1,0:T(4,128)(2,1)}, bf16[4,256]{1,0:T(4,128)(2,1)}, bf16[2...) custom-call(s32[4]{0:T(128)S(1)} %copy-done.7, s32[4,2]{1,0:T(4,128)S(1)} %copy.24.routes, ...), custom_call_target="tpu_custom_call" | custom-call | tf_op jit(solution)/shard_map/pallas_call | solution.py:208
  20.3 0.0 copy-start
  20.3 1.2 %copy-done = bf16[2048,384]{1,0:T(8,128)(2,1)} copy-done((bf16[2048,384]{1,0:T(8,128)(2,1)}, bf16[2048,384]{1,0:T(8,128)(2,1)S(1)}, u32[]{:S(2)}) %copy-start) | copy-done | bytes 1572888
  21.4 0.0 copy-start.2
  21.4 1.1 %copy-done.2 = bf16[384,2048]{1,0:T(8,128)(2,1)} copy-done((bf16[384,2048]{1,0:T(8,128)(2,1)}, bf16[384,2048]{1,0:T(8,128)(2,1)S(1)}, u32[]{:S(2)}) %copy-start.2) | copy-done | bytes 1572888
  22.6 0.1 all-to-all-done.pieces
  22.6 0.0 copy-start.9
  22.6 0.3 broadcast_in_dim.2
  23.0 30.6 %all_to_all.15.own = bf16[128,4,1152]{2,1,0:T(4,128)(2,1)S(1)} all-to-all(bf16[128,4,1152]{2,1,0:T(4,128)(2,1)S(1)} %bitcast.19), channel_id=1, replica_groups=mesh['ep'=128] {'ep'}, dimensions={0} | all-to-all | bytes 2359296 | tf_op jit(solution)/shard_map/all_to_all | solution.py:260
  53.5 1.0 %collective-permute-start = (bf16[128,4,1152]{2,1,0:T(4,128)(2,1)S(1)}, bf16[128,4,1152]{2,1,0:T(4,128)(2,1)}, u32[]{:S(2)}, u32[]{:S(2)}) collective-permute-start(bf16[128,4,1152]{2,1,0:T(4,128)(2,1)S(1)} %all_to_all.15.own), channel_id=1, source_target_pairs={{0,1},{1,0},{2,3},{3,2},{4,5},{5,4},{6,7},{7,6},{8,9},{9,8},{10,11... | collective-permute-start | bytes 3538952 | tf_op jit(solution)/shard_map/ppermute | solution.py:23
  54.5 0.0 copy-done.9
  54.5 0.1 pad_add_fusion.ids
  54.6 2.5 %collective-permute-done.theirs = bf16[128,4,1152]{2,1,0:T(4,128)(2,1)} collective-permute-done((bf16[128,4,1152]{2,1,0:T(4,128)(2,1)S(1)}, bf16[128,4,1152]{2,1,0:T(4,128)(2,1)}, u32[]{:S(2)}, u32[]{:S(2)}) %collective-permute-start) | collective-permute-done | bytes 1179680 | tf_op jit(solution)/shard_map/ppermute | solution.py:23
  57.1 0.0 copy-start.1
  57.1 1.4 %copy-done.1 = bf16[2048,384]{1,0:T(8,128)(2,1)S(1)} copy-done((bf16[2048,384]{1,0:T(8,128)(2,1)S(1)}, bf16[2048,384]{1,0:T(8,128)(2,1)}, u32[]{:S(2)}) %copy-start.1) | copy-done | bytes 1572888
  58.5 0.0 copy-start.3
  58.5 1.4 %copy-done.3 = bf16[384,2048]{1,0:T(8,128)(2,1)S(1)} copy-done((bf16[384,2048]{1,0:T(8,128)(2,1)S(1)}, bf16[384,2048]{1,0:T(8,128)(2,1)}, u32[]{:S(2)}) %copy-start.3) | copy-done | bytes 1572888
  59.9 6.9 %shard_map.222 = (bf16[512,1024]{1,0:T(8,128)(2,1)S(1)}, f32[512,1024]{1,0:T(8,128)S(1)}) custom-call(s32[2]{0:T(128)S(1)} %pad_add_fusion.ids, bf16[128,4,1152]{2,1,0:T(4,128)(2,1)S(1)} %all_to_all.15.own, bf16[128,4,1152]{2,1,0:T(4,128)(2,1)} %collective-permute-done.theirs, bf16[8,144,256]{2,1,0:T(8,128)(2,1)S(1)} %all-to-all-done.pieces, ...), custom_call_target="tpu_custom_call" | custom-call | tf_op jit(solution)/shard_map/pallas_call | solution.py:208
  66.8 0.5 collective-permute-start.1
  67.2 2.3 %collective-permute-done.1.y_recv = bf16[512,1024]{1,0:T(8,128)(2,1)S(1)} collective-permute-done((bf16[512,1024]{1,0:T(8,128)(2,1)S(1)}, bf16[512,1024]{1,0:T(8,128)(2,1)S(1)}, u32[]{:S(2)}, u32[]{:S(2)}) %collective-permute-start.1) | collective-permute-done | bytes 1048608 | tf_op jit(solution)/shard_map/ppermute | solution.py:23
  69.5 0.3 shard_map.223
  69.8 22.8 %all_to_all.16.parts = bf16[128,4,1024]{2,1,0:T(4,128)(2,1)S(1)} all-to-all(bf16[128,4,1024]{2,1,0:T(4,128)(2,1)S(1)} %shard_map.223), channel_id=1, replica_groups=mesh['ep'=128] {'ep'}, dimensions={0} | all-to-all | bytes 2097152 | tf_op jit(solution)/shard_map/all_to_all | solution.py:271
  92.6 0.8 shard_map.224
  (1 shorter events, 0.0 us)
Async XLA Ops:
  0.6 10.6 %copy-start.10 = (s32[4,2]{0,1:T(2,128)S(1)}, s32[4,2]{0,1:T(2,128)}, u32[]{:S(2)}) copy-start(s32[4,2]{0,1:T(2,128)} %param.33) | copy-start | bytes 100
  0.6 10.7 %copy-start.11 = (f32[4,2]{0,1:T(2,128)S(1)}, f32[4,2]{0,1:T(2,128)}, u32[]{:S(2)}) copy-start(f32[4,2]{0,1:T(2,128)} %param.34) | copy-start | bytes 100
  0.7 10.8 %copy-start.12 = (f32[8]{0:T(128)S(1)}, f32[8]{0:T(128)}, u32[]{:S(2)}) copy-start(f32[8]{0:T(128)} %param.29) | copy-start | bytes 100
  0.7 10.9 %copy-start.6 = (f32[2048]{0:T(1024)S(1)}, f32[2048]{0:T(1024)}, u32[]{:S(2)}) copy-start(f32[2048]{0:T(1024)} %param.32) | copy-start | bytes 24580
  0.7 10.9 %copy-start.5 = (f32[2048]{0:T(1024)S(1)}, f32[2048]{0:T(1024)}, u32[]{:S(2)}) copy-start(f32[2048]{0:T(1024)} %param.31) | copy-start | bytes 24580
  0.7 10.9 %copy-start.8 = (f32[128]{0:T(128)S(1)}, f32[128]{0:T(128)}, u32[]{:S(2)}) copy-start(f32[128]{0:T(128)} %param.30) | copy-start | bytes 1540
  0.7 10.8 %copy-start.7 = (s32[4]{0:T(128)S(1)}, s32[4]{0:T(128)}, u32[]{:S(2)}) copy-start(s32[4]{0:T(128)} %lengths.1) | copy-start | bytes 52
  0.7 10.8 %copy-start.4 = (bf16[4,2048]{1,0:T(4,128)(2,1)S(1)}, bf16[4,2048]{1,0:T(4,128)(2,1)}, u32[]{:S(2)}) copy-start(bf16[4,2048]{1,0:T(4,128)(2,1)} %tokens.1) | copy-start | bytes 49156
  2.8 19.9 %all-to-all-start = ((bf16[8,144,256]{2,1,0:T(8,128)(2,1)}), bf16[8,144,256]{2,1,0:T(8,128)(2,1)S(1)}, u32[]{:S(2)}, u32[]{:S(2)}) async-start(bf16[8,144,256]{2,1,0:T(8,128)(2,1)} %shard_map.221), calls=%async_computation | async-start | bytes 1179648 | tf_op jit(solution)/shard_map/all_to_all | solution.py:236
  20.3 1.2 %copy-start = (bf16[2048,384]{1,0:T(8,128)(2,1)}, bf16[2048,384]{1,0:T(8,128)(2,1)S(1)}, u32[]{:S(2)}) copy-start(bf16[2048,384]{1,0:T(8,128)(2,1)S(1)} %get-tuple-element.19.w_up) | copy-start | bytes 4718596
  21.4 1.1 %copy-start.2 = (bf16[384,2048]{1,0:T(8,128)(2,1)}, bf16[384,2048]{1,0:T(8,128)(2,1)S(1)}, u32[]{:S(2)}) copy-start(bf16[384,2048]{1,0:T(8,128)(2,1)S(1)} %get-tuple-element.20.w_down) | copy-start | bytes 4718596
  22.6 31.9 %copy-start.9 = (bf16[2048]{0:T(1024)(128)(2,1)S(1)}, bf16[2048]{0:T(1024)(128)(2,1)}, u32[]{:S(2)}) copy-start(bf16[2048]{0:T(1024)(128)(2,1)} %param.41) | copy-start | bytes 12292
  53.5 3.6 %collective-permute-start = (bf16[128,4,1152]{2,1,0:T(4,128)(2,1)S(1)}, bf16[128,4,1152]{2,1,0:T(4,128)(2,1)}, u32[]{:S(2)}, u32[]{:S(2)}) collective-permute-start(bf16[128,4,1152]{2,1,0:T(4,128)(2,1)S(1)} %all_to_all.15.own), channel_id=1, source_target_pairs={{0,1},{1,0},{2,3},{3,2},{4,5},{5,4},{6,7},{7,6},{8,9},{9,8},{10,11... | collective-permute-start | bytes 3538952 | tf_op jit(solution)/shard_map/ppermute | solution.py:23
  57.1 1.4 %copy-start.1 = (bf16[2048,384]{1,0:T(8,128)(2,1)S(1)}, bf16[2048,384]{1,0:T(8,128)(2,1)}, u32[]{:S(2)}) copy-start(bf16[2048,384]{1,0:T(8,128)(2,1)} %copy-done) | copy-start | bytes 4718596
  58.5 1.4 %copy-start.3 = (bf16[384,2048]{1,0:T(8,128)(2,1)S(1)}, bf16[384,2048]{1,0:T(8,128)(2,1)}, u32[]{:S(2)}) copy-start(bf16[384,2048]{1,0:T(8,128)(2,1)} %copy-done.2) | copy-start | bytes 4718596
  66.8 2.7 %collective-permute-start.1 = (bf16[512,1024]{1,0:T(8,128)(2,1)S(1)}, bf16[512,1024]{1,0:T(8,128)(2,1)S(1)}, u32[]{:S(2)}, u32[]{:S(2)}) collective-permute-start(bf16[512,1024]{1,0:T(8,128)(2,1)S(1)} %get-tuple-element.22), channel_id=1, source_target_pairs={{0,1},{1,0},{2,3},{3,2},{4,5},{5,4},{6,7},{7,6},{8,9},{9,8},{10,11... | collective-permute-start | bytes 3145736 | tf_op jit(solution)/shard_map/ppermute | solution.py:23

commit v2 on v1

--- a/solution.py
+++ b/solution.py
@@ -34,8 +34,8 @@
 
 def attend_kernel(
     lengths, routes, route_weights, tokens, mix_lambda, head_gain, attn_gain, ffn_gain,
-    query_hbm, key_hbm, value_hbm, cache_keys, cache_values, out_hbm, gate_hbm, up_hbm, down_hbm,
-    pair, hidden, key_new, value_new, w_gate, w_up, w_down,
+    query_hbm, key_hbm, value_hbm, cache_keys, cache_values, out_hbm,
+    pair, hidden, key_new, value_new,
     query_w, key_w, value_w, keys, values, out_w, sem, query_rows, head_rows,
 ):
     span = keys.shape[0] // 4
@@ -55,7 +55,6 @@
     for s in range(4):
         on_values.append(fetch(cache_values.at[pl.ds(s * span, span), :], values.at[pl.ds(s * span, span), :]))
     on_out = [fetch(out_hbm.at[pl.ds(k * 256, 256), :], out_w.at[pl.ds(k * 256, 256), :]) for k in range(4)]
-    ahead = [fetch(gate_hbm, w_gate), fetch(up_hbm, w_up), fetch(down_hbm, w_down)]
 
     x = tokens[...].astype(f32)
     normed = rms_norm(x, attn_gain[...], 1e-06).astype(bf16)
@@ -128,33 +127,52 @@
     for half in range(2):
         pair[half, :, 0:HALF] = ffn_in[:, half * HALF : (half + 1) * HALF]
         pair[half, :, HALF:] = tail.astype(bf16)
-    for copy in ahead:
-        copy.wait()
-
-
-def pieces_kernel(gate, up, down, out, sem):
-    copies = []
-    for m, ref in enumerate((gate, up, down)):
+
+
+def pieces_kernel(gate, up, down, out, held, sem):
+    copies = [pltpu.make_async_copy(ref, held.at[m], sem.at[m]) for m, ref in enumerate((gate, up, down))]
+    for copy in copies:
+        copy.start()
+    for m in range(3):
+        copies[m].wait()
         for k in range(8):
-            size = min(UNITS, ref.shape[0] - k * UNITS)
-            source = ref.at[pl.ds(k * UNITS, size), :]
-            target = out.at[k, pl.ds(m * UNITS, size), :]
-            copies.append(pltpu.make_async_copy(source, target, sem.at[m * 8 + k]))
-            copies[-1].start()
+            size = min(UNITS, held.shape[1] - k * UNITS)
+            out[k, m * UNITS : m * UNITS + size, :] = held[m, k * UNITS : k * UNITS + size, :]
             if size < UNITS:
                 out[k, m * UNITS + size : (m + 1) * UNITS, :] = jnp.zeros((UNITS - size, 256), bf16)
-    for copy in copies:
-        copy.wait()
 
 
 def dot(a, b):
     return jnp.dot(a, b, preferred_element_type=f32)
 
 
-def ffn_kernel(ids, own, theirs, pieces, branch, w_gate, w_up, w_down, y_other, y_own, rows, near, far):
-    core, expert = ids[0], ids[1]
-    for side, ref in enumerate((own, theirs)):
-        rows[side] = ref[...].reshape(512, HALF + TAIL)
+def half_sums(x, w_gate, w_up, near, first):
+    both = None
+    for j in range(4):
+        term = dot_last(x[:, j * 256 : (j + 1) * 256], near[first + j])
+        both = term if both is None else both + term
+    return dot(x, w_gate), dot(x, w_up), both
+
+
+def near_kernel(
+    ids, own, pieces, branch, gate_hbm, up_hbm, down_hbm,
+    gate_sum, up_sum, both, near, far, gate_rest, up_rest, w_down,
+    w_gate, w_up, sem,
+):
+    core = ids[0]
+    mine = pl.ds(pl.multiple_of(core * HALF, HALF), HALF)
+    rest = pl.ds(pl.multiple_of((1 - core) * HALF, HALF), HALF)
+    copies = [
+        pltpu.make_async_copy(source, target, sem.at[k])
+        for k, (source, target) in enumerate(
+            (
+                (gate_hbm.at[mine, :], w_gate), (up_hbm.at[mine, :], w_up),
+                (gate_hbm.at[rest, :], gate_rest), (up_hbm.at[rest, :], up_rest), (down_hbm, w_down),
+            )
+        )
+    ]
+    for copy in copies:
+        copy.start()
     near[...] = jnp.zeros_like(near)
     far[...] = jnp.zeros_like(far)
     for b in range(8):
@@ -162,31 +180,45 @@
         near[b, 128 : 128 + UNITS, :] = pieces[b, UNITS : 2 * UNITS, :]
         near[b, 64:72, :] = jnp.broadcast_to(branch[:, b * 256 : (b + 1) * 256], (8, 256))
         far[0:UNITS, b * 256 : (b + 1) * 256] = pieces[b, 2 * UNITS :, :]
-    halves = (core, 1 - core)
-    gate_sum = up_sum = both = None
-    for side in range(2):
-        base = pl.multiple_of(halves[side] * HALF, HALF)
-        x = rows[side, :, 0:HALF]
-        gate_part = dot(x, w_gate[pl.ds(base, HALF), :])
-        up_part = dot(x, w_up[pl.ds(base, HALF), :])
-        gate_sum = gate_part if side == 0 else gate_sum + gate_part
-        up_sum = up_part if side == 0 else up_sum + up_part
-        for j in range(4):
-            xj = rows[side, :, j * 256 : (j + 1) * 256]
-            term = lax.dot_general(xj, near[halves[side] * 4 + j], (((1,), (1,)), ((), ())), preferred_element_type=f32)
-            both = term if both is None else both + term
+    x = own[:, :, 0:HALF].reshape(512, HALF)
+    copies[0].wait()
+    copies[1].wait()
+    gate_sum[...], up_sum[...], both[...] = half_sums(x, w_gate[...], w_up[...], near, core * 4)
+    for copy in copies[2:]:
+        copy.wait()
+
+
+def out_half(act, dense_act, weight, gate, w_down, far, half):
+    columns = pl.ds(pl.multiple_of(half * HALF, HALF), HALF)
+    return weight * dot(act, w_down[:, columns]) + gate * dot(dense_act, far[:, columns])
+
+
+def rest_kernel(
+    ids, theirs, gate_near, up_near, both_near, near, far, gate_rest, up_rest, w_down, y_other, act_out, dense_out, scales
+):
+    core, expert = ids[0], ids[1]
+    x = theirs[:, :, 0:HALF].reshape(512, HALF)
+    gate_sum, up_sum, both = half_sums(x, gate_rest[...], up_rest[...], near, (1 - core) * 4)
+    gate_sum = gate_sum + gate_near[...]
+    up_sum = up_sum + up_near[...]
+    both = both + both_near[...]
     act = (gate_sum * jax.nn.sigmoid(gate_sum) * up_sum).astype(bf16)
     dense_gate = both[:, 0:128]
     dense_act = dense_gate * jax.nn.sigmoid(dense_gate) * both[:, 128:256]
     lane = lax.broadcasted_iota(jnp.int32, (512, 128), 1)
     gate = jax.nn.sigmoid(jnp.sum(jnp.where(lane == 64, dense_gate, 0.0), axis=1, keepdims=True))
-    tail = rows[0, :, HALF : HALF + TAIL].astype(f32)
+    tail = theirs[:, :, HALF : HALF + TAIL].reshape(512, TAIL).astype(f32)
     weight = jnp.sum(jnp.where((lane == expert) | (lane == expert + 8), tail, 0.0), axis=1, keepdims=True)
     dense_act = jnp.where(lane < UNITS, dense_act, 0.0).astype(bf16)
-    for side, ref in ((1, y_other), (0, y_own)):
-        base = pl.multiple_of(halves[side] * HALF, HALF)
-        total = weight * dot(act, w_down[:, pl.ds(base, HALF)]) + gate * dot(dense_act, far[:, pl.ds(base, HALF)])
-        ref[...] = total.astype(ref.dtype)
+    act_out[...] = act
+    dense_out[...] = dense_act
+    scales[0] = jnp.broadcast_to(weight, (512, 128))
+    scales[1] = jnp.broadcast_to(gate, (512, 128))
+    y_other[...] = out_half(act, dense_act, weight, gate, w_down, far, 1 - core).astype(bf16)
+
+
+def own_kernel(ids, act, dense_act, scales, far, w_down, y_own):
+    y_own[...] = out_half(act[...], dense_act[...], scales[0, :, 0:1], scales[1, :, 0:1], w_down, far, ids[0])
 
 
 def join_kernel(y_own, y_recv, out):
@@ -229,44 +261,56 @@
         pieces_kernel,
         [((8, PIECE, 256), bf16, True)],
         [jnp.swapaxes(dense_gate[0], 0, 1), jnp.swapaxes(dense_up[0], 0, 1), dense_down[0]],
-        [pltpu.SemaphoreType.DMA((24,))],
+        [pltpu.VMEM((3, 352, 256), bf16), pltpu.SemaphoreType.DMA((3,))],
         {0: hbm, 1: hbm, 2: hbm},
     )
     columns = [[16 * b + j for b in range(8)] for j in range(16)]
     pieces = lax.all_to_all(pieces, "ep", 0, 0, axis_index_groups=columns, tiled=True)
 
     positions = cache_keys.shape[0] * cache_keys.shape[1] * KV_HEADS
-    pair, hidden_state, key_new, value_new, w_gate, w_up, w_down = call(
+    pair, hidden_state, key_new, value_new = call(
         attend_kernel,
         [
             ((2, rows, HALF + TAIL), bf16, True), ((rows, D), f32, True),
             ((rows, KV_HEADS * HEAD_DIM), bf16, False), ((rows, KV_HEADS * HEAD_DIM), bf16, False),
-            (exp_gate.shape, bf16, True), (exp_up.shape, bf16, True), (exp_down.shape, bf16, True),
         ],
         [
             lengths, routes, route_weights, tokens, mix_lambda.reshape(HEADS, 1), head_gain.reshape(1, HEAD_DIM),
             attn_gain.reshape(1, D), ffn_gain.reshape(1, D), query_w, key_w, value_w,
-            cache_keys.reshape(positions, HEAD_DIM), cache_values.reshape(positions, HEAD_DIM), out_w, exp_gate, exp_up, exp_down,
+            cache_keys.reshape(positions, HEAD_DIM), cache_values.reshape(positions, HEAD_DIM), out_w,
         ],
         [
             pltpu.VMEM(query_w.shape, bf16), pltpu.VMEM(key_w.shape, bf16), pltpu.VMEM(value_w.shape, bf16),
             pltpu.VMEM((positions, HEAD_DIM), bf16), pltpu.VMEM((positions, HEAD_DIM), bf16), pltpu.VMEM(out_w.shape, bf16),
-            pltpu.SemaphoreType.DMA((21,)), pltpu.VMEM((32, HEAD_DIM), f32), pltpu.VMEM((rows, HEADS * HEAD_DIM), f32),
+            pltpu.SemaphoreType.DMA((18,)), pltpu.VMEM((32, HEAD_DIM), f32), pltpu.VMEM((rows, HEADS * HEAD_DIM), f32),
         ],
-        {0: smem, 1: smem, 2: smem, **{k: hbm for k in range(8, 17)}},
+        {0: smem, 1: smem, 2: smem, **{k: hbm for k in range(8, 14)}},
     )
     outgoing = jnp.broadcast_to(pair[None], (64, 2, rows, HALF + TAIL)).reshape(DEVICES, rows, HALF + TAIL)
     outgoing, pieces = lax.optimization_barrier((outgoing, pieces))
     own = lax.all_to_all(outgoing, "ep", 0, 0, tiled=True)
     theirs = to_partner(own)
-    y_other, y_own = call(
-        ffn_kernel,
-        [((512, HALF), bf16, True), ((512, HALF), f32, True)],
-        [ids, own, theirs, pieces, branch_gate.reshape(1, D), w_gate, w_up, w_down],
-        [pltpu.VMEM((2, 512, HALF + TAIL), bf16), pltpu.VMEM((8, 256, 256), bf16), pltpu.VMEM((128, D), bf16)],
+    hidden_units = exp_gate.shape[1]
+    gate_near, up_near, both_near, near, far, gate_rest, up_rest, w_down = call(
+        near_kernel,
+        [
+            ((512, hidden_units), f32, True), ((512, hidden_units), f32, True), ((512, 256), f32, True),
+            ((8, 256, 256), bf16, True), ((128, D), bf16, True),
+            ((HALF, hidden_units), bf16, True), ((HALF, hidden_units), bf16, True), (exp_down.shape, bf16, True),
+        ],
+        [ids, own, pieces, branch_gate.reshape(1, D), exp_gate, exp_up, exp_down],
+        [pltpu.VMEM((HALF, hidden_units), bf16), pltpu.VMEM((HALF, hidden_units), bf16), pltpu.SemaphoreType.DMA((5,))],
+        {0: smem, 4: hbm, 5: hbm, 6: hbm},
+    )
+    y_other, act, dense_act, scales = call(
+        rest_kernel,
+        [((512, HALF), bf16, True), ((512, hidden_units), bf16, True), ((512, 128), bf16, True), ((2, 512, 128), f32, True)],
+        [ids, theirs, gate_near, up_near, both_near, near, far, gate_rest, up_rest, w_down],
+        [],
         {0: smem},
     )
     y_recv = to_partner(y_other)
+    (y_own,) = call(own_kernel, [((512, HALF), f32, True)], [ids, act, dense_act, scales, far, w_down], [], {0: smem})
     (joined,) = call(join_kernel, [((DEVICES, rows, HALF), bf16, True)], [y_own, y_recv])
     parts = lax.all_to_all(joined, "ep", 0, 0, tiled=True)
     (output,) = call(last_kernel, [((rows, D), bf16, False)], [hidden_state, parts])

time: 93.8 us -> 85.7 us (0.914)
  local copies, waits for them, and re-layouts: 5.73 us -> 0.62 us
  blocking collectives: 53.4 us -> 50.8 us
  Pallas kernels: 18.7 us -> 20 us
  waiting for transfers between devices: 4.85 us -> 3.61 us
    unnamed x28 -> x20, local copies, waits for them, and re-layouts: 5.34 us -> 0.22 us
    ppermute x2, waiting for transfers between devices: 4.78 us -> 1.11 us  [to_partner(): return lax.ppermute(x, 'ep', [(i, i ^ 1) for i in range(DEVICES)])]
    all_to_all x1, waiting for transfers between devices: 0.06 us -> 2.5 us  [per_device(): lax.all_to_all(pieces, 'ep', 0, 0, axis_index_groups=columns, tiled=True)]
    all_to_all x1, blocking collectives: 30.6 us -> 28.2 us  [per_device(): own = lax.all_to_all(outgoing, 'ep', 0, 0, tiled=True)]
    pallas_call x5 -> x7, Pallas kernels: 18.7 us -> 20 us  [call(): pl.pallas_call(kernel, in_specs=[pl.BlockSpec(memory_space=spaces.get(k,...]
  transfers between devices with their start and end apart: 3 -> 3, of which waited for: 3 -> 2; matrix products, arithmetic and copies ran while one was open for 0% -> 0% of each run, Pallas kernels for 9% -> 16%
where the time goes in v2:
time: 85.7 us; the launch traced here: 85.4 us
  blocking collectives  50.8 us (59%)
  Pallas kernels  20 us (23%)
  starting transfers between devices  9.54 us (11%)
  waiting for transfers between devices  3.61 us (4%)
    all_to_all x1, blocking collectives, per_device(): own = lax.all_to_all(outgoing, 'ep', 0, 0, tiled=True)  28.2 us
    all_to_all x1, blocking collectives, per_device(): parts = lax.all_to_all(joined, 'ep', 0, 0, tiled=True)  22.6 us
    pallas_call x7, Pallas kernels, call(): pl.pallas_call(kernel, in_specs=[pl.BlockSpec(memory_space=spaces.get(k,...  20 us
    all_to_all x1, starting transfers between devices, per_device(): lax.all_to_all(pieces, 'ep', 0, 0, axis_index_groups=columns, tiled=True)  8.49 us
    all_to_all x1, waiting for transfers between devices, per_device(): lax.all_to_all(pieces, 'ep', 0, 0, axis_index_groups=columns, tiled=True)  2.5 us
  transfers between devices with their start and end apart: 3, of which 2 were waited for; matrix products, arithmetic and copies ran while one was open for 0% of the time, Pallas kernels for 16%

profile of v2, /device:TPU:1, one launch (start us, length us, event | category | flops | bytes accessed | tf_op | source)
XLA Modules:
  0.0 85.4 jit_solution(7112234372020397742)
XLA Ops:
  0.6 0.0 copy-start.6
  0.6 0.0 copy-start.7
  0.7 0.0 copy-start.8
  0.7 0.0 copy-start.2
  0.7 0.0 copy-start.1
  0.7 0.0 copy-start.4
  0.7 0.0 copy-start.3
  0.7 0.0 copy-start
  0.7 2.0 %shard_map.221 = bf16[8,144,256]{2,1,0:T(8,128)(2,1)} custom-call(bf16[352,256]{1,0:T(8,128)(2,1)} %bitcast.22, bf16[352,256]{1,0:T(8,128)(2,1)} %bitcast.23, bf16[352,256]{1,0:T(8,128)(2,1)} %bitcast.24), custom_call_target="tpu_custom_call" | custom-call | tf_op jit(solution)/shard_map/pallas_call | solution.py:240
  2.7 8.5 %all-to-all-start = ((bf16[8,144,256]{2,1,0:T(8,128)(2,1)}), bf16[8,144,256]{2,1,0:T(8,128)(2,1)S(1)}, u32[]{:S(2)}, u32[]{:S(2)}) async-start(bf16[8,144,256]{2,1,0:T(8,128)(2,1)} %shard_map.221), calls=%async_computation | async-start | bytes 1179648 | tf_op jit(solution)/shard_map/all_to_all | solution.py:268
  11.2 0.0 copy-done.6
  11.2 0.1 copy.24.routes
  11.3 0.0 copy-done.7
  11.3 0.1 copy.25.route_weights
  11.4 0.0 copy-done.8
  11.4 0.1 copy.26.mix_lambda
  11.5 0.0 copy-done.2
  11.5 0.0 copy-done.1
  11.5 0.0 copy-done.4
  11.5 0.0 copy-done.3
  11.5 0.0 copy-done
  11.5 8.6 %shard_map.220 = (bf16[2,4,1152]{2,1,0:T(4,128)(2,1)S(1)}, f32[4,2048]{1,0:T(4,128)S(1)}, bf16[4,256]{1,0:T(4,128)(2,1)}, bf16[4,256]{1,0:T(4,128)(2,1)}) custom-call(s32[4]{0:T(128)S(1)} %copy-done.3, s32[4,2]{1,0:T(4,128)S(1)} %copy.24.routes, f32[4,2]{1,0:T(4,128)S(1)} %copy.25.route_weights, bf16[4,2048]{1,0:T(4,128)(2,1)S(1)} %copy-done, ...), custom_call_target="tpu_custom_call" | custom-call | tf_op jit(solution)/shard_map/pallas_call | solution.py:240
  20.1 2.5 %all-to-all-done.pieces = bf16[8,144,256]{2,1,0:T(8,128)(2,1)S(1)} async-done(((bf16[8,144,256]{2,1,0:T(8,128)(2,1)}), bf16[8,144,256]{2,1,0:T(8,128)(2,1)S(1)}, u32[]{:S(2)}, u32[]{:S(2)}) %all-to-all-start) | async-done | bytes 589856 | tf_op jit(solution)/shard_map/all_to_all | solution.py:268
  22.6 0.0 copy-start.5
  22.6 0.3 broadcast_in_dim.2
  22.9 28.2 %all_to_all.15.own = bf16[128,4,1152]{2,1,0:T(4,128)(2,1)S(1)} all-to-all(bf16[128,4,1152]{2,1,0:T(4,128)(2,1)S(1)} %bitcast.19), channel_id=1, replica_groups=mesh['ep'=128] {'ep'}, dimensions={0} | all-to-all | bytes 2359296 | tf_op jit(solution)/shard_map/all_to_all | solution.py:291
  51.1 1.0 %collective-permute-start = (bf16[128,4,1152]{2,1,0:T(4,128)(2,1)S(1)}, bf16[128,4,1152]{2,1,0:T(4,128)(2,1)S(1)}, u32[]{:S(2)}, u32[]{:S(2)}) collective-permute-start(bf16[128,4,1152]{2,1,0:T(4,128)(2,1)S(1)} %all_to_all.15.own), channel_id=1, source_target_pairs={{0,1},{1,0},{2,3},{3,2},{4,5},{5,4},{6,7},{7,6},{8,9},{9,8},{10,11... | collective-permute-start | bytes 3538952 | tf_op jit(solution)/shard_map/ppermute | solution.py:23
  52.0 0.0 copy-done.5
  52.1 0.1 pad_add_fusion.ids
  52.2 3.5 %shard_map.222 = (f32[512,384]{1,0:T(8,128)S(1)}, f32[512,384]{1,0:T(8,128)S(1)}, f32[512,256]{1,0:T(8,128)S(1)}, bf16[8,256,256]{2,1,0:T(8,128)(2,1)S(1)}, bf16...) custom-call(s32[2]{0:T(128)S(1)} %pad_add_fusion.ids, ...), custom_call_target="tpu_custom_call" | custom-call | tf_op jit(solution)/shard_map/pallas_call | solution.py:240
  55.7 0.0 collective-permute-done.theirs
  55.7 3.3 %shard_map.223 = (bf16[512,1024]{1,0:T(8,128)(2,1)S(1)}, bf16[512,384]{1,0:T(8,128)(2,1)S(1)}, bf16[512,128]{1,0:T(8,128)(2,1)S(1)}, f32[2,512,128]{2,1,0:T(8,128)S(1)}) custom-call(s32[2]{0:T(128)S(1)} %pad_add_fusion.ids, bf16[128,4,1152]{2,1,0:T(4,128)(2,1)S(1)} %collective-permute-done.theirs, f32[512,384]{1,0:T(8,128)S(1)} %get-tuple-element.25.gate_near, ...), custom_call_target="tpu_custom_call" | custom-call | tf_op jit(solution)/shard_map/pallas_call | solution.py:240
  59.0 0.1 collective-permute-start.1
  59.1 1.5 %shard_map.224.y_own = f32[512,1024]{1,0:T(8,128)S(1)} custom-call(s32[2]{0:T(128)S(1)} %pad_add_fusion.ids, bf16[512,384]{1,0:T(8,128)(2,1)S(1)} %get-tuple-element.33.act, bf16[512,128]{1,0:T(8,128)(2,1)S(1)} %get-tuple-element.34.dense_act, f32[2,512,128]{2,1,0:T(8,128)S(1)} %get-tuple-element.35.scales, bf16[128,2048]{1,0:T(8,128)(2,1)S(1)} %get-tuple-element.29.far, ...), custom_call_target="tpu_custom_call" | custom-call | tf_op jit(solution)/shard_map/pallas_call | solution.py:240
  60.7 1.1 %collective-permute-done.1.y_recv = bf16[512,1024]{1,0:T(8,128)(2,1)S(1)} collective-permute-done((bf16[512,1024]{1,0:T(8,128)(2,1)S(1)}, bf16[512,1024]{1,0:T(8,128)(2,1)S(1)}, u32[]{:S(2)}, u32[]{:S(2)}) %collective-permute-start.1) | collective-permute-done | bytes 1048608 | tf_op jit(solution)/shard_map/ppermute | solution.py:23
  61.8 0.3 shard_map.225
  62.0 22.6 %all_to_all.16.parts = bf16[128,4,1024]{2,1,0:T(4,128)(2,1)S(1)} all-to-all(bf16[128,4,1024]{2,1,0:T(4,128)(2,1)S(1)} %shard_map.225), channel_id=1, replica_groups=mesh['ep'=128] {'ep'}, dimensions={0} | all-to-all | bytes 2097152 | tf_op jit(solution)/shard_map/all_to_all | solution.py:315
  84.6 0.8 shard_map.226
  (1 shorter events, 0.0 us)
Async XLA Ops:
  0.6 10.6 %copy-start.6 = (s32[4,2]{0,1:T(2,128)S(1)}, s32[4,2]{0,1:T(2,128)}, u32[]{:S(2)}) copy-start(s32[4,2]{0,1:T(2,128)} %param.33) | copy-start | bytes 100
  0.6 10.7 %copy-start.7 = (f32[4,2]{0,1:T(2,128)S(1)}, f32[4,2]{0,1:T(2,128)}, u32[]{:S(2)}) copy-start(f32[4,2]{0,1:T(2,128)} %param.34) | copy-start | bytes 100
  0.7 10.8 %copy-start.8 = (f32[8]{0:T(128)S(1)}, f32[8]{0:T(128)}, u32[]{:S(2)}) copy-start(f32[8]{0:T(128)} %param.29) | copy-start | bytes 100
  0.7 10.8 %copy-start.2 = (f32[2048]{0:T(1024)S(1)}, f32[2048]{0:T(1024)}, u32[]{:S(2)}) copy-start(f32[2048]{0:T(1024)} %param.32) | copy-start | bytes 24580
  0.7 10.8 %copy-start.1 = (f32[2048]{0:T(1024)S(1)}, f32[2048]{0:T(1024)}, u32[]{:S(2)}) copy-start(f32[2048]{0:T(1024)} %param.31) | copy-start | bytes 24580
  0.7 10.8 %copy-start.4 = (f32[128]{0:T(128)S(1)}, f32[128]{0:T(128)}, u32[]{:S(2)}) copy-start(f32[128]{0:T(128)} %param.30) | copy-start | bytes 1540
  0.7 10.8 %copy-start.3 = (s32[4]{0:T(128)S(1)}, s32[4]{0:T(128)}, u32[]{:S(2)}) copy-start(s32[4]{0:T(128)} %lengths.1) | copy-start | bytes 52
  0.7 10.8 %copy-start = (bf16[4,2048]{1,0:T(4,128)(2,1)S(1)}, bf16[4,2048]{1,0:T(4,128)(2,1)}, u32[]{:S(2)}) copy-start(bf16[4,2048]{1,0:T(4,128)(2,1)} %tokens.1) | copy-start | bytes 49156
  2.7 19.9 %all-to-all-start = ((bf16[8,144,256]{2,1,0:T(8,128)(2,1)}), bf16[8,144,256]{2,1,0:T(8,128)(2,1)S(1)}, u32[]{:S(2)}, u32[]{:S(2)}) async-start(bf16[8,144,256]{2,1,0:T(8,128)(2,1)} %shard_map.221), calls=%async_computation | async-start | bytes 1179648 | tf_op jit(solution)/shard_map/all_to_all | solution.py:268
  22.6 29.4 %copy-start.5 = (bf16[2048]{0:T(1024)(128)(2,1)S(1)}, bf16[2048]{0:T(1024)(128)(2,1)}, u32[]{:S(2)}) copy-start(bf16[2048]{0:T(1024)(128)(2,1)} %param.41) | copy-start | bytes 12292
  51.1 4.6 %collective-permute-start = (bf16[128,4,1152]{2,1,0:T(4,128)(2,1)S(1)}, bf16[128,4,1152]{2,1,0:T(4,128)(2,1)S(1)}, u32[]{:S(2)}, u32[]{:S(2)}) collective-permute-start(bf16[128,4,1152]{2,1,0:T(4,128)(2,1)S(1)} %all_to_all.15.own), channel_id=1, source_target_pairs={{0,1},{1,0},{2,3},{3,2},{4,5},{5,4},{6,7},{7,6},{8,9},{9,8},{10,11... | collective-permute-start | bytes 3538952 | tf_op jit(solution)/shard_map/ppermute | solution.py:23
  59.0 2.7 %collective-permute-start.1 = (bf16[512,1024]{1,0:T(8,128)(2,1)S(1)}, bf16[512,1024]{1,0:T(8,128)(2,1)S(1)}, u32[]{:S(2)}, u32[]{:S(2)}) collective-permute-start(bf16[512,1024]{1,0:T(8,128)(2,1)S(1)} %get-tuple-element.36), channel_id=1, source_target_pairs={{0,1},{1,0},{2,3},{3,2},{4,5},{5,4},{6,7},{7,6},{8,9},{9,8},{10,11... | collective-permute-start | bytes 3145736 | tf_op jit(solution)/shard_map/ppermute | solution.py:23

commit v3 on v2

v3 whole, which is shorter than its diff:
```python
import jax
import jax.numpy as jnp
from jax import lax
from jax.experimental import pallas as pl
from jax.experimental.pallas import tpu as pltpu
from jax.sharding import PartitionSpec as P


HEADS = 8
KV_HEADS = 2
HEAD_DIM = 128
DEVICES = 128
D = 2048
HALF = D // 2
UNITS = 48
PIECE = 3 * UNITS
TAIL = 128
f32 = jnp.float32
bf16 = jnp.bfloat16


def to_partner(x):
    return lax.ppermute(x, "ep", [(i, i ^ 1) for i in range(DEVICES)])


def rms_norm(values, gain, epsilon):
    scale = lax.rsqrt(jnp.mean(values * values, axis=-1, keepdims=True) + epsilon)
    return values * scale * gain


def dot_last(a, b):
    return lax.dot_general(a, b, (((1,), (1,)), ((), ())), preferred_element_type=f32)


def attend_kernel(
    lengths_hbm, routes_hbm, route_weights_hbm, tokens_hbm, mix_hbm, head_gain_hbm, attn_gain_hbm, ffn_gain_hbm,
    query_hbm, key_hbm, value_hbm, cache_keys, cache_values, out_hbm,
    pair, hidden, key_out, value_out,
    query_w, key_w, value_w, keys, values, out_w, sem, query_rows, head_rows,
    lengths, routes, route_weights, tokens, mix_lambda, head_gain, attn_gain, ffn_gain, key_new, value_new,
):
    span = keys.shape[0] // 4
    copies = []

    def fetch(source, target):
        copies.append(pltpu.make_async_copy(source, target, sem.at[len(copies)]))
        copies[-1].start()
        return copies[-1]

    on_tokens = [fetch(tokens_hbm, tokens), fetch(attn_gain_hbm, attn_gain)]
    on_query = [fetch(query_hbm.at[pl.ds(k * 512, 512), :], query_w.at[pl.ds(k * 512, 512), :]) for k in range(4)]
    on_key = fetch(key_hbm, key_w)
    on_value = fetch(value_hbm, value_w)
    on_small = [
        fetch(lengths_hbm, lengths), fetch(mix_hbm, mix_lambda), fetch(head_gain_hbm, head_gain), fetch(ffn_gain_hbm, ffn_gain),
        fetch(routes_hbm, routes), fetch(route_weights_hbm, route_weights),
    ]
    on_keys, on_values = [], []
    for s in range(4):
        on_keys.append(fetch(cache_keys.at[pl.ds(s * span, span), :], keys.at[pl.ds(s * span, span), :]))
    for s in range(4):
        on_values.append(fetch(cache_values.at[pl.ds(s * span, span), :], values.at[pl.ds(s * span, span), :]))
    on_out = [fetch(out_hbm.at[pl.ds(k * 256, 256), :], out_w.at[pl.ds(k * 256, 256), :]) for k in range(4)]

    for copy in on_tokens:
        copy.wait()
    x = tokens[...].astype(f32)
    normed = rms_norm(x, attn_gain[...], 1e-06).astype(bf16)
    query = None
    for k in range(4):
        on_query[k].wait()
        term = dot(normed[:, k * 512 : (k + 1) * 512], query_w[k * 512 : (k + 1) * 512, :])
        query = term if query is None else query + term
    query = query.astype(bf16).astype(f32)
    for s in range(4):
        for h in range(HEADS):
            query_rows[s * 8 + h : s * 8 + h + 1, :] = query[s : s + 1, h * HEAD_DIM : (h + 1) * HEAD_DIM]
    for copy in on_small:
        copy.wait()
    lane = lax.broadcasted_iota(jnp.int32, (4, TAIL), 1)
    row = lax.broadcasted_iota(jnp.int32, (4, TAIL), 0)
    tail = jnp.zeros((4, TAIL), f32)
    for t in range(4):
        for k in range(2):
            weight = jnp.full((4, TAIL), route_weights[k, t], f32)
            upper = weight.astype(bf16).astype(f32)
            there = row == t
            tail = jnp.where(there & (lane == routes[k, t]), upper, tail)
            tail = jnp.where(there & (lane == routes[k, t] + 8), weight - upper, tail)
    for half in range(2):
        pair[half, :, HALF:] = tail.astype(bf16)
    on_key.wait()
    knew = dot(normed, key_w[...]).astype(bf16)
    key_new[...] = knew
    written = [fetch(key_new, key_out)]
    on_value.wait()
    vnew = dot(normed, value_w[...]).astype(bf16)
    value_new[...] = vnew
    written.append(fetch(value_new, value_out))
    knew = knew.astype(f32)
    vnew = vnew.astype(f32)
    first = lax.broadcasted_iota(jnp.int32, (8, HEAD_DIM), 1) < HEAD_DIM // 2
    low_head = lax.broadcasted_iota(jnp.int32, (8, HEAD_DIM), 0) < 4
    lane = lax.broadcasted_iota(jnp.int32, (16, span), 1)
    row = lax.broadcasted_iota(jnp.int32, (16, span), 0)
    own_head = (lane & 1) == ((row >> 2) & 1)
    place = lane >> 1
    scale = (HEAD_DIM // 2) ** (-0.5)
    weights, own_weights = [], []
    lam = jnp.zeros((8, 1), f32)
    head = lax.broadcasted_iota(jnp.int32, (8, 1), 0)
    for h in range(HEADS):
        lam = jnp.where(head == h, mix_lambda[h], lam)
    for s in range(4):
        q = query_rows[s * 8 : s * 8 + 8, :]
        q = jnp.concatenate([jnp.where(first, q, 0.0), jnp.where(first, 0.0, q)])
        k_own = jnp.where(low_head, knew[s : s + 1, 0:HEAD_DIM], knew[s : s + 1, HEAD_DIM:])
        own = jnp.sum(q * jnp.concatenate([k_own, k_own]), axis=1, keepdims=True) * scale
        on_keys[s].wait()
        scores = dot_last(q.astype(bf16), keys[s * span : (s + 1) * span, :]) * scale
        scores = jnp.where(own_head & (place < lengths[s]), scores, -jnp.inf)
        largest = jnp.maximum(jnp.max(scores, axis=1, keepdims=True), own)
        raised = jnp.exp(scores - largest)
        own_raised = jnp.exp(own - largest)
        total = jnp.sum(raised, axis=1, keepdims=True) + own_raised
        prob = raised / total
        own_prob = own_raised / total
        weights.append((prob[0:8] - lam * prob[8:16]).astype(bf16))
        own_weights.append((own_prob[0:8] - lam * own_prob[8:16]).astype(bf16).astype(f32))
    for s in range(4):
        v_own = jnp.where(low_head, vnew[s : s + 1, 0:HEAD_DIM], vnew[s : s + 1, HEAD_DIM:])
        on_values[s].wait()
        mixed = dot(weights[s], values[s * span : (s + 1) * span, :]) + own_weights[s] * v_own
        heads = rms_norm(mixed, head_gain[...], 1e-05)
        for h in range(HEADS):
            head_rows[s : s + 1, h * HEAD_DIM : (h + 1) * HEAD_DIM] = heads[h : h + 1, :]
    heads = head_rows[...].astype(bf16)
    state = x
    for k in range(4):
        on_out[k].wait()
        state = state + dot(heads[:, k * 256 : (k + 1) * 256], out_w[k * 256 : (k + 1) * 256, :])
    hidden[...] = state
    ffn_in = rms_norm(state, ffn_gain[...], 1e-06).astype(bf16)
    for half in range(2):
        pair[half, :, 0:HALF] = ffn_in[:, half * HALF : (half + 1) * HALF]
    for copy in written:
        copy.wait()


def pieces_kernel(gate, up, down, out, held, sem):
    copies = [pltpu.make_async_copy(ref, held.at[m], sem.at[m]) for m, ref in enumerate((gate, up, down))]
    for copy in copies:
        copy.start()
    for m in range(3):
        copies[m].wait()
        for k in range(8):
            size = min(UNITS, held.shape[1] - k * UNITS)
            out[k, m * UNITS : m * UNITS + size, :] = held[m, k * UNITS : k * UNITS + size, :]
            if size < UNITS:
                out[k, m * UNITS + size : (m + 1) * UNITS, :] = jnp.zeros((UNITS - size, 256), bf16)


def dot(a, b):
    return jnp.dot(a, b, preferred_element_type=f32)


def dense_sums(x, near, first):
    both = None
    for j in range(4):
        term = dot_last(x[:, j * 256 : (j + 1) * 256], near[first + j])
        both = term if both is None else both + term
    return both


def near_kernel(ids, own, pieces, branch, gate_hbm, up_hbm, down_hbm, sums, both, near, w_rest, w_out, w_own, sem):
    core = ids[0]
    mine = pl.ds(pl.multiple_of(core * HALF, HALF), HALF)
    rest = pl.ds(pl.multiple_of((1 - core) * HALF, HALF), HALF)
    wide = gate_hbm.shape[1]
    left, right = pl.ds(0, wide), pl.ds(wide, wide)
    copies = [
        pltpu.make_async_copy(source, target, sem.at[k])
        for k, (source, target) in enumerate(
            (
                (gate_hbm.at[mine, :], w_own.at[:, left]), (up_hbm.at[mine, :], w_own.at[:, right]),
                (gate_hbm.at[rest, :], w_rest.at[:, left]), (up_hbm.at[rest, :], w_rest.at[:, right]),
                (down_hbm, w_out.at[pl.ds(0, wide), :]),
            )
        )
    ]
    for copy in copies:
        copy.start()
    near[...] = jnp.zeros_like(near)
    w_out[wide + UNITS :, :] = jnp.zeros((128 - UNITS, D), bf16)
    for b in range(8):
        near[b, 0:UNITS, :] = pieces[b, 0:UNITS, :]
        near[b, 128 : 128 + UNITS, :] = pieces[b, UNITS : 2 * UNITS, :]
        near[b, 64:72, :] = jnp.broadcast_to(branch[:, b * 256 : (b + 1) * 256], (8, 256))
        w_out[wide : wide + UNITS, b * 256 : (b + 1) * 256] = pieces[b, 2 * UNITS :, :]
    x = own[:, :, 0:HALF].reshape(512, HALF)
    both[...] = dense_sums(x, near, core * 4)
    copies[0].wait()
    copies[1].wait()
    sums[...] = dot(x, w_own[...])
    for copy in copies[2:]:
        copy.wait()


def rest_kernel(ids, theirs, sums_near, both_near, near, w_rest, w_out, y_other, acts):
    core, expert = ids[0], ids[1]
    x = theirs[:, :, 0:HALF].reshape(512, HALF)
    both = dense_sums(x, near, (1 - core) * 4) + both_near[...]
    sums = dot(x, w_rest[...]) + sums_near[...]
    wide = sums.shape[1] // 2
    gate_sum, up_sum = sums[:, 0:wide], sums[:, wide:]
    dense_gate = both[:, 0:128]
    lane = lax.broadcasted_iota(jnp.int32, (512, 128), 1)
    gate = jax.nn.sigmoid(jnp.sum(jnp.where(lane == 64, dense_gate, 0.0), axis=1, keepdims=True))
    tail = theirs[:, :, HALF : HALF + TAIL].reshape(512, TAIL).astype(f32)
    weight = jnp.sum(jnp.where((lane == expert) | (lane == expert + 8), tail, 0.0), axis=1, keepdims=True)
    dense_act = gate * (dense_gate * jax.nn.sigmoid(dense_gate) * both[:, 128:256])
    acts[:, 0:wide] = (weight * (gate_sum * jax.nn.sigmoid(gate_sum) * up_sum)).astype(bf16)
    acts[:, wide:] = jnp.where(lane < UNITS, dense_act, 0.0).astype(bf16)
    columns = pl.ds(pl.multiple_of((1 - core) * HALF, HALF), HALF)
    y_other[...] = dot(acts[...], w_out[:, columns]).astype(bf16)


def own_kernel(ids, acts, w_out, y_own):
    y_own[...] = dot(acts[...], w_out[:, pl.ds(pl.multiple_of(ids[0] * HALF, HALF), HALF)])


def join_kernel(y_own, y_recv, out):
    out[...] = (y_own[...] + y_recv[...].astype(f32)).astype(bf16).reshape(128, 4, HALF)


def last_kernel(hidden, parts, out):
    for half in range(2):
        total = jnp.zeros((4, HALF), f32)
        for chip in range(64):
            total = total + parts[2 * chip + half].astype(f32)
        cols = slice(half * HALF, (half + 1) * HALF)
        out[:, cols] = (hidden[:, cols] + total).astype(bf16)


def call(kernel, outs, operands, scratch=(), spaces=None):
    spaces = spaces or {}
    operands = [pltpu.with_memory_space_constraint(x, pltpu.HBM) if spaces.get(k) is pltpu.HBM else x for k, x in enumerate(operands)]
    return pl.pallas_call(
        kernel,
        in_specs=[pl.BlockSpec(memory_space=spaces.get(k, pltpu.VMEM)) for k in range(len(operands))],
        out_specs=[pl.BlockSpec(memory_space=space or pltpu.VMEM) for _, _, space in outs],
        out_shape=[space(shape, kind) if space else jax.ShapeDtypeStruct(shape, kind) for shape, kind, space in outs],
        scratch_shapes=list(scratch),
        compiler_params=pltpu.CompilerParams(vmem_limit_bytes=36 * 1024 * 1024),
    )(*operands)


def per_device(
    tokens, lengths, cache_keys, cache_values, query_w, key_w, value_w, out_w, mix_lambda, head_gain, attn_gain, ffn_gain,
    routes, route_weights, exp_gate, exp_up, exp_down, dense_gate, dense_up, dense_down, branch_gate,
):
    rows = tokens.shape[0]
    me = lax.axis_index("ep")
    core = me % 2
    ids = jnp.stack([core, me // 16]).astype(jnp.int32)

    smem, hbm, vmem = pltpu.SMEM, pltpu.HBM, pltpu.VMEM
    (pieces,) = call(
        pieces_kernel,
        [((8, PIECE, 256), bf16, vmem)],
        [jnp.swapaxes(dense_gate[0], 0, 1), jnp.swapaxes(dense_up[0], 0, 1), dense_down[0]],
        [pltpu.VMEM((3, 352, 256), bf16), pltpu.SemaphoreType.DMA((3,))],
        {0: hbm, 1: hbm, 2: hbm},
    )
    columns = [[16 * b + j for b in range(8)] for j in range(16)]
    pieces = lax.all_to_all(pieces, "ep", 0, 0, axis_index_groups=columns, tiled=True)

    positions = cache_keys.shape[0] * cache_keys.shape[1] * KV_HEADS
    pair, hidden_state, key_new, value_new = call(
        attend_kernel,
        [
            ((2, rows, HALF + TAIL), bf16, vmem), ((rows, D), f32, vmem),
            ((rows, KV_HEADS * HEAD_DIM), bf16, hbm), ((rows, KV_HEADS * HEAD_DIM), bf16, hbm),
        ],
        [
            lengths, routes.T, route_weights.T, tokens, mix_lambda, head_gain.reshape(1, HEAD_DIM),
            attn_gain.reshape(1, D), ffn_gain.reshape(1, D), query_w, key_w, value_w,
            cache_keys.reshape(positions, HEAD_DIM), cache_values.reshape(positions, HEAD_DIM), out_w,
        ],
        [
            pltpu.VMEM(query_w.shape, bf16), pltpu.VMEM(key_w.shape, bf16), pltpu.VMEM(value_w.shape, bf16),
            pltpu.VMEM((positions, HEAD_DIM), bf16), pltpu.VMEM((positions, HEAD_DIM), bf16), pltpu.VMEM(out_w.shape, bf16),
            pltpu.SemaphoreType.DMA((28,)), pltpu.VMEM((32, HEAD_DIM), f32), pltpu.VMEM((rows, HEADS * HEAD_DIM), f32),
            pltpu.SMEM((rows,), jnp.int32), pltpu.SMEM((2, rows), jnp.int32), pltpu.SMEM((2, rows), f32), pltpu.VMEM((rows, D), bf16),
            pltpu.SMEM((HEADS,), f32), pltpu.VMEM((1, HEAD_DIM), f32), pltpu.VMEM((1, D), f32), pltpu.VMEM((1, D), f32),
            pltpu.VMEM((rows, KV_HEADS * HEAD_DIM), bf16), pltpu.VMEM((rows, KV_HEADS * HEAD_DIM), bf16),
        ],
        {k: hbm for k in range(14)},
    )
    outgoing = jnp.broadcast_to(pair[None], (64, 2, rows, HALF + TAIL)).reshape(DEVICES, rows, HALF + TAIL)
    outgoing, pieces = lax.optimization_barrier((outgoing, pieces))
    own = lax.all_to_all(outgoing, "ep", 0, 0, tiled=True)
    theirs = to_partner(own)
    hidden_units = exp_gate.shape[1]
    sums, both, near, w_rest, w_out = call(
        near_kernel,
        [
            ((512, 2 * hidden_units), f32, vmem), ((512, 256), f32, vmem), ((8, 256, 256), bf16, vmem),
            ((HALF, 2 * hidden_units), bf16, vmem), ((hidden_units + 128, D), bf16, vmem),
        ],
        [ids, own, pieces, branch_gate.reshape(1, D), exp_gate, exp_up, exp_down],
        [pltpu.VMEM((HALF, 2 * hidden_units), bf16), pltpu.SemaphoreType.DMA((5,))],
        {0: smem, 4: hbm, 5: hbm, 6: hbm},
    )
    y_other, acts = call(
        rest_kernel,
        [((512, HALF), bf16, vmem), ((512, hidden_units + 128), bf16, vmem)],
        [ids, theirs, sums, both, near, w_rest, w_out],
        [],
        {0: smem},
    )
    y_recv = to_partner(y_other)
    (y_own,) = call(own_kernel, [((512, HALF), f32, vmem)], [ids, acts, w_out], [], {0: smem})
    (joined,) = call(join_kernel, [((DEVICES, rows, HALF), bf16, vmem)], [y_own, y_recv])
    parts = lax.all_to_all(joined, "ep", 0, 0, tiled=True)
    (output,) = call(last_kernel, [((rows, D), bf16, None)], [hidden_state, parts])
    return (output, key_new, value_new)


def solution(mesh):
    placed = (
        P("ep", None),
        P("ep"),
        P("ep", None, None, None),
        P("ep", None, None, None),
        P(),
        P(),
        P(),
        P(),
        P(),
        P(),
        P(),
        P(),
        P("ep", None),
        P("ep", None),
        P(None, "ep"),
        P(None, "ep"),
        P("ep", None),
        P("ep", None, None),
        P("ep", None, None),
        P("ep", None, None),
        P(),
    )

    return jax.shard_map(
        per_device,
        mesh=mesh,
        in_specs=placed,
        out_specs=(P("ep", None), P("ep", None), P("ep", None)),
        check_vma=False,
    )
```

time: 85.7 us -> 83.7 us (0.977)
  Pallas kernels: 20 us -> 18.1 us
  waiting for transfers between devices: 3.61 us -> 5.06 us
  blocking collectives: 50.8 us -> 49.7 us
    pallas_call x7, Pallas kernels: 20 us -> 18.1 us  [call(): pl.pallas_call(kernel, in_specs=[pl.BlockSpec(memory_space=spaces.get(k,...]
    all_to_all x1, waiting for transfers between devices: 2.5 us -> 3.67 us  [per_device(): lax.all_to_all(pieces, 'ep', 0, 0, axis_index_groups=columns, tiled=True)]
    all_to_all x1, blocking collectives: 28.2 us -> 27.1 us  [per_device(): own = lax.all_to_all(outgoing, 'ep', 0, 0, tiled=True)]
  transfers between devices with their start and end apart: 3 -> 3, of which waited for: 2 -> 2; matrix products, arithmetic and copies ran while one was open for 0% -> 0% of each run, Pallas kernels for 16% -> 15%
where the time goes in v3:
time: 83.7 us; the launch traced here: 83.5 us
  blocking collectives  49.7 us (59%)
  Pallas kernels  18.1 us (22%)
  starting transfers between devices  9.54 us (11%)
  waiting for transfers between devices  5.06 us (6%)
    all_to_all x1, blocking collectives, per_device(): own = lax.all_to_all(outgoing, 'ep', 0, 0, tiled=True)  27.1 us
    all_to_all x1, blocking collectives, per_device(): parts = lax.all_to_all(joined, 'ep', 0, 0, tiled=True)  22.6 us
    pallas_call x7, Pallas kernels, call(): pl.pallas_call(kernel, in_specs=[pl.BlockSpec(memory_space=spaces.get(k,...  18.1 us
    all_to_all x1, starting transfers between devices, per_device(): lax.all_to_all(pieces, 'ep', 0, 0, axis_index_groups=columns, tiled=True)  8.49 us
    all_to_all x1, waiting for transfers between devices, per_device(): lax.all_to_all(pieces, 'ep', 0, 0, axis_index_groups=columns, tiled=True)  3.67 us
  transfers between devices with their start and end apart: 3, of which 2 were waited for; matrix products, arithmetic and copies ran while one was open for 0% of the time, Pallas kernels for 15%

profile of v3, /device:TPU:1, one launch (start us, length us, event | category | flops | bytes accessed | tf_op | source)
XLA Modules:
  0.0 83.5 jit_solution(16655991999452829400)
XLA Ops:
  0.6 1.9 %shard_map.221 = bf16[8,144,256]{2,1,0:T(8,128)(2,1)} custom-call(bf16[352,256]{1,0:T(8,128)(2,1)} %bitcast.20, bf16[352,256]{1,0:T(8,128)(2,1)} %bitcast.21, bf16[352,256]{1,0:T(8,128)(2,1)} %bitcast.22), custom_call_target="tpu_custom_call" | custom-call | tf_op jit(solution)/shard_map/pallas_call | solution.py:248
  2.6 8.5 %all-to-all-start = ((bf16[8,144,256]{2,1,0:T(8,128)(2,1)}), bf16[8,144,256]{2,1,0:T(8,128)(2,1)S(1)}, u32[]{:S(2)}, u32[]{:S(2)}) async-start(bf16[8,144,256]{2,1,0:T(8,128)(2,1)} %shard_map.221), calls=%async_computation | async-start | bytes 1179648 | tf_op jit(solution)/shard_map/all_to_all | solution.py:276
  11.1 7.7 %shard_map.220 = (bf16[2,4,1152]{2,1,0:T(4,128)(2,1)S(1)}, f32[4,2048]{1,0:T(4,128)S(1)}, bf16[4,256]{1,0:T(4,128)(2,1)}, bf16[4,256]{1,0:T(4,128)(2,1)}) custom-call(s32[4]{0:T(128)} %lengths_hbm.1, s32[2,4]{1,0:T(2,128)} %bitcast.25, f32[2,4]{1,0:T(2,128)} %bitcast.26, bf16[4,2048]{1,0:T(4,128)(2,1)} %tokens_hbm.1, f32[8]{0:T(128)} %mix_hbm.1, ...), custom_call_target="tpu_custom_call" | custom-call | tf_op jit(solution)/shard_map/pallas_call | solution.py:248
  18.8 3.7 %all-to-all-done.pieces = bf16[8,144,256]{2,1,0:T(8,128)(2,1)S(1)} async-done(((bf16[8,144,256]{2,1,0:T(8,128)(2,1)}), bf16[8,144,256]{2,1,0:T(8,128)(2,1)S(1)}, u32[]{:S(2)}, u32[]{:S(2)}) %all-to-all-start) | async-done | bytes 589856 | tf_op jit(solution)/shard_map/all_to_all | solution.py:276
  22.5 0.0 copy-start
  22.5 0.3 broadcast_in_dim.2
  22.8 27.1 %all_to_all.15.own = bf16[128,4,1152]{2,1,0:T(4,128)(2,1)S(1)} all-to-all(bf16[128,4,1152]{2,1,0:T(4,128)(2,1)S(1)} %bitcast.17), channel_id=1, replica_groups=mesh['ep'=128] {'ep'}, dimensions={0} | all-to-all | bytes 2359296 | tf_op jit(solution)/shard_map/all_to_all | solution.py:302
  49.9 1.0 %collective-permute-start = (bf16[128,4,1152]{2,1,0:T(4,128)(2,1)S(1)}, bf16[128,4,1152]{2,1,0:T(4,128)(2,1)S(1)}, u32[]{:S(2)}, u32[]{:S(2)}) collective-permute-start(bf16[128,4,1152]{2,1,0:T(4,128)(2,1)S(1)} %all_to_all.15.own), channel_id=1, source_target_pairs={{0,1},{1,0},{2,3},{3,2},{4,5},{5,4},{6,7},{7,6},{8,9},{9,8},{10,11... | collective-permute-start | bytes 3538952 | tf_op jit(solution)/shard_map/ppermute | solution.py:23
  50.8 0.0 copy-done
  50.8 0.1 pad_add_fusion.ids
  50.9 3.7 %shard_map.222 = (f32[512,768]{1,0:T(8,128)S(1)}, f32[512,256]{1,0:T(8,128)S(1)}, bf16[8,256,256]{2,1,0:T(8,128)(2,1)S(1)}, bf16[1024,768]{1,0:T(8,128)(2,1)S(1)}, bf16[512,2048]{1,0:T(8,128)(2,1)S(1)}) custom-call(s32[2]{0:T(128)S(1)} %pad_add_fusion.ids, bf16[128,4,1152]{2,1,0:T(4,128)(2,1)S(1)} %all_to_all.15.own, ...), custom_call_target="tpu_custom_call" | custom-call | tf_op jit(solution)/shard_map/pallas_call | solution.py:248
  54.6 0.0 collective-permute-done.theirs
  54.6 2.5 %shard_map.223 = (bf16[512,1024]{1,0:T(8,128)(2,1)S(1)}, bf16[512,512]{1,0:T(8,128)(2,1)S(1)}) custom-call(s32[2]{0:T(128)S(1)} %pad_add_fusion.ids, bf16[128,4,1152]{2,1,0:T(4,128)(2,1)S(1)} %collective-permute-done.theirs, f32[512,768]{1,0:T(8,128)S(1)} %get-tuple-element.20.sums_near, f32[512,256]{1,0:T(8,128)S(1)} %get-tuple-element.21.both_near, ...), custom_call_target="tpu_custom_call" | custom-call | tf_op jit(solution)/shard_map/pallas_call | solution.py:248
  57.1 0.1 collective-permute-start.1
  57.2 1.3 %shard_map.224.y_own = f32[512,1024]{1,0:T(8,128)S(1)} custom-call(s32[2]{0:T(128)S(1)} %pad_add_fusion.ids, bf16[512,512]{1,0:T(8,128)(2,1)S(1)} %get-tuple-element.25.acts, bf16[512,2048]{1,0:T(8,128)(2,1)S(1)} %get-tuple-element.24.w_out), custom_call_target="tpu_custom_call" | custom-call | tf_op jit(solution)/shard_map/pallas_call | solution.py:248
  58.4 1.4 %collective-permute-done.1.y_recv = bf16[512,1024]{1,0:T(8,128)(2,1)S(1)} collective-permute-done((bf16[512,1024]{1,0:T(8,128)(2,1)S(1)}, bf16[512,1024]{1,0:T(8,128)(2,1)S(1)}, u32[]{:S(2)}, u32[]{:S(2)}) %collective-permute-start.1) | collective-permute-done | bytes 1048608 | tf_op jit(solution)/shard_map/ppermute | solution.py:23
  59.8 0.3 shard_map.225
  60.1 22.6 %all_to_all.16.parts = bf16[128,4,1024]{2,1,0:T(4,128)(2,1)S(1)} all-to-all(bf16[128,4,1024]{2,1,0:T(4,128)(2,1)S(1)} %shard_map.225), channel_id=1, replica_groups=mesh['ep'=128] {'ep'}, dimensions={0} | all-to-all | bytes 2097152 | tf_op jit(solution)/shard_map/all_to_all | solution.py:325
  82.7 0.8 shard_map.226
  (1 shorter events, 0.0 us)
Async XLA Ops:
  2.6 19.9 %all-to-all-start = ((bf16[8,144,256]{2,1,0:T(8,128)(2,1)}), bf16[8,144,256]{2,1,0:T(8,128)(2,1)S(1)}, u32[]{:S(2)}, u32[]{:S(2)}) async-start(bf16[8,144,256]{2,1,0:T(8,128)(2,1)} %shard_map.221), calls=%async_computation | async-start | bytes 1179648 | tf_op jit(solution)/shard_map/all_to_all | solution.py:276
  22.5 28.4 %copy-start = (bf16[2048]{0:T(1024)(128)(2,1)S(1)}, bf16[2048]{0:T(1024)(128)(2,1)}, u32[]{:S(2)}) copy-start(bf16[2048]{0:T(1024)(128)(2,1)} %param.41) | copy-start | bytes 12292
  49.9 4.8 %collective-permute-start = (bf16[128,4,1152]{2,1,0:T(4,128)(2,1)S(1)}, bf16[128,4,1152]{2,1,0:T(4,128)(2,1)S(1)}, u32[]{:S(2)}, u32[]{:S(2)}) collective-permute-start(bf16[128,4,1152]{2,1,0:T(4,128)(2,1)S(1)} %all_to_all.15.own), channel_id=1, source_target_pairs={{0,1},{1,0},{2,3},{3,2},{4,5},{5,4},{6,7},{7,6},{8,9},{9,8},{10,11... | collective-permute-start | bytes 3538952 | tf_op jit(solution)/shard_map/ppermute | solution.py:23
  57.1 2.7 %collective-permute-start.1 = (bf16[512,1024]{1,0:T(8,128)(2,1)S(1)}, bf16[512,1024]{1,0:T(8,128)(2,1)S(1)}, u32[]{:S(2)}, u32[]{:S(2)}) collective-permute-start(bf16[512,1024]{1,0:T(8,128)(2,1)S(1)} %get-tuple-element.26), channel_id=1, source_target_pairs={{0,1},{1,0},{2,3},{3,2},{4,5},{5,4},{6,7},{7,6},{8,9},{9,8},{10,11... | collective-permute-start | bytes 3145736 | tf_op jit(solution)/shard_map/ppermute | solution.py:23

commit v4 on v3

--- a/solution.py
+++ b/solution.py
@@ -147,17 +147,22 @@
         copy.wait()
 
 
-def pieces_kernel(gate, up, down, out, held, sem):
-    copies = [pltpu.make_async_copy(ref, held.at[m], sem.at[m]) for m, ref in enumerate((gate, up, down))]
+def pieces_kernel(ids, gate, up, down, *refs):
+    outs, held, sem = refs[:4], refs[4], refs[5]
+    copies = [
+        pltpu.make_async_copy(ref, held.at[m, pl.ds(0, ref.shape[0]), :], sem.at[m]) for m, ref in enumerate((gate, up, down))
+    ]
     for copy in copies:
         copy.start()
+    held[:, gate.shape[0] :, :] = jnp.zeros((3, 8 * UNITS - gate.shape[0], 256), bf16)
     for m in range(3):
         copies[m].wait()
-        for k in range(8):
-            size = min(UNITS, held.shape[1] - k * UNITS)
-            out[k, m * UNITS : m * UNITS + size, :] = held[m, k * UNITS : k * UNITS + size, :]
-            if size < UNITS:
-                out[k, m * UNITS + size : (m + 1) * UNITS, :] = jnp.zeros((UNITS - size, 256), bf16)
+        for k in range(4):
+            for side in range(2):
+                run = 2 * jnp.bitwise_and(ids[3] + k, 3) + jnp.bitwise_xor(ids[2], side)
+                start = pl.multiple_of(run * UNITS, 16)
+                at = side * PIECE + m * UNITS
+                outs[k][at : at + UNITS, :] = held[m, pl.ds(start, UNITS), :]
 
 
 def dot(a, b):
@@ -172,7 +177,7 @@
     return both
 
 
-def near_kernel(ids, own, pieces, branch, gate_hbm, up_hbm, down_hbm, sums, both, near, w_rest, w_out, w_own, sem):
+def near_kernel(ids, own, first, second, third, fourth, crossed, branch, gate_hbm, up_hbm, down_hbm, sums, both, near, w_rest, w_out, w_own, sem):
     core = ids[0]
     mine = pl.ds(pl.multiple_of(core * HALF, HALF), HALF)
     rest = pl.ds(pl.multiple_of((1 - core) * HALF, HALF), HALF)
@@ -193,10 +198,14 @@
     near[...] = jnp.zeros_like(near)
     w_out[wide + UNITS :, :] = jnp.zeros((128 - UNITS, D), bf16)
     for b in range(8):
-        near[b, 0:UNITS, :] = pieces[b, 0:UNITS, :]
-        near[b, 128 : 128 + UNITS, :] = pieces[b, UNITS : 2 * UNITS, :]
         near[b, 64:72, :] = jnp.broadcast_to(branch[:, b * 256 : (b + 1) * 256], (8, 256))
-        w_out[wide : wide + UNITS, b * 256 : (b + 1) * 256] = pieces[b, 2 * UNITS :, :]
+    for k, ref in enumerate((first, second, third, fourth)):
+        for side in range(2):
+            block = 2 * jnp.bitwise_and(ids[3] + 4 - k, 3) + jnp.bitwise_xor(ids[2], side)
+            piece = ref[0:PIECE, :] if side == 0 else crossed[k]
+            near[block, 0:UNITS, :] = piece[0:UNITS, :]
+            near[block, 128 : 128 + UNITS, :] = piece[UNITS : 2 * UNITS, :]
+            w_out[wide : wide + UNITS, pl.ds(pl.multiple_of(block * 256, 256), 256)] = piece[2 * UNITS :, :]
     x = own[:, :, 0:HALF].reshape(512, HALF)
     both[...] = dense_sums(x, near, core * 4)
     copies[0].wait()
@@ -262,18 +271,18 @@
     rows = tokens.shape[0]
     me = lax.axis_index("ep")
     core = me % 2
-    ids = jnp.stack([core, me // 16]).astype(jnp.int32)
+    ids = jnp.stack([core, me // 16, me // 16 % 2, me // 32]).astype(jnp.int32)
 
     smem, hbm, vmem = pltpu.SMEM, pltpu.HBM, pltpu.VMEM
-    (pieces,) = call(
+    pieces = call(
         pieces_kernel,
-        [((8, PIECE, 256), bf16, vmem)],
-        [jnp.swapaxes(dense_gate[0], 0, 1), jnp.swapaxes(dense_up[0], 0, 1), dense_down[0]],
-        [pltpu.VMEM((3, 352, 256), bf16), pltpu.SemaphoreType.DMA((3,))],
-        {0: hbm, 1: hbm, 2: hbm},
-    )
-    columns = [[16 * b + j for b in range(8)] for j in range(16)]
-    pieces = lax.all_to_all(pieces, "ep", 0, 0, axis_index_groups=columns, tiled=True)
+        [((2 * PIECE, 256), bf16, vmem)] * 4,
+        [ids, jnp.swapaxes(dense_gate[0], 0, 1), jnp.swapaxes(dense_up[0], 0, 1), dense_down[0]],
+        [pltpu.VMEM((3, 8 * UNITS, 256), bf16), pltpu.SemaphoreType.DMA((3,))],
+        {0: smem, 1: hbm, 2: hbm, 3: hbm},
+    )
+    turned = [lax.ppermute(pieces[k], "ep", [(i, (i + 32 * k) % DEVICES) for i in range(DEVICES)]) for k in (1, 3, 2)]
+    pieces = [pieces[0], turned[0], turned[2], turned[1]]
 
     positions = cache_keys.shape[0] * cache_keys.shape[1] * KV_HEADS
     pair, hidden_state, key_new, value_new = call(
@@ -298,7 +307,7 @@
         {k: hbm for k in range(14)},
     )
     outgoing = jnp.broadcast_to(pair[None], (64, 2, rows, HALF + TAIL)).reshape(DEVICES, rows, HALF + TAIL)
-    outgoing, pieces = lax.optimization_barrier((outgoing, pieces))
+    crossed = lax.ppermute(jnp.stack([x[PIECE:] for x in pieces]), "ep", [(i, i ^ 16) for i in range(DEVICES)])
     own = lax.all_to_all(outgoing, "ep", 0, 0, tiled=True)
     theirs = to_partner(own)
     hidden_units = exp_gate.shape[1]
@@ -308,9 +317,9 @@
             ((512, 2 * hidden_units), f32, vmem), ((512, 256), f32, vmem), ((8, 256, 256), bf16, vmem),
             ((HALF, 2 * hidden_units), bf16, vmem), ((hidden_units + 128, D), bf16, vmem),
         ],
-        [ids, own, pieces, branch_gate.reshape(1, D), exp_gate, exp_up, exp_down],
+        [ids, own, *pieces, crossed, branch_gate.reshape(1, D), exp_gate, exp_up, exp_down],
         [pltpu.VMEM((HALF, 2 * hidden_units), bf16), pltpu.SemaphoreType.DMA((5,))],
-        {0: smem, 4: hbm, 5: hbm, 6: hbm},
+        {0: smem, 8: hbm, 9: hbm, 10: hbm},
     )
     y_other, acts = call(
         rest_kernel,

time: 83.7 us -> 91.1 us (1.088)
  blocking collectives: 49.7 us -> 24.5 us
  waiting for transfers between devices: 5.06 us -> 26.5 us
  starting transfers between devices: 9.54 us -> 19.5 us
  local copies, waits for them, and re-layouts: 0.32 us -> 1.37 us
    all_to_all x1 -> x0, blocking collectives: 27.1 us -> none  [per_device(): own = lax.all_to_all(outgoing, 'ep', 0, 0, tiled=True)]
    all_to_all x1, waiting for transfers between devices: 3.67 us -> 14.6 us  [per_device(): own = lax.all_to_all(outgoing, 'ep', 0, 0, tiled=True)]
    ppermute x0 -> x4, waiting for transfers between devices: none -> 10.8 us  [the longest x1 8.26 us: per_device(): lax.ppermute(jnp.stack([x[PIECE:] for x in pieces]), 'ep', [(i, i ^ 16) f...]
    ppermute x0 -> x4, starting transfers between devices: none -> 5.65 us  [the longest x3 4.19 us: per_device(): lax.ppermute(pieces[k], 'ep', [(i, (i + 32 * k) % DEVICES) for i in range...]
    all_to_all x1, starting transfers between devices: 8.49 us -> 11.5 us  [per_device(): own = lax.all_to_all(outgoing, 'ep', 0, 0, tiled=True)]
    all_to_all x1, blocking collectives: 22.6 us -> 24.5 us  [per_device(): parts = lax.all_to_all(joined, 'ep', 0, 0, tiled=True)]
    ppermute x2, starting transfers between devices: 1.05 us -> 2.33 us  [to_partner(): return lax.ppermute(x, 'ep', [(i, i ^ 1) for i in range(DEVICES)])]
    broadcast_in_dim x1, local copies, waits for them, and re-layouts: 0.31 us -> 1.34 us  [per_device(): jnp.broadcast_to(pair[None], (64, 2, rows, HALF + TAIL))]
  transfers between devices with their start and end apart: 3 -> 7, of which waited for: 2 -> 4; matrix products, arithmetic and copies ran while one was open for 0% -> 0% of each run, Pallas kernels for 15% -> 8%
where the time goes in v4:
time: 91.1 us; the launch traced here: 90.8 us
  waiting for transfers between devices  26.5 us (29%)
  blocking collectives  24.5 us (27%)
  starting transfers between devices  19.5 us (21%)
  Pallas kernels  18.1 us (20%)
  local copies, waits for them, and re-layouts  1.37 us (2%)
    all_to_all x1, blocking collectives, per_device(): parts = lax.all_to_all(joined, 'ep', 0, 0, tiled=True)  24.5 us
    pallas_call x7, Pallas kernels, call(): pl.pallas_call(kernel, in_specs=[pl.BlockSpec(memory_space=spaces.get(k,...  18.1 us
    all_to_all x1, waiting for transfers between devices, per_device(): own = lax.all_to_all(outgoing, 'ep', 0, 0, tiled=True)  14.6 us
    all_to_all x1, starting transfers between devices, per_device(): own = lax.all_to_all(outgoing, 'ep', 0, 0, tiled=True)  11.5 us
    ppermute x1, waiting for transfers between devices, per_device(): lax.ppermute(jnp.stack([x[PIECE:] for x in pieces]), 'ep', [(i, i ^ 16) f...  8.26 us
    ppermute x3, starting transfers between devices, per_device(): lax.ppermute(pieces[k], 'ep', [(i, (i + 32 * k) % DEVICES) for i in range...  4.19 us
    ppermute x3, waiting for transfers between devices, per_device(): lax.ppermute(pieces[k], 'ep', [(i, (i + 32 * k) % DEVICES) for i in range...  2.59 us
    ppermute x2, starting transfers between devices, to_partner(): return lax.ppermute(x, 'ep', [(i, i ^ 1) for i in range(DEVICES)])  2.33 us
  transfers between devices with their start and end apart: 7, of which 4 were waited for; matrix products, arithmetic and copies ran while one was open for 0% of the time, Pallas kernels for 8%

profile of v4, /device:TPU:1, one launch (start us, length us, event | category | flops | bytes accessed | tf_op | source)
XLA Modules:
  0.0 90.8 jit_solution(11174747785416183069)
XLA Ops:
  0.6 7.7 %shard_map.220 = (bf16[2,4,1152]{2,1,0:T(4,128)(2,1)S(1)}, f32[4,2048]{1,0:T(4,128)S(1)}, bf16[4,256]{1,0:T(4,128)(2,1)}, bf16[4,256]{1,0:T(4,128)(2,1)}) custom-call(s32[4]{0:T(128)} %lengths_hbm.1, s32[2,4]{1,0:T(2,128)} %bitcast.34, f32[2,4]{1,0:T(2,128)} %bitcast.35, bf16[4,2048]{1,0:T(4,128)(2,1)} %tokens_hbm.1, f32[8]{0:T(128)} %mix_hbm.1, ...), custom_call_target="tpu_custom_call" | custom-call | tf_op jit(solution)/shard_map/pallas_call | solution.py:257
  8.4 1.3 %broadcast_in_dim.2 = bf16[64,2,4,1152]{3,2,1,0:T(4,128)(2,1)} broadcast(bf16[2,4,1152]{2,1,0:T(4,128)(2,1)S(1)} %get-tuple-element.19), dimensions={1,2,3} | broadcast | bytes 1198080 | tf_op jit(solution)/shard_map/broadcast_in_dim | solution.py:309
  9.7 0.0 copy-start
  9.7 11.5 %all-to-all-start = ((bf16[128,4,1152]{2,1,0:T(4,128)(2,1)}), bf16[128,4,1152]{2,1,0:T(4,128)(2,1)S(1)}, u32[]{:S(2)}, u32[]{:S(2)}) async-start(bf16[128,4,1152]{2,1,0:T(4,128)(2,1)} %bitcast.11), calls=%async_computation | async-start | bytes 2359296 | tf_op jit(solution)/shard_map/all_to_all | solution.py:311
  21.2 0.1 pad_add_fusion.ids
  21.3 1.7 %shard_map.221 = (bf16[288,256]{1,0:T(8,128)(2,1)S(1)}, bf16[288,256]{1,0:T(8,128)(2,1)S(1)}, bf16[288,256]{1,0:T(8,128)(2,1)S(1)}, bf16[288,256]{1,0:T(8,128)(2,1)S(1)}) custom-call(s32[4]{0:T(128)S(1)} %pad_add_fusion.ids, bf16[352,256]{1,0:T(8,128)(2,1)} %bitcast.29, bf16[352,256]{1,0:T(8,128)(2,1)} %bitcast.30, bf16[352,256]{1,0:T(8,128)(2,1)} %bitcast.31), custom_call_target="tpu_custom_call" | custom-call | tf_op jit(solution)/shard_map/pallas_call | solution.py:257
  23.0 3.3 %collective-permute-start.3 = (bf16[288,256]{1,0:T(8,128)(2,1)S(1)}, bf16[288,256]{1,0:T(8,128)(2,1)S(1)}, u32[]{:S(2)}, u32[]{:S(2)}) collective-permute-start(bf16[288,256]{1,0:T(8,128)(2,1)S(1)} %get-tuple-element.23), channel_id=1, source_target_pairs={{0,96},{1,97},{2,98},{3,99},{4,100},{5,101},{6,102},{7,103},{8,104... | collective-permute-start | bytes 442376 | tf_op jit(solution)/shard_map/ppermute | solution.py:284
  26.3 0.1 collective-permute-start.2
  26.4 0.8 collective-permute-start.1
  27.2 14.6 %all-to-all-done.own = bf16[128,4,1152]{2,1,0:T(4,128)(2,1)S(1)} async-done(((bf16[128,4,1152]{2,1,0:T(4,128)(2,1)}), bf16[128,4,1152]{2,1,0:T(4,128)(2,1)S(1)}, u32[]{:S(2)}, u32[]{:S(2)}) %all-to-all-start) | async-done | bytes 1179680 | tf_op jit(solution)/shard_map/all_to_all | solution.py:311
  41.8 1.0 %collective-permute-start = (bf16[128,4,1152]{2,1,0:T(4,128)(2,1)S(1)}, bf16[128,4,1152]{2,1,0:T(4,128)(2,1)S(1)}, u32[]{:S(2)}, u32[]{:S(2)}) collective-permute-start(bf16[128,4,1152]{2,1,0:T(4,128)(2,1)S(1)} %all-to-all-done.own), channel_id=1, source_target_pairs={{0,1},{1,0},{2,3},{3,2},{4,5},{5,4},{6,7},{7,6},{8,9},{9,8},{10,11... | collective-permute-start | bytes 3538952 | tf_op jit(solution)/shard_map/ppermute | solution.py:23
  42.8 0.0 collective-permute-done.3.fourth
  42.8 0.0 collective-permute-done.2.third
  42.8 2.6 %collective-permute-done.1.second = bf16[288,256]{1,0:T(8,128)(2,1)S(1)} collective-permute-done((bf16[288,256]{1,0:T(8,128)(2,1)S(1)}, bf16[288,256]{1,0:T(8,128)(2,1)S(1)}, u32[]{:S(2)}, u32[]{:S(2)}) %collective-permute-start.1) | collective-permute-done | bytes 147488 | tf_op jit(solution)/shard_map/ppermute | solution.py:284
  45.5 1.5 %collective-permute-start.4 = (bf16[4,144,256]{2,1,0:T(8,128)(2,1)S(1)}, bf16[4,144,256]{2,1,0:T(8,128)(2,1)S(1)}, u32[]{:S(2)}, u32[]{:S(2)}) collective-permute-start(bf16[4,144,256]{2,1,0:T(8,128)(2,1)S(1)} %pad_maximum_fusion), channel_id=1, source_target_pairs={{0,16},{1,17},{2,18},{3,19},{4,20},{5,21},{6,22},{7,23},{8,24},{9,... | collective-permute-start | bytes 884744 | tf_op jit(solution)/shard_map/ppermute | solution.py:310
  46.9 0.0 copy-done
  47.0 8.3 %collective-permute-done.4.crossed = bf16[4,144,256]{2,1,0:T(8,128)(2,1)S(1)} collective-permute-done((bf16[4,144,256]{2,1,0:T(8,128)(2,1)S(1)}, bf16[4,144,256]{2,1,0:T(8,128)(2,1)S(1)}, u32[]{:S(2)}, u32[]{:S(2)}) %collective-permute-start.4) | collective-permute-done | bytes 294944 | tf_op jit(solution)/shard_map/ppermute | solution.py:310
  55.2 3.9 %shard_map.222 = (f32[512,768]{1,0:T(8,128)S(1)}, f32[512,256]{1,0:T(8,128)S(1)}, bf16[8,256,256]{2,1,0:T(8,128)(2,1)S(1)}, bf16[1024,768]{1,0:T(8,128)(2,1)S(1)}, bf16[512,2048]{1,0:T(8,128)(2,1)S(1)}) custom-call(s32[4]{0:T(128)S(1)} %pad_add_fusion.ids, bf16[128,4,1152]{2,1,0:T(4,128)(2,1)S(1)} %all-to-all-done.own, ...), custom_call_target="tpu_custom_call" | custom-call | tf_op jit(solution)/shard_map/pallas_call | solution.py:257
  59.1 0.0 collective-permute-done.theirs
  59.1 2.5 %shard_map.223 = (bf16[512,1024]{1,0:T(8,128)(2,1)S(1)}, bf16[512,512]{1,0:T(8,128)(2,1)S(1)}) custom-call(s32[4]{0:T(128)S(1)} %pad_add_fusion.ids, bf16[128,4,1152]{2,1,0:T(4,128)(2,1)S(1)} %collective-permute-done.theirs, f32[512,768]{1,0:T(8,128)S(1)} %get-tuple-element.24.sums_near, f32[512,256]{1,0:T(8,128)S(1)} %get-tuple-element.25.both_near, ...), custom_call_target="tpu_custom_call" | custom-call | tf_op jit(solution)/shard_map/pallas_call | solution.py:257
  61.6 1.4 %collective-permute-start.5 = (bf16[512,1024]{1,0:T(8,128)(2,1)S(1)}, bf16[512,1024]{1,0:T(8,128)(2,1)S(1)}, u32[]{:S(2)}, u32[]{:S(2)}) collective-permute-start(bf16[512,1024]{1,0:T(8,128)(2,1)S(1)} %get-tuple-element.30), channel_id=1, source_target_pairs={{0,1},{1,0},{2,3},{3,2},{4,5},{5,4},{6,7},{7,6},{8,9},{9,8},{10,11... | collective-permute-start | bytes 3145736 | tf_op jit(solution)/shard_map/ppermute | solution.py:23
  63.0 1.3 %shard_map.224.y_own = f32[512,1024]{1,0:T(8,128)S(1)} custom-call(s32[4]{0:T(128)S(1)} %pad_add_fusion.ids, bf16[512,512]{1,0:T(8,128)(2,1)S(1)} %get-tuple-element.29.acts, bf16[512,2048]{1,0:T(8,128)(2,1)S(1)} %get-tuple-element.28.w_out), custom_call_target="tpu_custom_call" | custom-call | tf_op jit(solution)/shard_map/pallas_call | solution.py:257
  64.2 1.0 %collective-permute-done.5.y_recv = bf16[512,1024]{1,0:T(8,128)(2,1)S(1)} collective-permute-done((bf16[512,1024]{1,0:T(8,128)(2,1)S(1)}, bf16[512,1024]{1,0:T(8,128)(2,1)S(1)}, u32[]{:S(2)}, u32[]{:S(2)}) %collective-permute-start.5) | collective-permute-done | bytes 1048608 | tf_op jit(solution)/shard_map/ppermute | solution.py:23
  65.2 0.3 shard_map.225
  65.5 24.5 %all_to_all.10.parts = bf16[128,4,1024]{2,1,0:T(4,128)(2,1)S(1)} all-to-all(bf16[128,4,1024]{2,1,0:T(4,128)(2,1)S(1)} %shard_map.225), channel_id=1, replica_groups=mesh['ep'=128] {'ep'}, dimensions={0} | all-to-all | bytes 2097152 | tf_op jit(solution)/shard_map/all_to_all | solution.py:334
  90.0 0.8 shard_map.226
  (6 shorter events, 0.1 us)
Async XLA Ops:
  9.7 37.2 %copy-start = (bf16[2048]{0:T(1024)(128)(2,1)S(1)}, bf16[2048]{0:T(1024)(128)(2,1)}, u32[]{:S(2)}) copy-start(bf16[2048]{0:T(1024)(128)(2,1)} %param.41) | copy-start | bytes 12292
  9.7 32.1 %all-to-all-start = ((bf16[128,4,1152]{2,1,0:T(4,128)(2,1)}), bf16[128,4,1152]{2,1,0:T(4,128)(2,1)S(1)}, u32[]{:S(2)}, u32[]{:S(2)}) async-start(bf16[128,4,1152]{2,1,0:T(4,128)(2,1)} %bitcast.11), calls=%async_computation | async-start | bytes 2359296 | tf_op jit(solution)/shard_map/all_to_all | solution.py:311
  23.0 19.8 %collective-permute-start.3 = (bf16[288,256]{1,0:T(8,128)(2,1)S(1)}, bf16[288,256]{1,0:T(8,128)(2,1)S(1)}, u32[]{:S(2)}, u32[]{:S(2)}) collective-permute-start(bf16[288,256]{1,0:T(8,128)(2,1)S(1)} %get-tuple-element.23), channel_id=1, source_target_pairs={{0,96},{1,97},{2,98},{3,99},{4,100},{5,101},{6,102},{7,103},{8,104... | collective-permute-start | bytes 442376 | tf_op jit(solution)/shard_map/ppermute | solution.py:284
  26.3 16.5 %collective-permute-start.2 = (bf16[288,256]{1,0:T(8,128)(2,1)S(1)}, bf16[288,256]{1,0:T(8,128)(2,1)S(1)}, u32[]{:S(2)}, u32[]{:S(2)}) collective-permute-start(bf16[288,256]{1,0:T(8,128)(2,1)S(1)} %get-tuple-element.22), channel_id=1, source_target_pairs={{0,64},{1,65},{2,66},{3,67},{4,68},{5,69},{6,70},{7,71},{8,72},{9,... | collective-permute-start | bytes 442376 | tf_op jit(solution)/shard_map/ppermute | solution.py:284
  26.4 19.0 %collective-permute-start.1 = (bf16[288,256]{1,0:T(8,128)(2,1)S(1)}, bf16[288,256]{1,0:T(8,128)(2,1)S(1)}, u32[]{:S(2)}, u32[]{:S(2)}) collective-permute-start(bf16[288,256]{1,0:T(8,128)(2,1)S(1)} %get-tuple-element.21), channel_id=1, source_target_pairs={{0,32},{1,33},{2,34},{3,35},{4,36},{5,37},{6,38},{7,39},{8,40},{9,... | collective-permute-start | bytes 442376 | tf_op jit(solution)/shard_map/ppermute | solution.py:284
  41.8 17.3 %collective-permute-start = (bf16[128,4,1152]{2,1,0:T(4,128)(2,1)S(1)}, bf16[128,4,1152]{2,1,0:T(4,128)(2,1)S(1)}, u32[]{:S(2)}, u32[]{:S(2)}) collective-permute-start(bf16[128,4,1152]{2,1,0:T(4,128)(2,1)S(1)} %all-to-all-done.own), channel_id=1, source_target_pairs={{0,1},{1,0},{2,3},{3,2},{4,5},{5,4},{6,7},{7,6},{8,9},{9,8},{10,11... | collective-permute-start | bytes 3538952 | tf_op jit(solution)/shard_map/ppermute | solution.py:23
  45.5 9.7 %collective-permute-start.4 = (bf16[4,144,256]{2,1,0:T(8,128)(2,1)S(1)}, bf16[4,144,256]{2,1,0:T(8,128)(2,1)S(1)}, u32[]{:S(2)}, u32[]{:S(2)}) collective-permute-start(bf16[4,144,256]{2,1,0:T(8,128)(2,1)S(1)} %pad_maximum_fusion), channel_id=1, source_target_pairs={{0,16},{1,17},{2,18},{3,19},{4,20},{5,21},{6,22},{7,23},{8,24},{9,... | collective-permute-start | bytes 884744 | tf_op jit(solution)/shard_map/ppermute | solution.py:310
  61.6 3.6 %collective-permute-start.5 = (bf16[512,1024]{1,0:T(8,128)(2,1)S(1)}, bf16[512,1024]{1,0:T(8,128)(2,1)S(1)}, u32[]{:S(2)}, u32[]{:S(2)}) collective-permute-start(bf16[512,1024]{1,0:T(8,128)(2,1)S(1)} %get-tuple-element.30), channel_id=1, source_target_pairs={{0,1},{1,0},{2,3},{3,2},{4,5},{5,4},{6,7},{7,6},{8,9},{9,8},{10,11... | collective-permute-start | bytes 3145736 | tf_op jit(solution)/shard_map/ppermute | solution.py:23

commit v5 on v4

--- a/solution.py
+++ b/solution.py
@@ -33,9 +33,10 @@
 
 
 def attend_kernel(
-    lengths_hbm, routes_hbm, route_weights_hbm, tokens_hbm, mix_hbm, head_gain_hbm, attn_gain_hbm, ffn_gain_hbm,
+    ids, lengths_hbm, routes_hbm, route_weights_hbm, tokens_hbm, mix_hbm, head_gain_hbm, attn_gain_hbm, ffn_gain_hbm,
     query_hbm, key_hbm, value_hbm, cache_keys, cache_values, out_hbm,
-    pair, hidden, key_out, value_out,
+    gate_hbm, up_hbm, down_hbm,
+    pair, hidden, key_out, value_out, w_own, w_rest, w_down,
     query_w, key_w, value_w, keys, values, out_w, sem, query_rows, head_rows,
     lengths, routes, route_weights, tokens, mix_lambda, head_gain, attn_gain, ffn_gain, key_new, value_new,
 ):
@@ -62,6 +63,12 @@
         on_values.append(fetch(cache_values.at[pl.ds(s * span, span), :], values.at[pl.ds(s * span, span), :]))
     on_out = [fetch(out_hbm.at[pl.ds(k * 256, 256), :], out_w.at[pl.ds(k * 256, 256), :]) for k in range(4)]
 
+    wide = gate_hbm.shape[1]
+    ahead = [fetch(down_hbm, w_down)]
+    for half, target in ((ids[0], w_own), (1 - ids[0], w_rest)):
+        rows = pl.ds(pl.multiple_of(half * HALF, HALF), HALF)
+        ahead.append(fetch(gate_hbm.at[rows, :], target.at[:, pl.ds(0, wide)]))
+        ahead.append(fetch(up_hbm.at[rows, :], target.at[:, pl.ds(wide, wide)]))
     for copy in on_tokens:
         copy.wait()
     x = tokens[...].astype(f32)
@@ -143,7 +150,7 @@
     ffn_in = rms_norm(state, ffn_gain[...], 1e-06).astype(bf16)
     for half in range(2):
         pair[half, :, 0:HALF] = ffn_in[:, half * HALF : (half + 1) * HALF]
-    for copy in written:
+    for copy in written + ahead:
         copy.wait()
 
 
@@ -177,24 +184,11 @@
     return both
 
 
-def near_kernel(ids, own, first, second, third, fourth, crossed, branch, gate_hbm, up_hbm, down_hbm, sums, both, near, w_rest, w_out, w_own, sem):
+def near_kernel(ids, own, first, second, third, fourth, crossed, branch, w_own, w_down, sums, both, near, w_out, sem):
     core = ids[0]
-    mine = pl.ds(pl.multiple_of(core * HALF, HALF), HALF)
-    rest = pl.ds(pl.multiple_of((1 - core) * HALF, HALF), HALF)
-    wide = gate_hbm.shape[1]
-    left, right = pl.ds(0, wide), pl.ds(wide, wide)
-    copies = [
-        pltpu.make_async_copy(source, target, sem.at[k])
-        for k, (source, target) in enumerate(
-            (
-                (gate_hbm.at[mine, :], w_own.at[:, left]), (up_hbm.at[mine, :], w_own.at[:, right]),
-                (gate_hbm.at[rest, :], w_rest.at[:, left]), (up_hbm.at[rest, :], w_rest.at[:, right]),
-                (down_hbm, w_out.at[pl.ds(0, wide), :]),
-            )
-        )
-    ]
-    for copy in copies:
-        copy.start()
+    wide = w_down.shape[0]
+    copy = pltpu.make_async_copy(w_down, w_out.at[pl.ds(0, wide), :], sem)
+    copy.start()
     near[...] = jnp.zeros_like(near)
     w_out[wide + UNITS :, :] = jnp.zeros((128 - UNITS, D), bf16)
     for b in range(8):
@@ -208,11 +202,8 @@
             w_out[wide : wide + UNITS, pl.ds(pl.multiple_of(block * 256, 256), 256)] = piece[2 * UNITS :, :]
     x = own[:, :, 0:HALF].reshape(512, HALF)
     both[...] = dense_sums(x, near, core * 4)
-    copies[0].wait()
-    copies[1].wait()
     sums[...] = dot(x, w_own[...])
-    for copy in copies[2:]:
-        copy.wait()
+    copy.wait()
 
 
 def rest_kernel(ids, theirs, sums_near, both_near, near, w_rest, w_out, y_other, acts):
@@ -269,6 +260,7 @@
     routes, route_weights, exp_gate, exp_up, exp_down, dense_gate, dense_up, dense_down, branch_gate,
 ):
     rows = tokens.shape[0]
+    hidden_units = exp_gate.shape[1]
     me = lax.axis_index("ep")
     core = me % 2
     ids = jnp.stack([core, me // 16, me // 16 % 2, me // 32]).astype(jnp.int32)
@@ -285,41 +277,41 @@
     pieces = [pieces[0], turned[0], turned[2], turned[1]]
 
     positions = cache_keys.shape[0] * cache_keys.shape[1] * KV_HEADS
-    pair, hidden_state, key_new, value_new = call(
+    pair, hidden_state, key_new, value_new, w_own, w_rest, w_down = call(
         attend_kernel,
         [
             ((2, rows, HALF + TAIL), bf16, vmem), ((rows, D), f32, vmem),
             ((rows, KV_HEADS * HEAD_DIM), bf16, hbm), ((rows, KV_HEADS * HEAD_DIM), bf16, hbm),
+            ((HALF, 2 * hidden_units), bf16, vmem), ((HALF, 2 * hidden_units), bf16, vmem), (exp_down.shape, bf16, vmem),
         ],
         [
-            lengths, routes.T, route_weights.T, tokens, mix_lambda, head_gain.reshape(1, HEAD_DIM),
+            ids, lengths, routes.T, route_weights.T, tokens, mix_lambda, head_gain.reshape(1, HEAD_DIM),
             attn_gain.reshape(1, D), ffn_gain.reshape(1, D), query_w, key_w, value_w,
-            cache_keys.reshape(positions, HEAD_DIM), cache_values.reshape(positions, HEAD_DIM), out_w,
+            cache_keys.reshape(positions, HEAD_DIM), cache_values.reshape(positions, HEAD_DIM), out_w, exp_gate, exp_up, exp_down,
         ],
         [
             pltpu.VMEM(query_w.shape, bf16), pltpu.VMEM(key_w.shape, bf16), pltpu.VMEM(value_w.shape, bf16),
             pltpu.VMEM((positions, HEAD_DIM), bf16), pltpu.VMEM((positions, HEAD_DIM), bf16), pltpu.VMEM(out_w.shape, bf16),
-            pltpu.SemaphoreType.DMA((28,)), pltpu.VMEM((32, HEAD_DIM), f32), pltpu.VMEM((rows, HEADS * HEAD_DIM), f32),
+            pltpu.SemaphoreType.DMA((33,)), pltpu.VMEM((32, HEAD_DIM), f32), pltpu.VMEM((rows, HEADS * HEAD_DIM), f32),
             pltpu.SMEM((rows,), jnp.int32), pltpu.SMEM((2, rows), jnp.int32), pltpu.SMEM((2, rows), f32), pltpu.VMEM((rows, D), bf16),
             pltpu.SMEM((HEADS,), f32), pltpu.VMEM((1, HEAD_DIM), f32), pltpu.VMEM((1, D), f32), pltpu.VMEM((1, D), f32),
             pltpu.VMEM((rows, KV_HEADS * HEAD_DIM), bf16), pltpu.VMEM((rows, KV_HEADS * HEAD_DIM), bf16),
         ],
-        {k: hbm for k in range(14)},
+        {0: smem, **{k: hbm for k in range(1, 18)}},
     )
     outgoing = jnp.broadcast_to(pair[None], (64, 2, rows, HALF + TAIL)).reshape(DEVICES, rows, HALF + TAIL)
     crossed = lax.ppermute(jnp.stack([x[PIECE:] for x in pieces]), "ep", [(i, i ^ 16) for i in range(DEVICES)])
     own = lax.all_to_all(outgoing, "ep", 0, 0, tiled=True)
     theirs = to_partner(own)
-    hidden_units = exp_gate.shape[1]
-    sums, both, near, w_rest, w_out = call(
+    sums, both, near, w_out = call(
         near_kernel,
         [
             ((512, 2 * hidden_units), f32, vmem), ((512, 256), f32, vmem), ((8, 256, 256), bf16, vmem),
-            ((HALF, 2 * hidden_units), bf16, vmem), ((hidden_units + 128, D), bf16, vmem),
+            ((hidden_units + 128, D), bf16, vmem),
         ],
-        [ids, own, *pieces, crossed, branch_gate.reshape(1, D), exp_gate, exp_up, exp_down],
-        [pltpu.VMEM((HALF, 2 * hidden_units), bf16), pltpu.SemaphoreType.DMA((5,))],
-        {0: smem, 8: hbm, 9: hbm, 10: hbm},
+        [ids, own, *pieces, crossed, branch_gate.reshape(1, D), w_own, w_down],
+        [pltpu.SemaphoreType.DMA],
+        {0: smem},
     )
     y_other, acts = call(
         rest_kernel,

time: 91.1 us -> 93.6 us (1.027)
  local copies, waits for them, and re-layouts: 1.37 us -> 5.1 us
    unnamed x2 -> x10, local copies, waits for them, and re-layouts: 0.01 us -> 3.73 us
  transfers between devices with their start and end apart: 7 -> 7, of which waited for: 4 -> 4; matrix products, arithmetic and copies ran while one was open for 0% -> 0% of each run, Pallas kernels for 8% -> 6%
where the time goes in v5:
time: 93.6 us; the launch traced here: 93.3 us
  waiting for transfers between devices  26 us (28%)
  blocking collectives  24.4 us (26%)
  starting transfers between devices  19.5 us (21%)
  Pallas kernels  17.4 us (19%)
  local copies, waits for them, and re-layouts  5.1 us (5%)
    all_to_all x1, blocking collectives, per_device(): parts = lax.all_to_all(joined, 'ep', 0, 0, tiled=True)  24.4 us
    pallas_call x7, Pallas kernels, call(): pl.pallas_call(kernel, in_specs=[pl.BlockSpec(memory_space=spaces.get(k,...  17.4 us
    all_to_all x1, waiting for transfers between devices, per_device(): own = lax.all_to_all(outgoing, 'ep', 0, 0, tiled=True)  14 us
    all_to_all x1, starting transfers between devices, per_device(): own = lax.all_to_all(outgoing, 'ep', 0, 0, tiled=True)  11.5 us
    ppermute x1, waiting for transfers between devices, per_device(): lax.ppermute(jnp.stack([x[PIECE:] for x in pieces]), 'ep', [(i, i ^ 16) f...  8.22 us
    ppermute x3, starting transfers between devices, per_device(): lax.ppermute(pieces[k], 'ep', [(i, (i + 32 * k) % DEVICES) for i in range...  4.19 us
    unnamed x10, local copies, waits for them, and re-layouts  3.73 us
    ppermute x3, waiting for transfers between devices, per_device(): lax.ppermute(pieces[k], 'ep', [(i, (i + 32 * k) % DEVICES) for i in range...  2.67 us
  transfers between devices with their start and end apart: 7, of which 4 were waited for; matrix products, arithmetic and copies ran while one was open for 0% of the time, Pallas kernels for 6%

profile of v5, /device:TPU:1, one launch (start us, length us, event | category | flops | bytes accessed | tf_op | source)
XLA Modules:
  0.0 93.3 jit_solution(2065667637179987811)
XLA Ops:
  0.7 0.1 pad_add_fusion.ids
  0.7 8.3 %shard_map.220 = (bf16[2,4,1152]{2,1,0:T(4,128)(2,1)S(1)}, f32[4,2048]{1,0:T(4,128)S(1)}, bf16[4,256]{1,0:T(4,128)(2,1)}, bf16[4,256]{1,0:T(4,128)(2,1)}, bf16[1...) custom-call(s32[4]{0:T(128)S(1)} %pad_add_fusion.ids, s32[4]{0:T(128)} %lengths_hbm.1, ...), custom_call_target="tpu_custom_call" | custom-call | tf_op jit(solution)/shard_map/pallas_call | solution.py:248
  9.1 0.0 copy-start
  9.1 1.2 %copy-done = bf16[384,2048]{1,0:T(8,128)(2,1)} copy-done((bf16[384,2048]{1,0:T(8,128)(2,1)}, bf16[384,2048]{1,0:T(8,128)(2,1)S(1)}, u32[]{:S(2)}) %copy-start) | copy-done | bytes 1572888
  10.2 0.0 copy-start.2
  10.2 1.1 %copy-done.2 = bf16[1024,768]{1,0:T(8,128)(2,1)} copy-done((bf16[1024,768]{1,0:T(8,128)(2,1)}, bf16[1024,768]{1,0:T(8,128)(2,1)S(1)}, u32[]{:S(2)}) %copy-start.2) | copy-done | bytes 1572888
  11.4 1.3 %broadcast_in_dim.2 = bf16[64,2,4,1152]{3,2,1,0:T(4,128)(2,1)} broadcast(bf16[2,4,1152]{2,1,0:T(4,128)(2,1)S(1)} %get-tuple-element.21), dimensions={1,2,3} | broadcast | bytes 1198080 | tf_op jit(solution)/shard_map/broadcast_in_dim | solution.py:302
  12.7 0.0 copy-start.4
  12.7 11.5 %all-to-all-start = ((bf16[128,4,1152]{2,1,0:T(4,128)(2,1)}), bf16[128,4,1152]{2,1,0:T(4,128)(2,1)S(1)}, u32[]{:S(2)}, u32[]{:S(2)}) async-start(bf16[128,4,1152]{2,1,0:T(4,128)(2,1)} %bitcast.27), calls=%async_computation | async-start | bytes 2359296 | tf_op jit(solution)/shard_map/all_to_all | solution.py:304
  24.2 2.4 %shard_map.221 = (bf16[288,256]{1,0:T(8,128)(2,1)S(1)}, bf16[288,256]{1,0:T(8,128)(2,1)S(1)}, bf16[288,256]{1,0:T(8,128)(2,1)}, bf16[288,256]{1,0:T(8,128)(2,1)}) custom-call(s32[4]{0:T(128)S(1)} %pad_add_fusion.ids, bf16[352,256]{1,0:T(8,128)(2,1)} %bitcast.30, bf16[352,256]{1,0:T(8,128)(2,1)} %bitcast.31, bf16[352,256]{1,0:T(8,128)(2,1)} %bitcast.32), custom_call_target="tpu_custom_call" | custom-call | tf_op jit(solution)/shard_map/pallas_call | solution.py:248
  26.6 3.3 %collective-permute-start.3 = (bf16[288,256]{1,0:T(8,128)(2,1)}, bf16[288,256]{1,0:T(8,128)(2,1)S(1)}, u32[]{:S(2)}, u32[]{:S(2)}) collective-permute-start(bf16[288,256]{1,0:T(8,128)(2,1)} %get-tuple-element.25), channel_id=1, source_target_pairs={{0,96},{1,97},{2,98},{3,99},{4,100},{5,101},{6,102},{7,103},{8,104... | collective-permute-start | bytes 442376 | tf_op jit(solution)/shard_map/ppermute | solution.py:276
  29.9 0.1 collective-permute-start.2
  30.0 0.8 collective-permute-start.1
  30.8 14.0 %all-to-all-done.own = bf16[128,4,1152]{2,1,0:T(4,128)(2,1)S(1)} async-done(((bf16[128,4,1152]{2,1,0:T(4,128)(2,1)}), bf16[128,4,1152]{2,1,0:T(4,128)(2,1)S(1)}, u32[]{:S(2)}, u32[]{:S(2)}) %all-to-all-start) | async-done | bytes 1179680 | tf_op jit(solution)/shard_map/all_to_all | solution.py:304
  44.9 1.0 %collective-permute-start = (bf16[128,4,1152]{2,1,0:T(4,128)(2,1)S(1)}, bf16[128,4,1152]{2,1,0:T(4,128)(2,1)S(1)}, u32[]{:S(2)}, u32[]{:S(2)}) collective-permute-start(bf16[128,4,1152]{2,1,0:T(4,128)(2,1)S(1)} %all-to-all-done.own), channel_id=1, source_target_pairs={{0,1},{1,0},{2,3},{3,2},{4,5},{5,4},{6,7},{7,6},{8,9},{9,8},{10,11... | collective-permute-start | bytes 3538952 | tf_op jit(solution)/shard_map/ppermute | solution.py:23
  45.8 0.0 collective-permute-done.3.fourth
  45.9 0.0 collective-permute-done.2.third
  45.9 2.7 %collective-permute-done.1.second = bf16[288,256]{1,0:T(8,128)(2,1)S(1)} collective-permute-done((bf16[288,256]{1,0:T(8,128)(2,1)S(1)}, bf16[288,256]{1,0:T(8,128)(2,1)S(1)}, u32[]{:S(2)}, u32[]{:S(2)}) %collective-permute-start.1) | collective-permute-done | bytes 147488 | tf_op jit(solution)/shard_map/ppermute | solution.py:276
  48.6 1.5 %collective-permute-start.4 = (bf16[4,144,256]{2,1,0:T(8,128)(2,1)S(1)}, bf16[4,144,256]{2,1,0:T(8,128)(2,1)S(1)}, u32[]{:S(2)}, u32[]{:S(2)}) collective-permute-start(bf16[4,144,256]{2,1,0:T(8,128)(2,1)S(1)} %pad_maximum_fusion), channel_id=1, source_target_pairs={{0,16},{1,17},{2,18},{3,19},{4,20},{5,21},{6,22},{7,23},{8,24},{9,... | collective-permute-start | bytes 884744 | tf_op jit(solution)/shard_map/ppermute | solution.py:303
  50.1 0.0 copy-done.4
  50.1 8.2 %collective-permute-done.4.crossed = bf16[4,144,256]{2,1,0:T(8,128)(2,1)S(1)} collective-permute-done((bf16[4,144,256]{2,1,0:T(8,128)(2,1)S(1)}, bf16[4,144,256]{2,1,0:T(8,128)(2,1)S(1)}, u32[]{:S(2)}, u32[]{:S(2)}) %collective-permute-start.4) | collective-permute-done | bytes 294944 | tf_op jit(solution)/shard_map/ppermute | solution.py:303
  58.4 0.0 copy-start.1
  58.4 1.4 %copy-done.1 = bf16[384,2048]{1,0:T(8,128)(2,1)S(1)} copy-done((bf16[384,2048]{1,0:T(8,128)(2,1)S(1)}, bf16[384,2048]{1,0:T(8,128)(2,1)}, u32[]{:S(2)}) %copy-start.1) | copy-done | bytes 1572888
  59.8 0.0 copy-start.3
  59.8 2.1 %shard_map.222 = (f32[512,768]{1,0:T(8,128)S(1)}, f32[512,256]{1,0:T(8,128)S(1)}, bf16[8,256,256]{2,1,0:T(8,128)(2,1)S(1)}, bf16[512,2048]{1,0:T(8,128)(2,1)S(1)}) custom-call(s32[4]{0:T(128)S(1)} %pad_add_fusion.ids, bf16[128,4,1152]{2,1,0:T(4,128)(2,1)S(1)} %all-to-all-done.own, bf16[288,256]{1,0:T(8,128)(2,1)S(1)} %get-tuple-element.22.first, ...), custom_call_target="tpu_custom_call" | custom-call | tf_op jit(solution)/shard_map/pallas_call | solution.py:248
  61.8 0.0 collective-permute-done.theirs
  61.8 0.0 copy-done.3
  61.9 2.4 %shard_map.223 = (bf16[512,1024]{1,0:T(8,128)(2,1)S(1)}, bf16[512,512]{1,0:T(8,128)(2,1)S(1)}) custom-call(s32[4]{0:T(128)S(1)} %pad_add_fusion.ids, bf16[128,4,1152]{2,1,0:T(4,128)(2,1)S(1)} %collective-permute-done.theirs, f32[512,768]{1,0:T(8,128)S(1)} %get-tuple-element.28.sums_near, f32[512,256]{1,0:T(8,128)S(1)} %get-tuple-element.29.both_near, ...), custom_call_target="tpu_custom_call" | custom-call | tf_op jit(solution)/shard_map/pallas_call | solution.py:248
  64.2 1.3 %collective-permute-start.5 = (bf16[512,1024]{1,0:T(8,128)(2,1)S(1)}, bf16[512,1024]{1,0:T(8,128)(2,1)S(1)}, u32[]{:S(2)}, u32[]{:S(2)}) collective-permute-start(bf16[512,1024]{1,0:T(8,128)(2,1)S(1)} %get-tuple-element.34), channel_id=1, source_target_pairs={{0,1},{1,0},{2,3},{3,2},{4,5},{5,4},{6,7},{7,6},{8,9},{9,8},{10,11... | collective-permute-start | bytes 3145736 | tf_op jit(solution)/shard_map/ppermute | solution.py:23
  65.6 1.3 %shard_map.224.y_own = f32[512,1024]{1,0:T(8,128)S(1)} custom-call(s32[4]{0:T(128)S(1)} %pad_add_fusion.ids, bf16[512,512]{1,0:T(8,128)(2,1)S(1)} %get-tuple-element.33.acts, bf16[512,2048]{1,0:T(8,128)(2,1)S(1)} %get-tuple-element.32.w_out), custom_call_target="tpu_custom_call" | custom-call | tf_op jit(solution)/shard_map/pallas_call | solution.py:248
  66.8 1.0 %collective-permute-done.5.y_recv = bf16[512,1024]{1,0:T(8,128)(2,1)S(1)} collective-permute-done((bf16[512,1024]{1,0:T(8,128)(2,1)S(1)}, bf16[512,1024]{1,0:T(8,128)(2,1)S(1)}, u32[]{:S(2)}, u32[]{:S(2)}) %collective-permute-start.5) | collective-permute-done | bytes 1048608 | tf_op jit(solution)/shard_map/ppermute | solution.py:23
  67.9 0.2 shard_map.225
  68.1 24.4 %all_to_all.10.parts = bf16[128,4,1024]{2,1,0:T(4,128)(2,1)S(1)} all-to-all(bf16[128,4,1024]{2,1,0:T(4,128)(2,1)S(1)} %shard_map.225), channel_id=1, replica_groups=mesh['ep'=128] {'ep'}, dimensions={0} | all-to-all | bytes 2097152 | tf_op jit(solution)/shard_map/all_to_all | solution.py:326
  92.5 0.8 shard_map.226
  (6 shorter events, 0.1 us)
Async XLA Ops:
  9.1 1.2 %copy-start = (bf16[384,2048]{1,0:T(8,128)(2,1)}, bf16[384,2048]{1,0:T(8,128)(2,1)S(1)}, u32[]{:S(2)}) copy-start(bf16[384,2048]{1,0:T(8,128)(2,1)S(1)} %get-tuple-element.27.w_down) | copy-start | bytes 4718596
  10.2 1.1 %copy-start.2 = (bf16[1024,768]{1,0:T(8,128)(2,1)}, bf16[1024,768]{1,0:T(8,128)(2,1)S(1)}, u32[]{:S(2)}) copy-start(bf16[1024,768]{1,0:T(8,128)(2,1)S(1)} %get-tuple-element.31.w_rest) | copy-start | bytes 4718596
  12.7 37.4 %copy-start.4 = (bf16[2048]{0:T(1024)(128)(2,1)S(1)}, bf16[2048]{0:T(1024)(128)(2,1)}, u32[]{:S(2)}) copy-start(bf16[2048]{0:T(1024)(128)(2,1)} %param.41) | copy-start | bytes 12292
  12.7 32.1 %all-to-all-start = ((bf16[128,4,1152]{2,1,0:T(4,128)(2,1)}), bf16[128,4,1152]{2,1,0:T(4,128)(2,1)S(1)}, u32[]{:S(2)}, u32[]{:S(2)}) async-start(bf16[128,4,1152]{2,1,0:T(4,128)(2,1)} %bitcast.27), calls=%async_computation | async-start | bytes 2359296 | tf_op jit(solution)/shard_map/all_to_all | solution.py:304
  26.6 19.2 %collective-permute-start.3 = (bf16[288,256]{1,0:T(8,128)(2,1)}, bf16[288,256]{1,0:T(8,128)(2,1)S(1)}, u32[]{:S(2)}, u32[]{:S(2)}) collective-permute-start(bf16[288,256]{1,0:T(8,128)(2,1)} %get-tuple-element.25), channel_id=1, source_target_pairs={{0,96},{1,97},{2,98},{3,99},{4,100},{5,101},{6,102},{7,103},{8,104... | collective-permute-start | bytes 442376 | tf_op jit(solution)/shard_map/ppermute | solution.py:276
  29.9 15.9 %collective-permute-start.2 = (bf16[288,256]{1,0:T(8,128)(2,1)}, bf16[288,256]{1,0:T(8,128)(2,1)S(1)}, u32[]{:S(2)}, u32[]{:S(2)}) collective-permute-start(bf16[288,256]{1,0:T(8,128)(2,1)} %get-tuple-element.24), channel_id=1, source_target_pairs={{0,64},{1,65},{2,66},{3,67},{4,68},{5,69},{6,70},{7,71},{8,72},{9,... | collective-permute-start | bytes 442376 | tf_op jit(solution)/shard_map/ppermute | solution.py:276
  30.0 18.5 %collective-permute-start.1 = (bf16[288,256]{1,0:T(8,128)(2,1)S(1)}, bf16[288,256]{1,0:T(8,128)(2,1)S(1)}, u32[]{:S(2)}, u32[]{:S(2)}) collective-permute-start(bf16[288,256]{1,0:T(8,128)(2,1)S(1)} %get-tuple-element.23), channel_id=1, source_target_pairs={{0,32},{1,33},{2,34},{3,35},{4,36},{5,37},{6,38},{7,39},{8,40},{9,... | collective-permute-start | bytes 442376 | tf_op jit(solution)/shard_map/ppermute | solution.py:276
  44.9 17.0 %collective-permute-start = (bf16[128,4,1152]{2,1,0:T(4,128)(2,1)S(1)}, bf16[128,4,1152]{2,1,0:T(4,128)(2,1)S(1)}, u32[]{:S(2)}, u32[]{:S(2)}) collective-permute-start(bf16[128,4,1152]{2,1,0:T(4,128)(2,1)S(1)} %all-to-all-done.own), channel_id=1, source_target_pairs={{0,1},{1,0},{2,3},{3,2},{4,5},{5,4},{6,7},{7,6},{8,9},{9,8},{10,11... | collective-permute-start | bytes 3538952 | tf_op jit(solution)/shard_map/ppermute | solution.py:23
  48.6 9.8 %collective-permute-start.4 = (bf16[4,144,256]{2,1,0:T(8,128)(2,1)S(1)}, bf16[4,144,256]{2,1,0:T(8,128)(2,1)S(1)}, u32[]{:S(2)}, u32[]{:S(2)}) collective-permute-start(bf16[4,144,256]{2,1,0:T(8,128)(2,1)S(1)} %pad_maximum_fusion), channel_id=1, source_target_pairs={{0,16},{1,17},{2,18},{3,19},{4,20},{5,21},{6,22},{7,23},{8,24},{9,... | collective-permute-start | bytes 884744 | tf_op jit(solution)/shard_map/ppermute | solution.py:303
  58.4 1.4 %copy-start.1 = (bf16[384,2048]{1,0:T(8,128)(2,1)S(1)}, bf16[384,2048]{1,0:T(8,128)(2,1)}, u32[]{:S(2)}) copy-start(bf16[384,2048]{1,0:T(8,128)(2,1)} %copy-done) | copy-start | bytes 4718596
  59.8 2.1 %copy-start.3 = (bf16[1024,768]{1,0:T(8,128)(2,1)S(1)}, bf16[1024,768]{1,0:T(8,128)(2,1)}, u32[]{:S(2)}) copy-start(bf16[1024,768]{1,0:T(8,128)(2,1)} %copy-done.2) | copy-start | bytes 4718596
  64.2 3.6 %collective-permute-start.5 = (bf16[512,1024]{1,0:T(8,128)(2,1)S(1)}, bf16[512,1024]{1,0:T(8,128)(2,1)S(1)}, u32[]{:S(2)}, u32[]{:S(2)}) collective-permute-start(bf16[512,1024]{1,0:T(8,128)(2,1)S(1)} %get-tuple-element.34), channel_id=1, source_target_pairs={{0,1},{1,0},{2,3},{3,2},{4,5},{5,4},{6,7},{7,6},{8,9},{9,8},{10,11... | collective-permute-start | bytes 3145736 | tf_op jit(solution)/shard_map/ppermute | solution.py:23

commit v6 on v5

--- a/solution.py
+++ b/solution.py
@@ -35,8 +35,8 @@
 def attend_kernel(
     ids, lengths_hbm, routes_hbm, route_weights_hbm, tokens_hbm, mix_hbm, head_gain_hbm, attn_gain_hbm, ffn_gain_hbm,
     query_hbm, key_hbm, value_hbm, cache_keys, cache_values, out_hbm,
-    gate_hbm, up_hbm, down_hbm,
-    pair, hidden, key_out, value_out, w_own, w_rest, w_down,
+    gate_hbm, up_hbm,
+    pair, hidden, key_out, value_out, w_own, w_rest,
     query_w, key_w, value_w, keys, values, out_w, sem, query_rows, head_rows,
     lengths, routes, route_weights, tokens, mix_lambda, head_gain, attn_gain, ffn_gain, key_new, value_new,
 ):
@@ -64,7 +64,7 @@
     on_out = [fetch(out_hbm.at[pl.ds(k * 256, 256), :], out_w.at[pl.ds(k * 256, 256), :]) for k in range(4)]
 
     wide = gate_hbm.shape[1]
-    ahead = [fetch(down_hbm, w_down)]
+    ahead = []
     for half, target in ((ids[0], w_own), (1 - ids[0], w_rest)):
         rows = pl.ds(pl.multiple_of(half * HALF, HALF), HALF)
         ahead.append(fetch(gate_hbm.at[rows, :], target.at[:, pl.ds(0, wide)]))
@@ -277,27 +277,27 @@
     pieces = [pieces[0], turned[0], turned[2], turned[1]]
 
     positions = cache_keys.shape[0] * cache_keys.shape[1] * KV_HEADS
-    pair, hidden_state, key_new, value_new, w_own, w_rest, w_down = call(
+    pair, hidden_state, key_new, value_new, w_own, w_rest = call(
         attend_kernel,
         [
             ((2, rows, HALF + TAIL), bf16, vmem), ((rows, D), f32, vmem),
             ((rows, KV_HEADS * HEAD_DIM), bf16, hbm), ((rows, KV_HEADS * HEAD_DIM), bf16, hbm),
-            ((HALF, 2 * hidden_units), bf16, vmem), ((HALF, 2 * hidden_units), bf16, vmem), (exp_down.shape, bf16, vmem),
+            ((HALF, 2 * hidden_units), bf16, vmem), ((HALF, 2 * hidden_units), bf16, vmem),
         ],
         [
             ids, lengths, routes.T, route_weights.T, tokens, mix_lambda, head_gain.reshape(1, HEAD_DIM),
             attn_gain.reshape(1, D), ffn_gain.reshape(1, D), query_w, key_w, value_w,
-            cache_keys.reshape(positions, HEAD_DIM), cache_values.reshape(positions, HEAD_DIM), out_w, exp_gate, exp_up, exp_down,
+            cache_keys.reshape(positions, HEAD_DIM), cache_values.reshape(positions, HEAD_DIM), out_w, exp_gate, exp_up,
         ],
         [
             pltpu.VMEM(query_w.shape, bf16), pltpu.VMEM(key_w.shape, bf16), pltpu.VMEM(value_w.shape, bf16),
             pltpu.VMEM((positions, HEAD_DIM), bf16), pltpu.VMEM((positions, HEAD_DIM), bf16), pltpu.VMEM(out_w.shape, bf16),
-            pltpu.SemaphoreType.DMA((33,)), pltpu.VMEM((32, HEAD_DIM), f32), pltpu.VMEM((rows, HEADS * HEAD_DIM), f32),
+            pltpu.SemaphoreType.DMA((32,)), pltpu.VMEM((32, HEAD_DIM), f32), pltpu.VMEM((rows, HEADS * HEAD_DIM), f32),
             pltpu.SMEM((rows,), jnp.int32), pltpu.SMEM((2, rows), jnp.int32), pltpu.SMEM((2, rows), f32), pltpu.VMEM((rows, D), bf16),
             pltpu.SMEM((HEADS,), f32), pltpu.VMEM((1, HEAD_DIM), f32), pltpu.VMEM((1, D), f32), pltpu.VMEM((1, D), f32),
             pltpu.VMEM((rows, KV_HEADS * HEAD_DIM), bf16), pltpu.VMEM((rows, KV_HEADS * HEAD_DIM), bf16),
         ],
-        {0: smem, **{k: hbm for k in range(1, 18)}},
+        {0: smem, **{k: hbm for k in range(1, 17)}},
     )
     outgoing = jnp.broadcast_to(pair[None], (64, 2, rows, HALF + TAIL)).reshape(DEVICES, rows, HALF + TAIL)
     crossed = lax.ppermute(jnp.stack([x[PIECE:] for x in pieces]), "ep", [(i, i ^ 16) for i in range(DEVICES)])
@@ -309,9 +309,9 @@
             ((512, 2 * hidden_units), f32, vmem), ((512, 256), f32, vmem), ((8, 256, 256), bf16, vmem),
             ((hidden_units + 128, D), bf16, vmem),
         ],
-        [ids, own, *pieces, crossed, branch_gate.reshape(1, D), w_own, w_down],
+        [ids, own, *pieces, crossed, branch_gate.reshape(1, D), w_own, exp_down],
         [pltpu.SemaphoreType.DMA],
-        {0: smem},
+        {0: smem, 9: hbm},
     )
     y_other, acts = call(
         rest_kernel,

time: 93.6 us -> 92.2 us (0.985)
  local copies, waits for them, and re-layouts: 5.1 us -> 2.52 us
  Pallas kernels: 17.4 us -> 18.6 us
    unnamed x10 -> x6, local copies, waits for them, and re-layouts: 3.73 us -> 1.17 us
    pallas_call x7, Pallas kernels: 17.4 us -> 18.6 us  [call(): pl.pallas_call(kernel, in_specs=[pl.BlockSpec(memory_space=spaces.get(k,...]
  transfers between devices with their start and end apart: 7 -> 7, of which waited for: 4 -> 4; matrix products, arithmetic and copies ran while one was open for 0% -> 0% of each run, Pallas kernels for 6% -> 7%
where the time goes in v6:
time: 92.2 us; the launch traced here: 91.9 us
  waiting for transfers between devices  26 us (28%)
  blocking collectives  24.4 us (26%)
  starting transfers between devices  19.5 us (21%)
  Pallas kernels  18.6 us (20%)
  local copies, waits for them, and re-layouts  2.52 us (3%)
    all_to_all x1, blocking collectives, per_device(): parts = lax.all_to_all(joined, 'ep', 0, 0, tiled=True)  24.4 us
    pallas_call x7, Pallas kernels, call(): pl.pallas_call(kernel, in_specs=[pl.BlockSpec(memory_space=spaces.get(k,...  18.6 us
    all_to_all x1, waiting for transfers between devices, per_device(): own = lax.all_to_all(outgoing, 'ep', 0, 0, tiled=True)  14 us
    all_to_all x1, starting transfers between devices, per_device(): own = lax.all_to_all(outgoing, 'ep', 0, 0, tiled=True)  11.5 us
    ppermute x1, waiting for transfers between devices, per_device(): lax.ppermute(jnp.stack([x[PIECE:] for x in pieces]), 'ep', [(i, i ^ 16) f...  8.22 us
    ppermute x3, starting transfers between devices, per_device(): lax.ppermute(pieces[k], 'ep', [(i, (i + 32 * k) % DEVICES) for i in range...  4.19 us
    ppermute x3, waiting for transfers between devices, per_device(): lax.ppermute(pieces[k], 'ep', [(i, (i + 32 * k) % DEVICES) for i in range...  2.67 us
    ppermute x2, starting transfers between devices, to_partner(): return lax.ppermute(x, 'ep', [(i, i ^ 1) for i in range(DEVICES)])  2.31 us
  transfers between devices with their start and end apart: 7, of which 4 were waited for; matrix products, arithmetic and copies ran while one was open for 0% of the time, Pallas kernels for 7%

profile of v6, /device:TPU:1, one launch (start us, length us, event | category | flops | bytes accessed | tf_op | source)
XLA Modules:
  0.0 91.9 jit_solution(5482252006703014198)
XLA Ops:
  0.7 0.1 pad_add_fusion.ids
  0.7 8.3 %shard_map.220 = (bf16[2,4,1152]{2,1,0:T(4,128)(2,1)S(1)}, f32[4,2048]{1,0:T(4,128)S(1)}, bf16[4,256]{1,0:T(4,128)(2,1)}, bf16[4,256]{1,0:T(4,128)(2,1)}, bf16[1...) custom-call(s32[4]{0:T(128)S(1)} %pad_add_fusion.ids, s32[4]{0:T(128)} %lengths_hbm.1, s32[2,4]{1,0:T(2,128)} %bitcast.35, ...), custom_call_target="tpu_custom_call" | custom-call | tf_op jit(solution)/shard_map/pallas_call | solution.py:248
  9.1 0.0 copy-start
  9.1 1.2 %copy-done = bf16[1024,768]{1,0:T(8,128)(2,1)} copy-done((bf16[1024,768]{1,0:T(8,128)(2,1)}, bf16[1024,768]{1,0:T(8,128)(2,1)S(1)}, u32[]{:S(2)}) %copy-start) | copy-done | bytes 1572888
  10.2 1.3 %broadcast_in_dim.2 = bf16[64,2,4,1152]{3,2,1,0:T(4,128)(2,1)} broadcast(bf16[2,4,1152]{2,1,0:T(4,128)(2,1)S(1)} %get-tuple-element.20), dimensions={1,2,3} | broadcast | bytes 1198080 | tf_op jit(solution)/shard_map/broadcast_in_dim | solution.py:302
  11.5 0.0 copy-start.2
  11.5 11.5 %all-to-all-start = ((bf16[128,4,1152]{2,1,0:T(4,128)(2,1)}), bf16[128,4,1152]{2,1,0:T(4,128)(2,1)S(1)}, u32[]{:S(2)}, u32[]{:S(2)}) async-start(bf16[128,4,1152]{2,1,0:T(4,128)(2,1)} %bitcast.27), calls=%async_computation | async-start | bytes 2359296 | tf_op jit(solution)/shard_map/all_to_all | solution.py:304
  23.0 2.4 %shard_map.221 = (bf16[288,256]{1,0:T(8,128)(2,1)S(1)}, bf16[288,256]{1,0:T(8,128)(2,1)S(1)}, bf16[288,256]{1,0:T(8,128)(2,1)}, bf16[288,256]{1,0:T(8,128)(2,1)}) custom-call(s32[4]{0:T(128)S(1)} %pad_add_fusion.ids, bf16[352,256]{1,0:T(8,128)(2,1)} %bitcast.30, bf16[352,256]{1,0:T(8,128)(2,1)} %bitcast.31, bf16[352,256]{1,0:T(8,128)(2,1)} %bitcast.32), custom_call_target="tpu_custom_call" | custom-call | tf_op jit(solution)/shard_map/pallas_call | solution.py:248
  25.4 3.3 %collective-permute-start.3 = (bf16[288,256]{1,0:T(8,128)(2,1)}, bf16[288,256]{1,0:T(8,128)(2,1)S(1)}, u32[]{:S(2)}, u32[]{:S(2)}) collective-permute-start(bf16[288,256]{1,0:T(8,128)(2,1)} %get-tuple-element.24), channel_id=1, source_target_pairs={{0,96},{1,97},{2,98},{3,99},{4,100},{5,101},{6,102},{7,103},{8,104... | collective-permute-start | bytes 442376 | tf_op jit(solution)/shard_map/ppermute | solution.py:276
  28.7 0.1 collective-permute-start.2
  28.9 0.8 collective-permute-start.1
  29.6 14.0 %all-to-all-done.own = bf16[128,4,1152]{2,1,0:T(4,128)(2,1)S(1)} async-done(((bf16[128,4,1152]{2,1,0:T(4,128)(2,1)}), bf16[128,4,1152]{2,1,0:T(4,128)(2,1)S(1)}, u32[]{:S(2)}, u32[]{:S(2)}) %all-to-all-start) | async-done | bytes 1179680 | tf_op jit(solution)/shard_map/all_to_all | solution.py:304
  43.7 1.0 %collective-permute-start = (bf16[128,4,1152]{2,1,0:T(4,128)(2,1)S(1)}, bf16[128,4,1152]{2,1,0:T(4,128)(2,1)S(1)}, u32[]{:S(2)}, u32[]{:S(2)}) collective-permute-start(bf16[128,4,1152]{2,1,0:T(4,128)(2,1)S(1)} %all-to-all-done.own), channel_id=1, source_target_pairs={{0,1},{1,0},{2,3},{3,2},{4,5},{5,4},{6,7},{7,6},{8,9},{9,8},{10,11... | collective-permute-start | bytes 3538952 | tf_op jit(solution)/shard_map/ppermute | solution.py:23
  44.7 0.0 collective-permute-done.3.fourth
  44.7 0.0 collective-permute-done.2.third
  44.7 2.7 %collective-permute-done.1.second = bf16[288,256]{1,0:T(8,128)(2,1)S(1)} collective-permute-done((bf16[288,256]{1,0:T(8,128)(2,1)S(1)}, bf16[288,256]{1,0:T(8,128)(2,1)S(1)}, u32[]{:S(2)}, u32[]{:S(2)}) %collective-permute-start.1) | collective-permute-done | bytes 147488 | tf_op jit(solution)/shard_map/ppermute | solution.py:276
  47.4 1.5 %collective-permute-start.4 = (bf16[4,144,256]{2,1,0:T(8,128)(2,1)S(1)}, bf16[4,144,256]{2,1,0:T(8,128)(2,1)S(1)}, u32[]{:S(2)}, u32[]{:S(2)}) collective-permute-start(bf16[4,144,256]{2,1,0:T(8,128)(2,1)S(1)} %pad_maximum_fusion), channel_id=1, source_target_pairs={{0,16},{1,17},{2,18},{3,19},{4,20},{5,21},{6,22},{7,23},{8,24},{9,... | collective-permute-start | bytes 884744 | tf_op jit(solution)/shard_map/ppermute | solution.py:303
  48.9 0.0 copy-done.2
  48.9 8.2 %collective-permute-done.4.crossed = bf16[4,144,256]{2,1,0:T(8,128)(2,1)S(1)} collective-permute-done((bf16[4,144,256]{2,1,0:T(8,128)(2,1)S(1)}, bf16[4,144,256]{2,1,0:T(8,128)(2,1)S(1)}, u32[]{:S(2)}, u32[]{:S(2)}) %collective-permute-start.4) | collective-permute-done | bytes 294944 | tf_op jit(solution)/shard_map/ppermute | solution.py:303
  57.2 0.0 copy-start.1
  57.2 3.2 %shard_map.222 = (f32[512,768]{1,0:T(8,128)S(1)}, f32[512,256]{1,0:T(8,128)S(1)}, bf16[8,256,256]{2,1,0:T(8,128)(2,1)S(1)}, bf16[512,2048]{1,0:T(8,128)(2,1)S(1)}) custom-call(s32[4]{0:T(128)S(1)} %pad_add_fusion.ids, bf16[128,4,1152]{2,1,0:T(4,128)(2,1)S(1)} %all-to-all-done.own, bf16[288,256]{1,0:T(8,128)(2,1)S(1)} %get-tuple-element.21.first, ...), custom_call_target="tpu_custom_call" | custom-call | tf_op jit(solution)/shard_map/pallas_call | solution.py:248
  60.4 0.0 collective-permute-done.theirs
  60.4 0.0 copy-done.1
  60.4 2.4 %shard_map.223 = (bf16[512,1024]{1,0:T(8,128)(2,1)S(1)}, bf16[512,512]{1,0:T(8,128)(2,1)S(1)}) custom-call(s32[4]{0:T(128)S(1)} %pad_add_fusion.ids, bf16[128,4,1152]{2,1,0:T(4,128)(2,1)S(1)} %collective-permute-done.theirs, f32[512,768]{1,0:T(8,128)S(1)} %get-tuple-element.26.sums_near, f32[512,256]{1,0:T(8,128)S(1)} %get-tuple-element.27.both_near, ...), custom_call_target="tpu_custom_call" | custom-call | tf_op jit(solution)/shard_map/pallas_call | solution.py:248
  62.8 1.3 %collective-permute-start.5 = (bf16[512,1024]{1,0:T(8,128)(2,1)S(1)}, bf16[512,1024]{1,0:T(8,128)(2,1)S(1)}, u32[]{:S(2)}, u32[]{:S(2)}) collective-permute-start(bf16[512,1024]{1,0:T(8,128)(2,1)S(1)} %get-tuple-element.32), channel_id=1, source_target_pairs={{0,1},{1,0},{2,3},{3,2},{4,5},{5,4},{6,7},{7,6},{8,9},{9,8},{10,11... | collective-permute-start | bytes 3145736 | tf_op jit(solution)/shard_map/ppermute | solution.py:23
  64.2 1.3 %shard_map.224.y_own = f32[512,1024]{1,0:T(8,128)S(1)} custom-call(s32[4]{0:T(128)S(1)} %pad_add_fusion.ids, bf16[512,512]{1,0:T(8,128)(2,1)S(1)} %get-tuple-element.31.acts, bf16[512,2048]{1,0:T(8,128)(2,1)S(1)} %get-tuple-element.30.w_out), custom_call_target="tpu_custom_call" | custom-call | tf_op jit(solution)/shard_map/pallas_call | solution.py:248
  65.4 1.0 %collective-permute-done.5.y_recv = bf16[512,1024]{1,0:T(8,128)(2,1)S(1)} collective-permute-done((bf16[512,1024]{1,0:T(8,128)(2,1)S(1)}, bf16[512,1024]{1,0:T(8,128)(2,1)S(1)}, u32[]{:S(2)}, u32[]{:S(2)}) %collective-permute-start.5) | collective-permute-done | bytes 1048608 | tf_op jit(solution)/shard_map/ppermute | solution.py:23
  66.4 0.2 shard_map.225
  66.7 24.4 %all_to_all.10.parts = bf16[128,4,1024]{2,1,0:T(4,128)(2,1)S(1)} all-to-all(bf16[128,4,1024]{2,1,0:T(4,128)(2,1)S(1)} %shard_map.225), channel_id=1, replica_groups=mesh['ep'=128] {'ep'}, dimensions={0} | all-to-all | bytes 2097152 | tf_op jit(solution)/shard_map/all_to_all | solution.py:326
  91.1 0.8 shard_map.226
  (6 shorter events, 0.1 us)
Async XLA Ops:
  9.1 1.2 %copy-start = (bf16[1024,768]{1,0:T(8,128)(2,1)}, bf16[1024,768]{1,0:T(8,128)(2,1)S(1)}, u32[]{:S(2)}) copy-start(bf16[1024,768]{1,0:T(8,128)(2,1)S(1)} %get-tuple-element.29.w_rest) | copy-start | bytes 4718596
  11.5 37.4 %copy-start.2 = (bf16[2048]{0:T(1024)(128)(2,1)S(1)}, bf16[2048]{0:T(1024)(128)(2,1)}, u32[]{:S(2)}) copy-start(bf16[2048]{0:T(1024)(128)(2,1)} %param.41) | copy-start | bytes 12292
  11.5 32.1 %all-to-all-start = ((bf16[128,4,1152]{2,1,0:T(4,128)(2,1)}), bf16[128,4,1152]{2,1,0:T(4,128)(2,1)S(1)}, u32[]{:S(2)}, u32[]{:S(2)}) async-start(bf16[128,4,1152]{2,1,0:T(4,128)(2,1)} %bitcast.27), calls=%async_computation | async-start | bytes 2359296 | tf_op jit(solution)/shard_map/all_to_all | solution.py:304
  25.4 19.2 %collective-permute-start.3 = (bf16[288,256]{1,0:T(8,128)(2,1)}, bf16[288,256]{1,0:T(8,128)(2,1)S(1)}, u32[]{:S(2)}, u32[]{:S(2)}) collective-permute-start(bf16[288,256]{1,0:T(8,128)(2,1)} %get-tuple-element.24), channel_id=1, source_target_pairs={{0,96},{1,97},{2,98},{3,99},{4,100},{5,101},{6,102},{7,103},{8,104... | collective-permute-start | bytes 442376 | tf_op jit(solution)/shard_map/ppermute | solution.py:276
  28.7 15.9 %collective-permute-start.2 = (bf16[288,256]{1,0:T(8,128)(2,1)}, bf16[288,256]{1,0:T(8,128)(2,1)S(1)}, u32[]{:S(2)}, u32[]{:S(2)}) collective-permute-start(bf16[288,256]{1,0:T(8,128)(2,1)} %get-tuple-element.23), channel_id=1, source_target_pairs={{0,64},{1,65},{2,66},{3,67},{4,68},{5,69},{6,70},{7,71},{8,72},{9,... | collective-permute-start | bytes 442376 | tf_op jit(solution)/shard_map/ppermute | solution.py:276
  28.9 18.5 %collective-permute-start.1 = (bf16[288,256]{1,0:T(8,128)(2,1)S(1)}, bf16[288,256]{1,0:T(8,128)(2,1)S(1)}, u32[]{:S(2)}, u32[]{:S(2)}) collective-permute-start(bf16[288,256]{1,0:T(8,128)(2,1)S(1)} %get-tuple-element.22), channel_id=1, source_target_pairs={{0,32},{1,33},{2,34},{3,35},{4,36},{5,37},{6,38},{7,39},{8,40},{9,... | collective-permute-start | bytes 442376 | tf_op jit(solution)/shard_map/ppermute | solution.py:276
  43.7 16.7 %collective-permute-start = (bf16[128,4,1152]{2,1,0:T(4,128)(2,1)S(1)}, bf16[128,4,1152]{2,1,0:T(4,128)(2,1)S(1)}, u32[]{:S(2)}, u32[]{:S(2)}) collective-permute-start(bf16[128,4,1152]{2,1,0:T(4,128)(2,1)S(1)} %all-to-all-done.own), channel_id=1, source_target_pairs={{0,1},{1,0},{2,3},{3,2},{4,5},{5,4},{6,7},{7,6},{8,9},{9,8},{10,11... | collective-permute-start | bytes 3538952 | tf_op jit(solution)/shard_map/ppermute | solution.py:23
  47.4 9.8 %collective-permute-start.4 = (bf16[4,144,256]{2,1,0:T(8,128)(2,1)S(1)}, bf16[4,144,256]{2,1,0:T(8,128)(2,1)S(1)}, u32[]{:S(2)}, u32[]{:S(2)}) collective-permute-start(bf16[4,144,256]{2,1,0:T(8,128)(2,1)S(1)} %pad_maximum_fusion), channel_id=1, source_target_pairs={{0,16},{1,17},{2,18},{3,19},{4,20},{5,21},{6,22},{7,23},{8,24},{9,... | collective-permute-start | bytes 884744 | tf_op jit(solution)/shard_map/ppermute | solution.py:303
  57.2 3.3 %copy-start.1 = (bf16[1024,768]{1,0:T(8,128)(2,1)S(1)}, bf16[1024,768]{1,0:T(8,128)(2,1)}, u32[]{:S(2)}) copy-start(bf16[1024,768]{1,0:T(8,128)(2,1)} %copy-done) | copy-start | bytes 4718596
  62.8 3.6 %collective-permute-start.5 = (bf16[512,1024]{1,0:T(8,128)(2,1)S(1)}, bf16[512,1024]{1,0:T(8,128)(2,1)S(1)}, u32[]{:S(2)}, u32[]{:S(2)}) collective-permute-start(bf16[512,1024]{1,0:T(8,128)(2,1)S(1)} %get-tuple-element.32), channel_id=1, source_target_pairs={{0,1},{1,0},{2,3},{3,2},{4,5},{5,4},{6,7},{7,6},{8,9},{9,8},{10,11... | collective-permute-start | bytes 3145736 | tf_op jit(solution)/shard_map/ppermute | solution.py:23

commit v7 on v5

--- a/solution.py
+++ b/solution.py
@@ -206,7 +206,7 @@
     copy.wait()
 
 
-def rest_kernel(ids, theirs, sums_near, both_near, near, w_rest, w_out, y_other, acts):
+def rest_kernel(ids, theirs, sums_near, both_near, near, w_rest, w_out, y_first, y_second, acts):
     core, expert = ids[0], ids[1]
     x = theirs[:, :, 0:HALF].reshape(512, HALF)
     both = dense_sums(x, near, (1 - core) * 4) + both_near[...]
@@ -222,15 +222,20 @@
     acts[:, 0:wide] = (weight * (gate_sum * jax.nn.sigmoid(gate_sum) * up_sum)).astype(bf16)
     acts[:, wide:] = jnp.where(lane < UNITS, dense_act, 0.0).astype(bf16)
     columns = pl.ds(pl.multiple_of((1 - core) * HALF, HALF), HALF)
-    y_other[...] = dot(acts[...], w_out[:, columns]).astype(bf16)
+    total = dot(acts[...], w_out[:, columns]).astype(bf16)
+    y_first[...] = total[:, 0 : HALF // 2]
+    y_second[...] = total[:, HALF // 2 :]
 
 
 def own_kernel(ids, acts, w_out, y_own):
     y_own[...] = dot(acts[...], w_out[:, pl.ds(pl.multiple_of(ids[0] * HALF, HALF), HALF)])
 
 
-def join_kernel(y_own, y_recv, out):
-    out[...] = (y_own[...] + y_recv[...].astype(f32)).astype(bf16).reshape(128, 4, HALF)
+def join_kernel(y_own, first, second, out):
+    wide = first.shape[1]
+    for k, ref in enumerate((first, second)):
+        columns = slice(k * wide, (k + 1) * wide)
+        out[:, :, columns] = (y_own[:, columns] + ref[...].astype(f32)).astype(bf16).reshape(128, 4, wide)
 
 
 def last_kernel(hidden, parts, out):
@@ -313,16 +318,16 @@
         [pltpu.SemaphoreType.DMA],
         {0: smem},
     )
-    y_other, acts = call(
+    y_first, y_second, acts = call(
         rest_kernel,
-        [((512, HALF), bf16, vmem), ((512, hidden_units + 128), bf16, vmem)],
+        [((512, HALF // 2), bf16, vmem), ((512, HALF // 2), bf16, vmem), ((512, hidden_units + 128), bf16, vmem)],
         [ids, theirs, sums, both, near, w_rest, w_out],
         [],
         {0: smem},
     )
-    y_recv = to_partner(y_other)
+    y_recv = [to_partner(y_first), to_partner(y_second)]
     (y_own,) = call(own_kernel, [((512, HALF), f32, vmem)], [ids, acts, w_out], [], {0: smem})
-    (joined,) = call(join_kernel, [((DEVICES, rows, HALF), bf16, vmem)], [y_own, y_recv])
+    (joined,) = call(join_kernel, [((DEVICES, rows, HALF), bf16, vmem)], [y_own, *y_recv])
     parts = lax.all_to_all(joined, "ep", 0, 0, tiled=True)
     (output,) = call(last_kernel, [((rows, D), bf16, None)], [hidden_state, parts])
     return (output, key_new, value_new)

time: 93.6 us -> 93.6 us (level)
    ppermute x2 -> x3, starting transfers between devices: 2.32 us -> 2.41 us  [to_partner(): return lax.ppermute(x, 'ep', [(i, i ^ 1) for i in range(DEVICES)])]
  transfers between devices with their start and end apart: 7 -> 8, of which waited for: 4 -> 5; matrix products, arithmetic and copies ran while one was open for 0% -> 0% of each run, Pallas kernels for 6% -> 6%
where the time goes in v7:
time: 93.6 us; the launch traced here: 93.3 us
  waiting for transfers between devices  25.9 us (28%)
  blocking collectives  24.4 us (26%)
  starting transfers between devices  19.6 us (21%)
  Pallas kernels  17.4 us (19%)
  local copies, waits for them, and re-layouts  5.09 us (5%)
    all_to_all x1, blocking collectives, per_device(): parts = lax.all_to_all(joined, 'ep', 0, 0, tiled=True)  24.4 us
    pallas_call x7, Pallas kernels, call(): pl.pallas_call(kernel, in_specs=[pl.BlockSpec(memory_space=spaces.get(k,...  17.4 us
    all_to_all x1, waiting for transfers between devices, per_device(): own = lax.all_to_all(outgoing, 'ep', 0, 0, tiled=True)  14 us
    all_to_all x1, starting transfers between devices, per_device(): own = lax.all_to_all(outgoing, 'ep', 0, 0, tiled=True)  11.5 us
    ppermute x1, waiting for transfers between devices, per_device(): lax.ppermute(jnp.stack([x[PIECE:] for x in pieces]), 'ep', [(i, i ^ 16) f...  8.22 us
    ppermute x3, starting transfers between devices, per_device(): lax.ppermute(pieces[k], 'ep', [(i, (i + 32 * k) % DEVICES) for i in range...  4.19 us
    unnamed x10, local copies, waits for them, and re-layouts  3.72 us
    ppermute x3, waiting for transfers between devices, per_device(): lax.ppermute(pieces[k], 'ep', [(i, (i + 32 * k) % DEVICES) for i in range...  2.67 us
  transfers between devices with their start and end apart: 8, of which 5 were waited for; matrix products, arithmetic and copies ran while one was open for 0% of the time, Pallas kernels for 6%

profile of v7, /device:TPU:1, one launch (start us, length us, event | category | flops | bytes accessed | tf_op | source)
XLA Modules:
  0.0 93.3 jit_solution(8143809059255534625)
XLA Ops:
  0.7 0.1 pad_add_fusion.ids
  0.7 8.3 %shard_map.220 = (bf16[2,4,1152]{2,1,0:T(4,128)(2,1)S(1)}, f32[4,2048]{1,0:T(4,128)S(1)}, bf16[4,256]{1,0:T(4,128)(2,1)}, bf16[4,256]{1,0:T(4,128)(2,1)}, bf16[1...) custom-call(s32[4]{0:T(128)S(1)} %pad_add_fusion.ids, s32[4]{0:T(128)} %lengths_hbm.1, ...), custom_call_target="tpu_custom_call" | custom-call | tf_op jit(solution)/shard_map/pallas_call | solution.py:253
  9.1 0.0 copy-start
  9.1 1.2 %copy-done = bf16[384,2048]{1,0:T(8,128)(2,1)} copy-done((bf16[384,2048]{1,0:T(8,128)(2,1)}, bf16[384,2048]{1,0:T(8,128)(2,1)S(1)}, u32[]{:S(2)}) %copy-start) | copy-done | bytes 1572888
  10.2 0.0 copy-start.2
  10.2 1.1 %copy-done.2 = bf16[1024,768]{1,0:T(8,128)(2,1)} copy-done((bf16[1024,768]{1,0:T(8,128)(2,1)}, bf16[1024,768]{1,0:T(8,128)(2,1)S(1)}, u32[]{:S(2)}) %copy-start.2) | copy-done | bytes 1572888
  11.4 1.3 %broadcast_in_dim.2 = bf16[64,2,4,1152]{3,2,1,0:T(4,128)(2,1)} broadcast(bf16[2,4,1152]{2,1,0:T(4,128)(2,1)S(1)} %get-tuple-element.22), dimensions={1,2,3} | broadcast | bytes 1198080 | tf_op jit(solution)/shard_map/broadcast_in_dim | solution.py:307
  12.7 0.0 copy-start.4
  12.7 11.5 %all-to-all-start = ((bf16[128,4,1152]{2,1,0:T(4,128)(2,1)}), bf16[128,4,1152]{2,1,0:T(4,128)(2,1)S(1)}, u32[]{:S(2)}, u32[]{:S(2)}) async-start(bf16[128,4,1152]{2,1,0:T(4,128)(2,1)} %bitcast.27), calls=%async_computation | async-start | bytes 2359296 | tf_op jit(solution)/shard_map/all_to_all | solution.py:309
  24.2 2.4 %shard_map.221 = (bf16[288,256]{1,0:T(8,128)(2,1)S(1)}, bf16[288,256]{1,0:T(8,128)(2,1)S(1)}, bf16[288,256]{1,0:T(8,128)(2,1)}, bf16[288,256]{1,0:T(8,128)(2,1)}) custom-call(s32[4]{0:T(128)S(1)} %pad_add_fusion.ids, bf16[352,256]{1,0:T(8,128)(2,1)} %bitcast.30, bf16[352,256]{1,0:T(8,128)(2,1)} %bitcast.31, bf16[352,256]{1,0:T(8,128)(2,1)} %bitcast.32), custom_call_target="tpu_custom_call" | custom-call | tf_op jit(solution)/shard_map/pallas_call | solution.py:253
  26.6 3.3 %collective-permute-start.3 = (bf16[288,256]{1,0:T(8,128)(2,1)}, bf16[288,256]{1,0:T(8,128)(2,1)S(1)}, u32[]{:S(2)}, u32[]{:S(2)}) collective-permute-start(bf16[288,256]{1,0:T(8,128)(2,1)} %get-tuple-element.26), channel_id=1, source_target_pairs={{0,96},{1,97},{2,98},{3,99},{4,100},{5,101},{6,102},{7,103},{8,104... | collective-permute-start | bytes 442376 | tf_op jit(solution)/shard_map/ppermute | solution.py:281
  29.9 0.1 collective-permute-start.2
  30.0 0.8 collective-permute-start.1
  30.8 14.0 %all-to-all-done.own = bf16[128,4,1152]{2,1,0:T(4,128)(2,1)S(1)} async-done(((bf16[128,4,1152]{2,1,0:T(4,128)(2,1)}), bf16[128,4,1152]{2,1,0:T(4,128)(2,1)S(1)}, u32[]{:S(2)}, u32[]{:S(2)}) %all-to-all-start) | async-done | bytes 1179680 | tf_op jit(solution)/shard_map/all_to_all | solution.py:309
  44.8 1.0 %collective-permute-start = (bf16[128,4,1152]{2,1,0:T(4,128)(2,1)S(1)}, bf16[128,4,1152]{2,1,0:T(4,128)(2,1)S(1)}, u32[]{:S(2)}, u32[]{:S(2)}) collective-permute-start(bf16[128,4,1152]{2,1,0:T(4,128)(2,1)S(1)} %all-to-all-done.own), channel_id=1, source_target_pairs={{0,1},{1,0},{2,3},{3,2},{4,5},{5,4},{6,7},{7,6},{8,9},{9,8},{10,11... | collective-permute-start | bytes 3538952 | tf_op jit(solution)/shard_map/ppermute | solution.py:23
  45.8 0.0 collective-permute-done.3.fourth
  45.8 0.0 collective-permute-done.2.third
  45.9 2.7 %collective-permute-done.1.second = bf16[288,256]{1,0:T(8,128)(2,1)S(1)} collective-permute-done((bf16[288,256]{1,0:T(8,128)(2,1)S(1)}, bf16[288,256]{1,0:T(8,128)(2,1)S(1)}, u32[]{:S(2)}, u32[]{:S(2)}) %collective-permute-start.1) | collective-permute-done | bytes 147488 | tf_op jit(solution)/shard_map/ppermute | solution.py:281
  48.6 1.5 %collective-permute-start.4 = (bf16[4,144,256]{2,1,0:T(8,128)(2,1)S(1)}, bf16[4,144,256]{2,1,0:T(8,128)(2,1)S(1)}, u32[]{:S(2)}, u32[]{:S(2)}) collective-permute-start(bf16[4,144,256]{2,1,0:T(8,128)(2,1)S(1)} %pad_maximum_fusion), channel_id=1, source_target_pairs={{0,16},{1,17},{2,18},{3,19},{4,20},{5,21},{6,22},{7,23},{8,24},{9,... | collective-permute-start | bytes 884744 | tf_op jit(solution)/shard_map/ppermute | solution.py:308
  50.1 0.0 copy-done.4
  50.1 8.2 %collective-permute-done.4.crossed = bf16[4,144,256]{2,1,0:T(8,128)(2,1)S(1)} collective-permute-done((bf16[4,144,256]{2,1,0:T(8,128)(2,1)S(1)}, bf16[4,144,256]{2,1,0:T(8,128)(2,1)S(1)}, u32[]{:S(2)}, u32[]{:S(2)}) %collective-permute-start.4) | collective-permute-done | bytes 294944 | tf_op jit(solution)/shard_map/ppermute | solution.py:308
  58.3 0.0 copy-start.1
  58.3 1.4 %copy-done.1 = bf16[384,2048]{1,0:T(8,128)(2,1)S(1)} copy-done((bf16[384,2048]{1,0:T(8,128)(2,1)S(1)}, bf16[384,2048]{1,0:T(8,128)(2,1)}, u32[]{:S(2)}) %copy-start.1) | copy-done | bytes 1572888
  59.8 0.0 copy-start.3
  59.8 2.1 %shard_map.222 = (f32[512,768]{1,0:T(8,128)S(1)}, f32[512,256]{1,0:T(8,128)S(1)}, bf16[8,256,256]{2,1,0:T(8,128)(2,1)S(1)}, bf16[512,2048]{1,0:T(8,128)(2,1)S(1)}) custom-call(s32[4]{0:T(128)S(1)} %pad_add_fusion.ids, bf16[128,4,1152]{2,1,0:T(4,128)(2,1)S(1)} %all-to-all-done.own, bf16[288,256]{1,0:T(8,128)(2,1)S(1)} %get-tuple-element.23.first, ...), custom_call_target="tpu_custom_call" | custom-call | tf_op jit(solution)/shard_map/pallas_call | solution.py:253
  61.8 0.0 collective-permute-done.theirs
  61.8 0.0 copy-done.3
  61.8 2.4 %shard_map.223 = (bf16[512,512]{1,0:T(8,128)(2,1)S(1)}, bf16[512,512]{1,0:T(8,128)(2,1)S(1)}, bf16[512,512]{1,0:T(8,128)(2,1)S(1)}) custom-call(s32[4]{0:T(128)S(1)} %pad_add_fusion.ids, bf16[128,4,1152]{2,1,0:T(4,128)(2,1)S(1)} %collective-permute-done.theirs, f32[512,768]{1,0:T(8,128)S(1)} %get-tuple-element.29.sums_near, ...), custom_call_target="tpu_custom_call" | custom-call | tf_op jit(solution)/shard_map/pallas_call | solution.py:253
  64.2 1.3 %collective-permute-start.5 = (bf16[512,512]{1,0:T(8,128)(2,1)S(1)}, bf16[512,512]{1,0:T(8,128)(2,1)S(1)}, u32[]{:S(2)}, u32[]{:S(2)}) collective-permute-start(bf16[512,512]{1,0:T(8,128)(2,1)S(1)} %get-tuple-element.35), channel_id=1, source_target_pairs={{0,1},{1,0},{2,3},{3,2},{4,5},{5,4},{6,7},{7,6},{8,9},{9,8},{10,11... | collective-permute-start | bytes 1572872 | tf_op jit(solution)/shard_map/ppermute | solution.py:23
  65.6 0.1 collective-permute-start.6
  65.7 1.3 %shard_map.224.y_own = f32[512,1024]{1,0:T(8,128)S(1)} custom-call(s32[4]{0:T(128)S(1)} %pad_add_fusion.ids, bf16[512,512]{1,0:T(8,128)(2,1)S(1)} %get-tuple-element.34.acts, bf16[512,2048]{1,0:T(8,128)(2,1)S(1)} %get-tuple-element.33.w_out), custom_call_target="tpu_custom_call" | custom-call | tf_op jit(solution)/shard_map/pallas_call | solution.py:253
  66.9 0.2 collective-permute-done.5.first
  67.1 0.7 collective-permute-done.6.second
  67.9 0.2 shard_map.225
  68.1 24.4 %all_to_all.10.parts = bf16[128,4,1024]{2,1,0:T(4,128)(2,1)S(1)} all-to-all(bf16[128,4,1024]{2,1,0:T(4,128)(2,1)S(1)} %shard_map.225), channel_id=1, replica_groups=mesh['ep'=128] {'ep'}, dimensions={0} | all-to-all | bytes 2097152 | tf_op jit(solution)/shard_map/all_to_all | solution.py:331
  92.5 0.8 shard_map.226
  (6 shorter events, 0.1 us)
Async XLA Ops:
  9.1 1.2 %copy-start = (bf16[384,2048]{1,0:T(8,128)(2,1)}, bf16[384,2048]{1,0:T(8,128)(2,1)S(1)}, u32[]{:S(2)}) copy-start(bf16[384,2048]{1,0:T(8,128)(2,1)S(1)} %get-tuple-element.28.w_down) | copy-start | bytes 4718596
  10.2 1.1 %copy-start.2 = (bf16[1024,768]{1,0:T(8,128)(2,1)}, bf16[1024,768]{1,0:T(8,128)(2,1)S(1)}, u32[]{:S(2)}) copy-start(bf16[1024,768]{1,0:T(8,128)(2,1)S(1)} %get-tuple-element.32.w_rest) | copy-start | bytes 4718596
  12.7 37.4 %copy-start.4 = (bf16[2048]{0:T(1024)(128)(2,1)S(1)}, bf16[2048]{0:T(1024)(128)(2,1)}, u32[]{:S(2)}) copy-start(bf16[2048]{0:T(1024)(128)(2,1)} %param.41) | copy-start | bytes 12292
  12.7 32.1 %all-to-all-start = ((bf16[128,4,1152]{2,1,0:T(4,128)(2,1)}), bf16[128,4,1152]{2,1,0:T(4,128)(2,1)S(1)}, u32[]{:S(2)}, u32[]{:S(2)}) async-start(bf16[128,4,1152]{2,1,0:T(4,128)(2,1)} %bitcast.27), calls=%async_computation | async-start | bytes 2359296 | tf_op jit(solution)/shard_map/all_to_all | solution.py:309
  26.6 19.2 %collective-permute-start.3 = (bf16[288,256]{1,0:T(8,128)(2,1)}, bf16[288,256]{1,0:T(8,128)(2,1)S(1)}, u32[]{:S(2)}, u32[]{:S(2)}) collective-permute-start(bf16[288,256]{1,0:T(8,128)(2,1)} %get-tuple-element.26), channel_id=1, source_target_pairs={{0,96},{1,97},{2,98},{3,99},{4,100},{5,101},{6,102},{7,103},{8,104... | collective-permute-start | bytes 442376 | tf_op jit(solution)/shard_map/ppermute | solution.py:281
  29.9 15.9 %collective-permute-start.2 = (bf16[288,256]{1,0:T(8,128)(2,1)}, bf16[288,256]{1,0:T(8,128)(2,1)S(1)}, u32[]{:S(2)}, u32[]{:S(2)}) collective-permute-start(bf16[288,256]{1,0:T(8,128)(2,1)} %get-tuple-element.25), channel_id=1, source_target_pairs={{0,64},{1,65},{2,66},{3,67},{4,68},{5,69},{6,70},{7,71},{8,72},{9,... | collective-permute-start | bytes 442376 | tf_op jit(solution)/shard_map/ppermute | solution.py:281
  30.0 18.5 %collective-permute-start.1 = (bf16[288,256]{1,0:T(8,128)(2,1)S(1)}, bf16[288,256]{1,0:T(8,128)(2,1)S(1)}, u32[]{:S(2)}, u32[]{:S(2)}) collective-permute-start(bf16[288,256]{1,0:T(8,128)(2,1)S(1)} %get-tuple-element.24), channel_id=1, source_target_pairs={{0,32},{1,33},{2,34},{3,35},{4,36},{5,37},{6,38},{7,39},{8,40},{9,... | collective-permute-start | bytes 442376 | tf_op jit(solution)/shard_map/ppermute | solution.py:281
  44.8 17.0 %collective-permute-start = (bf16[128,4,1152]{2,1,0:T(4,128)(2,1)S(1)}, bf16[128,4,1152]{2,1,0:T(4,128)(2,1)S(1)}, u32[]{:S(2)}, u32[]{:S(2)}) collective-permute-start(bf16[128,4,1152]{2,1,0:T(4,128)(2,1)S(1)} %all-to-all-done.own), channel_id=1, source_target_pairs={{0,1},{1,0},{2,3},{3,2},{4,5},{5,4},{6,7},{7,6},{8,9},{9,8},{10,11... | collective-permute-start | bytes 3538952 | tf_op jit(solution)/shard_map/ppermute | solution.py:23
  48.6 9.8 %collective-permute-start.4 = (bf16[4,144,256]{2,1,0:T(8,128)(2,1)S(1)}, bf16[4,144,256]{2,1,0:T(8,128)(2,1)S(1)}, u32[]{:S(2)}, u32[]{:S(2)}) collective-permute-start(bf16[4,144,256]{2,1,0:T(8,128)(2,1)S(1)} %pad_maximum_fusion), channel_id=1, source_target_pairs={{0,16},{1,17},{2,18},{3,19},{4,20},{5,21},{6,22},{7,23},{8,24},{9,... | collective-permute-start | bytes 884744 | tf_op jit(solution)/shard_map/ppermute | solution.py:308
  58.3 1.4 %copy-start.1 = (bf16[384,2048]{1,0:T(8,128)(2,1)S(1)}, bf16[384,2048]{1,0:T(8,128)(2,1)}, u32[]{:S(2)}) copy-start(bf16[384,2048]{1,0:T(8,128)(2,1)} %copy-done) | copy-start | bytes 4718596
  59.8 2.1 %copy-start.3 = (bf16[1024,768]{1,0:T(8,128)(2,1)S(1)}, bf16[1024,768]{1,0:T(8,128)(2,1)}, u32[]{:S(2)}) copy-start(bf16[1024,768]{1,0:T(8,128)(2,1)} %copy-done.2) | copy-start | bytes 4718596
  64.2 2.9 %collective-permute-start.5 = (bf16[512,512]{1,0:T(8,128)(2,1)S(1)}, bf16[512,512]{1,0:T(8,128)(2,1)S(1)}, u32[]{:S(2)}, u32[]{:S(2)}) collective-permute-start(bf16[512,512]{1,0:T(8,128)(2,1)S(1)} %get-tuple-element.35), channel_id=1, source_target_pairs={{0,1},{1,0},{2,3},{3,2},{4,5},{5,4},{6,7},{7,6},{8,9},{9,8},{10,11... | collective-permute-start | bytes 1572872 | tf_op jit(solution)/shard_map/ppermute | solution.py:23
  65.6 2.3 %collective-permute-start.6 = (bf16[512,512]{1,0:T(8,128)(2,1)S(1)}, bf16[512,512]{1,0:T(8,128)(2,1)S(1)}, u32[]{:S(2)}, u32[]{:S(2)}) collective-permute-start(bf16[512,512]{1,0:T(8,128)(2,1)S(1)} %get-tuple-element.36), channel_id=1, source_target_pairs={{0,1},{1,0},{2,3},{3,2},{4,5},{5,4},{6,7},{7,6},{8,9},{9,8},{10,11... | collective-permute-start | bytes 1572872 | tf_op jit(solution)/shard_map/ppermute | solution.py:23
